TPU v7x, 128 devices: a whole 4x4x4 slice. The times are simulated.
128 devices in a mesh: ep: 32 (over z, y, core), tp: 4 (over x).
Axes of the slice: x: 4, y: 4, z: 4, core: 2. Of those that a mesh axis runs over, the one named last changes fastest.
Arguments:
- queries: bfloat16 [16384, 1024], P('ep', 'tp'), may hold values from -6 to 6
- key_rows: bfloat16 [16384, 512], P('ep', 'tp'), may hold values from -6 to 6
- value_rows: bfloat16 [16384, 512], P('ep', 'tp'), may hold values from -6 to 6
- forget_logit: float32 [8, 16384], P('tp', 'ep'), may hold values from -1 to 17
- out_weight: bfloat16 [1024, 2048], P('tp'), may hold values from -0.1875 to 0.1875
- out_gain: float32 [2048], replicated, may hold values from 0.1 to 1.9
- moe_input: bfloat16 [16384, 2048], P('ep'), may hold values from -6 to 6
- moe_gain: float32 [2048], replicated, may hold values from 0.1 to 1.9
- router_group: bfloat16 [2048, 4], replicated, may hold values from -2 to 2
- router_expert: bfloat16 [2048, 32], replicated, may hold values from -0.125 to 0.125
- route_group: int32 [16384], P('ep'), may hold values from 0 to 3
- route_pick: int32 [16384, 2], P('ep'), may hold values from 0 to 7, as said below
- expert_gate: bfloat16 [32, 2048, 1024], P('ep', None, 'tp'), may hold values from -0.125 to 0.125
- expert_up: bfloat16 [32, 2048, 1024], P('ep', None, 'tp'), may hold values from -0.125 to 0.125
- expert_down: bfloat16 [32, 1024, 2048], P('ep', 'tp'), may hold values from -42 to 42
Outputs:
- mixer_out: bfloat16 [16384, 2048], P(('ep', 'tp'))
- moe_out: bfloat16 [16384, 2048], P(('ep', 'tp'))
Inputs may be any that keep to these rules, and one draw needn't show every extreme that they name: `route_pick`: the two entries of a row differ.
All inputs are finite; a program needn't handle non-finite values.
Results may differ from a plain program's by a relative error of at most 0.013.
Values may be sent and summed in bfloat16 or wider, within the bound.
No kernel may reach another device: no remote copies, remote signals or barrier semaphores. Data moves between devices by JAX's collectives and lax.ppermute only.
A program may use at most 128 MiB of HBM per device.

v0:
```python
import math

import jax
import jax.numpy as jnp
from jax import lax
from jax.sharding import PartitionSpec as P

DH = 128
GROUPS = 4


def copy_for_each(shard, axis):
    copies = jnp.broadcast_to(shard, (lax.axis_size(axis), *shard.shape))
    return lax.all_to_all(copies, axis, split_axis=0, concat_axis=0, tiled=True)


def in_order(tiles, dim):
    dims = list(tiles.shape[1:])
    dims[dim] *= tiles.shape[0]
    return jnp.moveaxis(tiles, 0, dim).reshape(dims)


def collect(shard, axis, dim):
    tiles = copy_for_each(shard, axis)
    return in_order(tiles, dim)


def in_one_piece(arrays, axis, dim, along):
    both = jnp.concatenate(arrays, axis=along)
    result, at, outs = (lax.all_gather(both, axis, axis=dim, tiled=True), 0, [])
    for a in arrays:
        outs.append(lax.slice_in_dim(result, at, at + a.shape[along], axis=along))
        at += a.shape[along]
    return tuple(outs)


def rms_scale(row_block, scale_gain):
    values = row_block.astype(jnp.float32)
    return (
        values * lax.rsqrt(jnp.mean(values * values, axis=-1, keepdims=True) + 1e-06) * scale_gain
    )


def slot_ranks(chosen, block_rows, experts):
    expert_ids = jnp.arange(experts, dtype=jnp.int32)
    matches = chosen[:, :, None] == expert_ids
    usage = jnp.any(matches, axis=1).astype(jnp.int32)
    grouped = usage.reshape(-1, block_rows, experts)
    before = (jnp.cumsum(grouped, axis=1) - grouped).reshape(-1, experts)
    return jnp.sum(jnp.where(matches, before[:, None, :], 0), axis=2)


def expert_hidden(arrived, gate_part, up_part):
    flat = arrived.reshape(-1, arrived.shape[-1])
    gated = jnp.dot(flat, gate_part, preferred_element_type=jnp.float32)
    lifted = jnp.dot(flat, up_part, preferred_element_type=jnp.float32)
    hidden = (jax.nn.silu(gated) * lifted).astype(jnp.bfloat16)
    return hidden.reshape(arrived.shape[:-1] + (gate_part.shape[1],))


def body(
    queries,
    key_rows,
    value_rows,
    forget_logit,
    out_weight,
    out_gain,
    moe_input,
    moe_gain,
    router_group,
    router_expert,
    route_group,
    route_pick,
    expert_gate,
    expert_up,
    expert_down,
):
    tp_count = lax.axis_size("tp")
    ep_count = lax.axis_size("ep")
    tp_index = lax.axis_index("tp")
    ep_index = lax.axis_index("ep")
    rows_group = queries.shape[0]
    query_heads = forget_logit.shape[0]
    key_heads = key_rows.shape[1] // DH
    ratio = query_heads // key_heads
    own_start = ep_index * rows_group
    own_pos = own_start + jnp.arange(rows_group, dtype=jnp.int32)
    local_cum = jnp.cumsum(jax.nn.log_sigmoid(forget_logit), axis=1)
    every_cum = collect(local_cum, "ep", 1).reshape(query_heads, ep_count, rows_group)
    shard_totals = every_cum[:, :, -1]
    offsets = jnp.cumsum(shard_totals, axis=1) - shard_totals
    cum_gate = (every_cum + offsets[:, :, None]).reshape(query_heads, ep_count * rows_group)
    own_cum = lax.dynamic_slice_in_dim(cum_gate, own_start, rows_group, 1).reshape(
        key_heads, ratio, rows_group, 1
    )
    query_stack = (
        queries.reshape(rows_group, key_heads, ratio, DH)
        .transpose(1, 2, 0, 3)
        .reshape(key_heads, ratio * rows_group, DH)
    )

    def attend_block(current, keys_block, values_block, start):
        piece_rows = keys_block.shape[0]

        def compute(state):
            row_top, row_total, weighted = state
            key_stack = keys_block.reshape(piece_rows, key_heads, DH).transpose(1, 0, 2)
            value_stack = values_block.reshape(piece_rows, key_heads, DH).transpose(1, 0, 2)
            scores = jnp.einsum(
                "gqd,gkd->gqk", query_stack, key_stack, preferred_element_type=jnp.float32
            ) / math.sqrt(DH)
            key_cum = lax.dynamic_slice_in_dim(cum_gate, start, piece_rows, 1).reshape(
                key_heads, ratio, 1, piece_rows
            )
            logits = scores.reshape(key_heads, ratio, rows_group, piece_rows) + own_cum - key_cum
            visible = (start + jnp.arange(piece_rows, dtype=jnp.int32))[None, :] <= own_pos[:, None]
            logits = jnp.where(visible, logits, -1e30)
            new_top = jnp.maximum(row_top, jnp.max(logits, axis=3))
            expo = jnp.where(visible, jnp.exp(logits - new_top[..., None]), 0.0)
            rescale = jnp.exp(row_top - new_top)
            row_total = row_total * rescale + jnp.sum(expo, axis=3)
            product = jnp.einsum(
                "gqk,gkd->gqd",
                expo.reshape(key_heads, ratio * rows_group, piece_rows).astype(jnp.bfloat16),
                value_stack,
                preferred_element_type=jnp.float32,
            )
            weighted = weighted * rescale.reshape(key_heads, ratio * rows_group, 1) + product
            return (new_top, row_total, weighted)

        return lax.cond(start < own_start + rows_group, compute, lambda state: state, current)

    initial = (
        jnp.full((key_heads, ratio, rows_group), -1e30, jnp.float32),
        jnp.zeros((key_heads, ratio, rows_group), jnp.float32),
        jnp.zeros((key_heads, ratio * rows_group, DH), jnp.float32),
    )
    current = initial
    keys_piece, values_piece = in_one_piece((key_rows, value_rows), "ep", 0, 1)
    piece_rows = keys_piece.shape[0]
    blocks = piece_rows // rows_group

    def advance(state, inputs):
        keys_block, values_block, block_index = inputs
        return (attend_block(state, keys_block, values_block, block_index * rows_group), None)

    current, _ = lax.scan(
        advance,
        current,
        (
            keys_piece.reshape(blocks, rows_group, -1),
            values_piece.reshape(blocks, rows_group, -1),
            jnp.arange(blocks, dtype=jnp.int32),
        ),
    )
    row_top, row_total, weighted = current
    attended = (weighted / row_total.reshape(key_heads, ratio * rows_group, 1)).astype(jnp.bfloat16)
    attended = (
        attended.reshape(key_heads, ratio, rows_group, DH)
        .transpose(2, 0, 1, 3)
        .reshape(rows_group, query_heads * DH)
    )
    group_rows = moe_input.shape[0]
    own_rows = group_rows // tp_count
    width_model = moe_input.shape[1]
    experts = expert_gate.shape[0] * ep_count
    per_group = experts // GROUPS
    capacity = tp_count * own_rows // experts
    own_first = tp_index * own_rows
    chosen_all = route_group[:, None] * per_group + route_pick
    rank_all = slot_ranks(chosen_all, own_rows, experts)
    chosen = lax.dynamic_slice_in_dim(chosen_all, own_first, own_rows, 0)
    ranks = lax.dynamic_slice_in_dim(rank_all, own_first, own_rows, 0)
    is_kept = ranks < capacity
    own_group = lax.dynamic_slice_in_dim(route_group, own_first, own_rows, 0)
    normed = rms_scale(
        lax.dynamic_slice_in_dim(moe_input, own_first, own_rows, 0), moe_gain
    ).astype(jnp.bfloat16)
    target = jnp.where(is_kept, chosen * capacity + ranks, experts * capacity)
    sources = jnp.broadcast_to(jnp.arange(own_rows, dtype=jnp.int32)[:, None], target.shape)
    slot_table = (
        jnp.full((experts * capacity,), own_rows, jnp.int32)
        .at[target.reshape(-1)]
        .set(sources.reshape(-1), mode="drop")
    )
    padded = jnp.concatenate([normed, jnp.zeros((1, width_model), jnp.bfloat16)], axis=0)
    outgoing = padded[slot_table].reshape(experts, capacity, width_model)
    arrived = lax.all_to_all(outgoing, "ep", split_axis=0, concat_axis=0, tiled=True)
    hidden_arrived = lax.all_gather(arrived[None], "tp", axis=0, tiled=True)
    hidden = expert_hidden(hidden_arrived, expert_gate[0], expert_up[0])
    hidden_rows = hidden.reshape(-1, hidden.shape[-1])
    mixer_term = jnp.dot(attended, out_weight, preferred_element_type=jnp.float32)
    expert_term = jnp.dot(hidden_rows, expert_down[0], preferred_element_type=jnp.float32)
    mixer_summed, expert_summed = (
        lax.psum_scatter(
            mixer_term.astype(jnp.bfloat16), "tp", scatter_dimension=0, tiled=True
        ).astype(jnp.float32),
        lax.psum_scatter(
            expert_term.astype(jnp.bfloat16), "tp", scatter_dimension=0, tiled=True
        ).astype(jnp.float32),
    )
    mixer_out = rms_scale(mixer_summed, out_gain).astype(jnp.bfloat16)
    group_logits = jnp.dot(normed, router_group, preferred_element_type=jnp.float32)
    expert_logits = jnp.dot(normed, router_expert, preferred_element_type=jnp.float32)
    group_top = jnp.max(group_logits, axis=1, keepdims=True)
    group_exp = jnp.exp(group_logits - group_top)
    group_hit = jnp.arange(GROUPS, dtype=jnp.int32)[None, :] == own_group[:, None]
    group_share = jnp.sum(jnp.where(group_hit, group_exp, 0.0), axis=1) / jnp.sum(group_exp, axis=1)
    expert_hit = jnp.arange(experts, dtype=jnp.int32)[None, None, :] == chosen[:, :, None]
    picked_logits = jnp.sum(jnp.where(expert_hit, expert_logits[:, None, :], 0.0), axis=2)
    shares = group_share[:, None] * jax.nn.sigmoid(picked_logits - picked_logits[:, ::-1])
    results = expert_summed.astype(jnp.bfloat16).reshape(ep_count, capacity, width_model)
    returned = lax.all_to_all(results, "ep", split_axis=0, concat_axis=0, tiled=True).reshape(
        experts * capacity, width_model
    )
    slot_index = jnp.where(is_kept, chosen * capacity + ranks, 0)
    picked = returned[slot_index]
    moe_out = jnp.sum(
        jnp.where(is_kept, shares, 0.0)[:, :, None] * picked.astype(jnp.float32), axis=1
    )
    return (mixer_out, moe_out.astype(jnp.bfloat16))


def solution(mesh):
    in_specs = (
        P("ep", "tp"),
        P("ep", "tp"),
        P("ep", "tp"),
        P("tp", "ep"),
        P("tp", None),
        P(),
        P("ep", None),
        P(),
        P(),
        P(),
        P("ep"),
        P("ep", None),
        P("ep", None, "tp"),
        P("ep", None, "tp"),
        P("ep", "tp", None),
    )
    out_specs = (P(("ep", "tp"), None), P(("ep", "tp"), None))
    return jax.shard_map(body, mesh=mesh, in_specs=in_specs, out_specs=out_specs, check_vma=False)
```

profile of v0, /device:TPU:0, one launch (start us, length us, event | category | flops | bytes accessed | tf_op | source)
XLA Modules:
  0.0 519.4 jit_solution(8422510485102352049)
XLA Ops:
  7.3 0.8 broadcast_multiply_fusion
  8.0 0.8 dynamic_slice.47
  9.5 1.2 fusion.22
  10.7 1.3 fusion.24
  13.7 1.4 scatter_custom_fusion
  15.2 3.3 gather_fusion
  18.5 37.0 %all_to_all.15 = bf16[32,16,2048]{2,1,0:T(8,128)(2,1)} all-to-all(bf16[32,16,2048]{2,1,0:T(8,128)(2,1)} %bitcast.90), channel_id=1, replica_groups=mesh['ep'=32,'tp'=4] {'ep'}, dimensions={0} | all-to-all | bytes 4194304 | tf_op jit(solution)/shard_map/all_to_all | solution.py:188
  55.5 0.8 copy-done.4
  56.4 0.7 pad_maximum_fusion
  57.2 79.2 %all-gather.6.cloned.1.call-done = bf16[128,16,2048]{2,1,0:T(8,128)(2,1)} async-done(((bf16[32,16,2048]{2,1,0:T(8,128)(2,1)}), bf16[128,16,2048]{2,1,0:T(8,128)(2,1)}) %all-gather.6.cloned.1.call-update) | async-done | bytes 8388624 | tf_op jit(solution)/shard_map/all_gather | solution.py:189
  136.4 7.2 %fusion.28 = f32[2048,256]{1,0:T(8,128)} fusion(bf16[2048,2048]{1,0:T(8,128)(2,1)} %bitcast.112, bf16[1,2048,256]{2,1,0:T(8,128)(2,1)S(1)} %copy-done.9), kind=kOutput, calls=%fused_computation.45 | convolution fusion | flops 2147483648 | bytes 11534336 | tf_op jit(solution)/shard_map/dot_general | solution.py:55
  143.6 13.2 %convolution_convert_fusion = bf16[2048,2048]{1,0:T(8,128)(2,1)} fusion(bf16[2048,2048]{1,0:T(8,128)(2,1)} %bitcast.113, f32[2048,256]{1,0:T(8,128)} %fusion.28, bf16[1,256,2048]{2,1,0:T(8,128)(2,1)S(1)} %copy-done, bf16[1,2048,256]{2,1,0:T(8,128)(2,1)S(1)} %copy-done.10), kind=kOutput, calls=%fused_computation.28 | convolution fusion | flops 4302307328 | bytes 20971520 | tf_op jit(solution)/shard_map/dot_general | solution.py:193
  159.3 7.3 %all-to-all-start = ((f32[32,2,512]{2,1,0:T(2,128)}), f32[32,2,512]{2,1,0:T(2,128)S(1)}, u32[]{:S(2)}, u32[]{:S(2)}) async-start(f32[32,2,512]{2,1,0:T(2,128)} %broadcast_in_dim.107), calls=%async_computation | async-start | bytes 262144 | tf_op jit(solution)/shard_map/all_to_all | solution.py:14
  166.9 7.4 %all-to-all-done = f32[32,2,512]{2,1,0:T(2,128)S(1)} async-done(((f32[32,2,512]{2,1,0:T(2,128)}), f32[32,2,512]{2,1,0:T(2,128)S(1)}, u32[]{:S(2)}, u32[]{:S(2)}) %all-to-all-start) | async-done | bytes 131104 | tf_op jit(solution)/shard_map/all_to_all | solution.py:14
  174.8 5.0 copy.60
  179.9 13.3 %all-gather.4.cloned.1.call-done = bf16[16384,256]{1,0:T(8,128)(2,1)} async-done(((bf16[512,256]{1,0:T(8,128)(2,1)}), bf16[16384,256]{1,0:T(8,128)(2,1)}) %all-gather.4.cloned.1.call-update) | async-done | bytes 8388624 | tf_op jit(solution)/shard_map/all_gather | solution.py:30
  193.2 5.7 %fusion.40 = (bf16[16384,128]{1,0:T(8,128)(2,1)}, bf16[16384,128]{1,0:T(8,128)(2,1)}) fusion(bf16[16384,256]{1,0:T(8,128)(2,1)} %all-gather.4.cloned.1.call-done), kind=kLoop, calls=%fused_computation.88 | loop fusion | bytes 16777216 | tf_op jit(solution)/shard_map/slice | solution.py:32
  199.0 48.6 %while.17 = (s32[]{:T(128)}, f32[1,2,512]{2,1,0:T(2,128)S(1)}, f32[1,2,512]{2,1,0:T(2,128)S(1)}, f32[1,1024,128]{2,1,0:T(8,128)S(1)}, s32[32]{0:T(128)S(1)}, /*i...) while((s32[]{:T(128)}, f32[1,2,512]{2,1,0:T(2,128)S(1)}, ...), condition=%wide.region_8.9_spmd.clone, body=%wide.region_3.8_spmd.clone.sunk | while | flops 274731008 | bytes 20051320 | solution.py:147
  200.2 7.1 %conditional.3 = ((f32[1,2,512]{2,1,0:T(2,128)S(1)}, f32[1,2,512]{2,1,0:T(2,128)S(1)}, f32[1,1024,128]{2,1,0:T(8,128)S(1)})) conditional(s32[]{:T(128)} %convert_element_type.102, (f32[1,2,512]{2,1,0:T(2,128)S(1)}, f32[1,2,512]{2,1,0:T(2,128)S(1)}, f32[1,1024,128]{2,1,0:T(8,128)S(1)}) %tuple.61, (s32[]{:T(128)}, s32[]{:T(128)}, ...), branch_computations={%region_4.4_spmd, %region_5.7_spmd} | conditional | flops 274731008 | bytes 20048974 | solution.py:131
  201.3 1.0 constant_dynamic-slice_fusion
  203.5 1.7 fusion.39
  205.7 1.6 fusion.5
  248.0 3.4 convolution_convert_fusion.1
  251.4 24.3 %reduce-scatter.5.cloned.1.call-done = bf16[512,2048]{1,0:T(8,128)(2,1)} async-done(((bf16[2048,2048]{1,0:T(8,128)(2,1)}), bf16[512,2048]{1,0:T(8,128)(2,1)}) %reduce-scatter.5.cloned.1.call-update) | async-done | bytes 2097168 | tf_op jit(solution)/shard_map/reduce_scatter | solution.py:198
  275.7 198.4 %all-to-all-start.2 = ((bf16[32,16,2048]{2,1,0:T(8,128)(2,1)}), bf16[32,16,2048]{2,1,0:T(8,128)(2,1)S(1)}, u32[]{:S(2)}, u32[]{:S(2)}) async-start(bf16[32,16,2048]{2,1,0:T(8,128)(2,1)} %bitcast.93), calls=%async_computation.4 | async-start | bytes 4194304 | tf_op jit(solution)/shard_map/all_to_all | solution.py:213
  474.5 23.4 %reduce-scatter.3.cloned.1.call-done = bf16[128,2048]{1,0:T(8,128)(2,1)} async-done(((bf16[512,2048]{1,0:T(8,128)(2,1)}), bf16[128,2048]{1,0:T(8,128)(2,1)}) %reduce-scatter.3.cloned.1.call-update) | async-done | bytes 524304 | tf_op jit(solution)/shard_map/reduce_scatter | solution.py:195
  497.9 1.2 fusion.19
  499.1 2.0 fusion.21
  501.1 3.0 all-to-all-done.2
  504.2 2.3 gather_fusion.1
  506.5 2.5 reshape.314
  509.0 3.9 multiply_reduce_fusion
  (194 shorter events, 28.8 us)
Async XLA Ops:
  7.2 136.5 %copy-start = (bf16[1,256,2048]{2,1,0:T(8,128)(2,1)S(1)}, bf16[1,256,2048]{2,1,0:T(8,128)(2,1)}, u32[]{:S(2)}) copy-start(bf16[1,256,2048]{2,1,0:T(8,128)(2,1)} %param.33) | copy-start | bytes 3145732
  7.2 4.9 copy-start.3
  7.2 5.2 %copy-start.6 = (bf16[2048,4]{0,1:T(4,128)(2,1)S(1)}, bf16[2048,4]{0,1:T(4,128)(2,1)}, u32[]{:S(2)}) copy-start(bf16[2048,4]{0,1:T(4,128)(2,1)} %param.27) | copy-start | bytes 49156
  7.2 129.2 %all-gather.6.cloned.1.call-start = ((), (), s32[]{:S(2)}) async-start(), calls=%async_computation.8 | async-start | bytes 10485760 | tf_op jit(solution)/shard_map/all_gather | solution.py:189
  55.5 0.9 copy-start.4
  55.5 1.0 copy-start.5
  55.5 81.0 %copy-start.9 = (bf16[1,2048,256]{2,1,0:T(8,128)(2,1)S(1)}, bf16[1,2048,256]{2,1,0:T(8,128)(2,1)}, u32[]{:S(2)}) copy-start(bf16[1,2048,256]{2,1,0:T(8,128)(2,1)} %param.31) | copy-start | bytes 3145732
  55.5 137.7 %all-gather.4.cloned.1.call-start = ((), (), s32[]{:S(2)}) async-start(), calls=%async_computation.5 | async-start | bytes 8650752 | tf_op jit(solution)/shard_map/all_gather | solution.py:30
  57.2 218.5 %reduce-scatter.5.cloned.1.call-start = ((), (), s32[]{:S(2)}) async-start(), calls=%async_computation.7 | async-start | bytes 10485760 | tf_op jit(solution)/shard_map/reduce_scatter | solution.py:198
  136.4 7.2 %copy-start.10 = (bf16[1,2048,256]{2,1,0:T(8,128)(2,1)S(1)}, bf16[1,2048,256]{2,1,0:T(8,128)(2,1)}, u32[]{:S(2)}) copy-start(bf16[1,2048,256]{2,1,0:T(8,128)(2,1)} %param.32) | copy-start | bytes 3145732
  156.8 0.7 copy-start.8
  156.8 10.0 %copy-start.2 = (bf16[512,256]{1,0:T(8,128)(2,1)S(1)}, bf16[512,256]{1,0:T(8,128)(2,1)}, u32[]{:S(2)}) copy-start(bf16[512,256]{1,0:T(8,128)(2,1)} %param.19) | copy-start | bytes 786436
  159.3 15.0 %all-to-all-start = ((f32[32,2,512]{2,1,0:T(2,128)}), f32[32,2,512]{2,1,0:T(2,128)S(1)}, u32[]{:S(2)}, u32[]{:S(2)}) async-start(f32[32,2,512]{2,1,0:T(2,128)} %broadcast_in_dim.107), calls=%async_computation | async-start | bytes 262144 | tf_op jit(solution)/shard_map/all_to_all | solution.py:14
  166.5 331.3 %reduce-scatter.3.cloned.1.call-start = ((), (), s32[]{:S(2)}) async-start(), calls=%async_computation.6 | async-start | bytes 2621440 | tf_op jit(solution)/shard_map/reduce_scatter | solution.py:195
  275.7 223.4 %copy-start.7 = (f32[2048]{0:T(1024)S(1)}, f32[2048]{0:T(1024)}, u32[]{:S(2)}) copy-start(f32[2048]{0:T(1024)} %param.24) | copy-start | bytes 24580
  275.7 228.5 %all-to-all-start.2 = ((bf16[32,16,2048]{2,1,0:T(8,128)(2,1)}), bf16[32,16,2048]{2,1,0:T(8,128)(2,1)S(1)}, u32[]{:S(2)}, u32[]{:S(2)}) async-start(bf16[32,16,2048]{2,1,0:T(8,128)(2,1)} %bitcast.93), calls=%async_computation.4 | async-start | bytes 4194304 | tf_op jit(solution)/shard_map/all_to_all | solution.py:213
  506.5 6.4 %copy-start.1 = (bf16[1,256,2048]{2,1,0:T(8,128)(2,1)S(1)}, bf16[1,256,2048]{2,1,0:T(8,128)(2,1)}, u32[]{:S(2)}) copy-start(bf16[1,256,2048]{2,1,0:T(8,128)(2,1)} %param.33) | copy-start | bytes 3145732
Sparse Core Ops, SparseCore 0:
  55.6 80.7 all-gather.5
  139.3 53.9 all-gather.3
  195.7 79.9 reduce-scatter.4
  277.9 219.9 reduce-scatter.2
where the time goes:
time: 523 us; the launch traced here: 519 us
  starting transfers between devices  206 us (39%)
  waiting for transfers between devices  151 us (29%)
  local copies, waits for them, and re-layouts  46.8 us (9%)
  blocking collectives  37 us (7%)
  matrix products  27.6 us (5%)
  loops' own time  22.8 us (4%)
  other arithmetic  14.5 us (3%)
  between operations  14.1 us (3%)
    all_to_all x1, starting transfers between devices, body(): lax.all_to_all(results, 'ep', split_axis=0, concat_axis=0, tiled=True)  198 us
    all_gather x1, waiting for transfers between devices, body(): hidden_arrived = lax.all_gather(arrived[None], 'tp', axis=0, tiled=True)  79.2 us
    all_to_all x1, blocking collectives, body(): lax.all_to_all(outgoing, 'ep', split_axis=0, concat_axis=0, tiled=True)  37 us
    reduce_scatter x1, waiting for transfers between devices, body(): lax.psum_scatter(expert_term.astype(jnp.bfloat16), 'tp', scatter_dimensio...  24.3 us
    reduce_scatter x1, waiting for transfers between devices, body(): lax.psum_scatter(mixer_term.astype(jnp.bfloat16), 'tp', scatter_dimension...  23.4 us
    another operation x1, loops' own time, body(): lax.scan(advance, current, (keys_piece.reshape(blocks, rows_group, -1), v...  22.1 us
    dynamic_slice x32, local copies, waits for them, and re-layouts, body(): lax.scan(advance, current, (keys_piece.reshape(blocks, rows_group, -1), v...  18.8 us
    all_gather x1, waiting for transfers between devices, in_one_piece(): result, at, outs = (lax.all_gather(both, axis, axis=dim, tiled=True), 0, [])  13.3 us
  transfers between devices with their start and end apart: 6, of which 6 were waited for; matrix products, arithmetic and copies ran while one was open for 13% of the time, Pallas kernels for 0%

commit v1 on v0

v1 whole, which is shorter than its diff:
```python
import math
import jax
import jax.numpy as jnp
from jax import lax
from jax.experimental import pallas as pl
from jax.experimental.pallas import tpu as pltpu
from jax.sharding import PartitionSpec as P

DH = 128
GROUPS = 4
BLOCK = 512
ROOT = math.sqrt(DH)
LOG2E = 1.4426950408889634
SCALE = LOG2E / ROOT
QT = 256


def attention_kernel(own_ref, q_ref, w_ref, kv_hbm, out_ref, buf, sems, top, gap, acc):
    own = own_ref[0]
    width = q_ref.shape[1]
    half = width // 2

    def copy(j):
        return pltpu.make_async_copy(kv_hbm.at[j], buf.at[j], sems.at[j])

    def launch(i, carry):
        copy(own - i).start()
        return carry

    lax.fori_loop(0, own + 1, launch, 0)
    top[...] = jnp.full_like(top, -1e30)
    gap[...] = jnp.zeros_like(gap)
    acc[...] = jnp.zeros_like(acc)

    def block(j, masked):
        copy(j).wait()
        gates = buf[j, BLOCK:, :]
        gates = jnp.concatenate([gates, jnp.zeros((DH - 16, 2 * DH), jnp.bfloat16)], axis=0)
        turned = jnp.transpose(gates.astype(jnp.float32)).astype(jnp.bfloat16)
        lane = lax.broadcasted_iota(jnp.int32, turned.shape, 1)
        zero = jnp.zeros_like(turned)
        extra = jnp.concatenate(
            [jnp.where(lane < 8, turned, zero), jnp.where(lane < 8, zero, turned)], axis=0
        )
        keys = jnp.concatenate([buf[j, :BLOCK, :DH], extra], axis=1)
        values = jnp.concatenate(
            [buf[j, c * DH : (c + 1) * DH, DH:] for c in range(BLOCK // DH)]
            , axis=1)
        values = jnp.concatenate([values, jnp.ones((16, BLOCK), jnp.bfloat16)], axis=0)
        if not masked:
            last = buf[j, BLOCK:, 2 * DH - DH :].astype(jnp.float32)
            for h in range(2):
                total = (
                    last[8 + 3 * h : 9 + 3 * h, DH - 1 : DH]
                    + last[9 + 3 * h : 10 + 3 * h, DH - 1 : DH]
                    + last[10 + 3 * h : 11 + 3 * h, DH - 1 : DH]
                )
                gap[:, h * half : (h + 1) * half] = gap[:, h * half : (h + 1) * half] + total
        for t in range(width // QT):
            cols = slice(t * QT, (t + 1) * QT)
            s = jnp.dot(keys, q_ref[:, cols], preferred_element_type=jnp.float32)
            if masked:
                key_at = lax.broadcasted_iota(jnp.int32, s.shape, 0)
                query_at = lax.broadcasted_iota(jnp.int32, s.shape, 1) + (t * QT) % half
                s = jnp.where(key_at <= query_at, s, -1e30)
            old = top[:, cols]
            new = jnp.maximum(old, jnp.max(s, axis=0, keepdims=True) + gap[:, cols])
            top[:, cols] = new
            shift = (new - gap[:, cols]) * SCALE
            p = jnp.exp2(s * SCALE - shift)
            part = jnp.dot(values, p.astype(jnp.bfloat16), preferred_element_type=jnp.float32)
            acc[:, cols] = acc[:, cols] * jnp.exp2((old - new) * SCALE) + part

    block(own, True)

    def step(i, carry):
        block(own - i, False)
        return carry

    lax.fori_loop(1, own + 1, step, 0)
    total = acc[DH : DH + 1, :]
    attended = acc[:DH, :] / total
    stacked = jnp.concatenate([attended[:, :half], attended[:, half:]], axis=0)
    rows = jnp.transpose(stacked).astype(jnp.bfloat16)
    out_ref[...] = jnp.dot(rows, w_ref[...], preferred_element_type=jnp.float32).astype(jnp.bfloat16)


def three(x):
    hi = lax.reduce_precision(x, 8, 7)
    mid = lax.reduce_precision(x - hi, 8, 7)
    return jnp.stack([hi, mid, x - hi - mid], axis=-2).astype(jnp.bfloat16)


def pack(keys, values, gates):
    turned = values.reshape(BLOCK // DH, DH, DH).transpose(0, 2, 1).reshape(BLOCK, DH)
    parts = three(gates * ROOT).reshape(6, 2, 2 * DH).transpose(1, 0, 2)
    parts = jnp.pad(parts, ((0, 0), (0, 2), (0, 0))).reshape(16, 2 * DH)
    return jnp.concatenate([jnp.concatenate([keys, turned], axis=1), parts], axis=0)


def widen(queries):
    rows = queries.shape[0]
    q = queries.reshape(rows, 2, DH).transpose(2, 1, 0).reshape(DH, 2 * rows)
    line = jnp.arange(DH, dtype=jnp.int32)[:, None]
    head = (jnp.arange(2 * rows, dtype=jnp.int32) // rows)[None, :]
    idx = line % 8
    pick = (line < 16) & (idx >= 3 * head) & (idx < 3 * head + 3)
    return jnp.concatenate([q, jnp.where(pick, -1.0, 0.0).astype(jnp.bfloat16)], axis=0)


def attention(own, q, w, kv):
    n = kv.shape[0]
    width = q.shape[1]
    return pl.pallas_call(
        attention_kernel,
        out_shape=jax.ShapeDtypeStruct((width // 2, w.shape[1]), jnp.bfloat16),
        in_specs=[
            pl.BlockSpec(memory_space=pltpu.SMEM),
            pl.BlockSpec(memory_space=pltpu.VMEM),
            pl.BlockSpec(memory_space=pltpu.VMEM),
            pl.BlockSpec(memory_space=pl.ANY),
        ],
        out_specs=pl.BlockSpec(memory_space=pltpu.VMEM),
        scratch_shapes=[
            pltpu.VMEM(kv.shape, jnp.bfloat16),
            pltpu.SemaphoreType.DMA((n,)),
            pltpu.VMEM((1, width), jnp.float32),
            pltpu.VMEM((1, width), jnp.float32),
            pltpu.VMEM((DH + 16, width), jnp.float32),
        ],
        compiler_params=pltpu.CompilerParams(vmem_limit_bytes=40 << 20),
        cost_estimate=pl.CostEstimate(flops=9_000_000_000, bytes_accessed=12_000_000, transcendentals=16_000_000),
    )(own, q, w, kv)


def shift(x, by):
    count = lax.axis_size("tp")
    return lax.ppermute(x, "tp", [(i, (i + by) % count) for i in range(count)])


def rms_scale(row_block, scale_gain):
    values = row_block.astype(jnp.float32)
    return (
        values * lax.rsqrt(jnp.mean(values * values, axis=-1, keepdims=True) + 1e-06) * scale_gain
    )


def expert_part(rows, gate, up, down):
    gated = jnp.dot(rows, gate, preferred_element_type=jnp.float32)
    lifted = jnp.dot(rows, up, preferred_element_type=jnp.float32)
    hidden = (jax.nn.silu(gated) * lifted).astype(jnp.bfloat16)
    return jnp.dot(hidden, down, preferred_element_type=jnp.float32)


def body(
    queries,
    key_rows,
    value_rows,
    forget_logit,
    out_weight,
    out_gain,
    moe_input,
    moe_gain,
    router_group,
    router_expert,
    route_group,
    route_pick,
    expert_gate,
    expert_up,
    expert_down,
):
    tp_count = lax.axis_size("tp")
    ep_count = lax.axis_size("ep")
    tp_index = lax.axis_index("tp")
    ep_index = lax.axis_index("ep")
    group_rows, width_model = moe_input.shape
    own_rows = group_rows // tp_count
    experts = ep_count
    per_group = experts // GROUPS
    capacity = tp_count * own_rows // experts
    slots = experts * capacity

    gate, up, down = expert_gate[0], expert_up[0], expert_down[0]
    half = gate.shape[1] // 2
    left = [shift(w, 1) for w in (gate, up, down)]
    right = [shift(w, -1) for w in (gate, up, down)]
    far_a = [shift(left[0][:, :half], 1), shift(left[1][:, :half], 1), shift(left[2][:half], 1)]
    far_b = [shift(right[0][:, half:], -1), shift(right[1][:, half:], -1), shift(right[2][half:], -1)]

    running = jnp.cumsum(jax.nn.log_sigmoid(forget_logit), axis=1)
    packed = pack(key_rows, value_rows, running)
    gathered = lax.all_gather(packed, "ep", axis=0, tiled=True).reshape(ep_count, *packed.shape)

    own_first = tp_index * own_rows
    own_group = lax.dynamic_slice_in_dim(route_group, own_first, own_rows, 0)
    own_pick = lax.dynamic_slice_in_dim(route_pick, own_first, own_rows, 0)
    chosen = own_group[:, None] * per_group + own_pick
    expert_hit = chosen[:, :, None] == jnp.arange(experts, dtype=jnp.int32)
    usage = jnp.any(expert_hit, axis=1).astype(jnp.bfloat16)
    place = jnp.arange(own_rows, dtype=jnp.int32)
    earlier = (place[None, :] < place[:, None]).astype(jnp.bfloat16)
    before = jnp.dot(earlier, usage, preferred_element_type=jnp.float32).astype(jnp.int32)
    ranks = jnp.sum(jnp.where(expert_hit, before[:, None, :], 0), axis=2)
    target = jnp.where(ranks < capacity, chosen * capacity + ranks, slots)
    normed = rms_scale(
        lax.dynamic_slice_in_dim(moe_input, own_first, own_rows, 0), moe_gain
    ).astype(jnp.bfloat16)
    slot_at = jnp.arange(slots, dtype=jnp.int32)[:, None]
    sent = ((slot_at == target[None, :, 0]) | (slot_at == target[None, :, 1])).astype(jnp.bfloat16)
    outgoing = jnp.dot(sent, normed, preferred_element_type=jnp.float32).astype(jnp.bfloat16)
    arrived = lax.all_to_all(
        outgoing.reshape(experts, capacity, width_model), "ep", split_axis=0, concat_axis=0, tiled=True
    ).reshape(slots, width_model)

    total = expert_part(arrived, gate, up, down)
    total = total + expert_part(arrived, *left)
    total = total + expert_part(arrived, *right)
    total = total + expert_part(arrived, *far_a)
    total = total + expert_part(arrived, *far_b)
    results = total.astype(jnp.bfloat16).reshape(experts, capacity, width_model)
    returned = lax.all_to_all(results, "ep", split_axis=0, concat_axis=0, tiled=True).reshape(
        slots, width_model
    )

    mixer_term = attention(ep_index.reshape(1), widen(queries), out_weight, gathered)
    mixer_summed = lax.psum_scatter(mixer_term, "tp", scatter_dimension=0, tiled=True)
    mixer_out = rms_scale(mixer_summed, out_gain).astype(jnp.bfloat16)

    group_logits = jnp.dot(normed, router_group, preferred_element_type=jnp.float32)
    expert_logits = jnp.dot(normed, router_expert, preferred_element_type=jnp.float32)
    group_top = jnp.max(group_logits, axis=1, keepdims=True)
    group_exp = jnp.exp(group_logits - group_top)
    group_hit = jnp.arange(GROUPS, dtype=jnp.int32)[None, :] == own_group[:, None]
    group_share = jnp.sum(jnp.where(group_hit, group_exp, 0.0), axis=1) / jnp.sum(group_exp, axis=1)
    picked_logits = jnp.sum(jnp.where(expert_hit, expert_logits[:, None, :], 0.0), axis=2)
    shares = group_share[:, None] * jax.nn.sigmoid(picked_logits - picked_logits[:, ::-1])
    column = jnp.arange(slots, dtype=jnp.int32)[None, :]
    weight = jnp.where(column == target[:, :1], shares[:, :1], 0.0) + jnp.where(
        column == target[:, 1:], shares[:, 1:], 0.0
    )
    high = lax.reduce_precision(weight, 8, 7)
    moe_out = jnp.dot(
        high.astype(jnp.bfloat16), returned, preferred_element_type=jnp.float32
    ) + jnp.dot((weight - high).astype(jnp.bfloat16), returned, preferred_element_type=jnp.float32)
    return (mixer_out, moe_out.astype(jnp.bfloat16))


def solution(mesh):
    in_specs = (
        P("ep", "tp"),
        P("ep", "tp"),
        P("ep", "tp"),
        P("tp", "ep"),
        P("tp", None),
        P(),
        P("ep", None),
        P(),
        P(),
        P(),
        P("ep"),
        P("ep", None),
        P("ep", None, "tp"),
        P("ep", None, "tp"),
        P("ep", "tp", None),
    )
    out_specs = (P(("ep", "tp"), None), P(("ep", "tp"), None))
    return jax.shard_map(body, mesh=mesh, in_specs=in_specs, out_specs=out_specs, check_vma=False)
```

time: 523 us -> 273 us (0.52)
  starting transfers between devices: 206 us -> 94.5 us
  waiting for transfers between devices: 151 us -> 78.3 us
  blocking collectives: 37 us -> 0 us
  local copies, waits for them, and re-layouts: 46.8 us -> 18.1 us
  matrix products: 27.6 us -> 51 us
  loops' own time: 22.8 us -> 0 us
    all_to_all x1, starting transfers between devices: 198 us -> 68.1 us  [body(): lax.all_to_all(results, 'ep', split_axis=0, concat_axis=0, tiled=True)]
    all_gather x2 -> x1, waiting for transfers between devices: 92.5 us -> 0.01 us  [body(): lax.all_gather(packed, 'ep', axis=0, tiled=True)]
    ppermute x0 -> x12, waiting for transfers between devices: none -> 48.9 us  [shift(): return lax.ppermute(x, 'tp', [(i, (i + by) % count) for i in range(count)])]
    reduce_scatter x2 -> x1, waiting for transfers between devices: 47.7 us -> 0.01 us  [body(): lax.psum_scatter(mixer_term, 'tp', scatter_dimension=0, tiled=True)]
    all_to_all x1 -> x0, blocking collectives: 37 us -> none  [body(): lax.all_to_all(outgoing, 'ep', split_axis=0, concat_axis=0, tiled=True)]
    all_to_all x1, waiting for transfers between devices: 3.03 us -> 29.4 us  [body(): lax.all_to_all(results, 'ep', split_axis=0, concat_axis=0, tiled=True)]
    dot_general x5 -> x14, matrix products: 27 us -> 50.5 us  [the longest x5 33.9 us: expert_part(): return jnp.dot(hidden, down, preferred_element_type=jnp.float32)]
    another operation x33 -> x0, loops' own time: 22.8 us -> none  [the longest x1 22.1 us: body(): lax.scan(advance, current, (keys_piece.reshape(blocks, rows_group, -1), v...]
  transfers between devices with their start and end apart: 6 -> 16, of which waited for: 6 -> 8; matrix products, arithmetic and copies ran while one was open for 13% -> 25% of each run, Pallas kernels for 0% -> 2%
where the time goes in v1:
time: 273 us; the launch traced here: 272 us
  starting transfers between devices  94.5 us (35%)
  waiting for transfers between devices  78.3 us (29%)
  matrix products  51 us (19%)
  local copies, waits for them, and re-layouts  18.1 us (7%)
  between operations  14.3 us (5%)
  other arithmetic  11.5 us (4%)
  Pallas kernels  4.39 us (2%)
    all_to_all x1, starting transfers between devices, body(): lax.all_to_all(results, 'ep', split_axis=0, concat_axis=0, tiled=True)  68.1 us
    ppermute x12, waiting for transfers between devices, shift(): return lax.ppermute(x, 'tp', [(i, (i + by) % count) for i in range(count)])  48.9 us
    dot_general x5, matrix products, expert_part(): return jnp.dot(hidden, down, preferred_element_type=jnp.float32)  33.9 us
    all_to_all x1, waiting for transfers between devices, body(): lax.all_to_all(results, 'ep', split_axis=0, concat_axis=0, tiled=True)  29.4 us
    ppermute x12, starting transfers between devices, shift(): return lax.ppermute(x, 'tp', [(i, (i + by) % count) for i in range(count)])  17.9 us
    dot_general x5, matrix products, expert_part(): gated = jnp.dot(rows, gate, preferred_element_type=jnp.float32)  12.5 us
    all_to_all x1, starting transfers between devices, body(): lax.all_to_all(outgoing.reshape(experts, capacity, width_model), 'ep', sp...  8.46 us
  transfers between devices with their start and end apart: 16, of which 8 were waited for; matrix products, arithmetic and copies ran while one was open for 25% of the time, Pallas kernels for 2%

profile of v1, /device:TPU:0, one launch (start us, length us, event | category | flops | bytes accessed | tf_op | source)
XLA Modules:
  0.0 272.2 jit_solution(16216608175150812638)
XLA Ops:
  18.3 2.1 convolution_convert_fusion
  20.4 8.5 %all-to-all-start = ((bf16[32,16,2048]{2,1,0:T(8,128)(2,1)}), bf16[32,16,2048]{2,1,0:T(8,128)(2,1)S(1)}, u32[]{:S(2)}, u32[]{:S(2)}) async-start(bf16[32,16,2048]{2,1,0:T(8,128)(2,1)} %bitcast.78), calls=%async_computation.1 | async-start | bytes 4194304 | tf_op jit(solution)/shard_map/all_to_all | solution.py:211
  28.9 1.8 collective-permute-start.3
  31.0 3.0 %collective-permute-start.4 = (bf16[2048,256]{1,0:T(8,128)(2,1)}, bf16[2048,256]{1,0:T(8,128)(2,1)}, u32[]{:S(2)}, u32[]{:S(2)}) collective-permute-start(bf16[2048,256]{1,0:T(8,128)(2,1)} %bitcast.83), channel_id=1, source_target_pairs={{0,3},{1,0},{2,1},{3,2},{4,7},{5,4},{6,5},{7,6},{8,11},{9,8},{10,9... | collective-permute-start | bytes 3145736 | tf_op jit(solution)/shard_map/ppermute | solution.py:138
  34.0 5.5 %collective-permute-done = bf16[2048,256]{1,0:T(8,128)(2,1)} collective-permute-done((bf16[2048,256]{1,0:T(8,128)(2,1)}, bf16[2048,256]{1,0:T(8,128)(2,1)}, u32[]{:S(2)}, u32[]{:S(2)}) %collective-permute-start) | collective-permute-done | bytes 1048608 | tf_op jit(solution)/shard_map/ppermute | solution.py:138
  41.9 1.9 slice.51
  43.8 11.5 %collective-permute-done.3 = bf16[2048,256]{1,0:T(8,128)(2,1)} collective-permute-done((bf16[2048,256]{1,0:T(8,128)(2,1)}, bf16[2048,256]{1,0:T(8,128)(2,1)}, u32[]{:S(2)}, u32[]{:S(2)}) %collective-permute-start.3) | collective-permute-done | bytes 1048608 | tf_op jit(solution)/shard_map/ppermute | solution.py:138
  56.8 1.9 slice.54
  58.8 3.2 %collective-permute-done.1 = bf16[2048,256]{1,0:T(8,128)(2,1)} collective-permute-done((bf16[2048,256]{1,0:T(8,128)(2,1)}, bf16[2048,256]{1,0:T(8,128)(2,1)}, u32[]{:S(2)}, u32[]{:S(2)}) %collective-permute-start.1) | collective-permute-done | bytes 1048608 | tf_op jit(solution)/shard_map/ppermute | solution.py:138
  63.6 1.9 slice.52
  65.5 12.3 %collective-permute-done.4 = bf16[2048,256]{1,0:T(8,128)(2,1)} collective-permute-done((bf16[2048,256]{1,0:T(8,128)(2,1)}, bf16[2048,256]{1,0:T(8,128)(2,1)}, u32[]{:S(2)}, u32[]{:S(2)}) %collective-permute-start.4) | collective-permute-done | bytes 1048608 | tf_op jit(solution)/shard_map/ppermute | solution.py:138
  79.3 1.9 slice.55
  81.2 3.2 %collective-permute-done.2 = bf16[256,2048]{1,0:T(8,128)(2,1)} collective-permute-done((bf16[256,2048]{1,0:T(8,128)(2,1)}, bf16[256,2048]{1,0:T(8,128)(2,1)}, u32[]{:S(2)}, u32[]{:S(2)}) %collective-permute-start.2) | collective-permute-done | bytes 1048608 | tf_op jit(solution)/shard_map/ppermute | solution.py:138
  86.1 1.9 slice.53
  87.9 12.3 %collective-permute-done.5 = bf16[256,2048]{1,0:T(8,128)(2,1)} collective-permute-done((bf16[256,2048]{1,0:T(8,128)(2,1)}, bf16[256,2048]{1,0:T(8,128)(2,1)}, u32[]{:S(2)}, u32[]{:S(2)}) %collective-permute-start.5) | collective-permute-done | bytes 1048608 | tf_op jit(solution)/shard_map/ppermute | solution.py:138
  101.8 1.9 slice.56
  103.7 3.5 %fusion.51 = f32[512,256]{1,0:T(8,128)} fusion(bf16[512,2048]{1,0:T(8,128)(2,1)S(1)} %bitcast.66, bf16[1,2048,256]{2,1,0:T(8,128)(2,1)} %param.27), kind=kOutput, calls=%fused_computation.104 | convolution fusion | flops 536870912 | bytes 3670016 | tf_op jit(solution)/shard_map/dot_general | solution.py:149
  107.2 2.8 %fusion.71 = f32[512,256]{1,0:T(8,128)} fusion(bf16[512,2048]{1,0:T(8,128)(2,1)S(1)} %bitcast.67, bf16[2048,256]{1,0:T(8,128)(2,1)} %collective-permute-done.3), kind=kOutput, calls=%fused_computation.120 | convolution fusion | flops 536870912 | bytes 3670016 | tf_op jit(solution)/shard_map/dot_general | solution.py:149
  109.9 1.7 collective-permute-start.11
  111.7 1.7 fusion.72
  113.4 2.7 %fusion.70 = f32[512,256]{1,0:T(8,128)} fusion(bf16[512,2048]{1,0:T(8,128)(2,1)S(1)} %bitcast.69, bf16[2048,256]{1,0:T(8,128)(2,1)} %collective-permute-done), kind=kOutput, calls=%fused_computation.119 | convolution fusion | flops 536870912 | bytes 3670016 | tf_op jit(solution)/shard_map/dot_general | solution.py:149
  116.9 5.5 %fusion.24 = f32[512,2048]{1,0:T(8,128)} fusion(bf16[128,2048]{1,0:T(8,128)(2,1)} %collective-permute-done.8, f32[512,128]{1,0:T(8,128)S(1)} %fusion.72, bf16[512,2048]{1,0:T(8,128)(2,1)S(1)} %bitcast.70, bf16[2048,128]{1,0:T(8,128)(2,1)} %collective-permute-done.7), kind=kOutput, calls=%fused_computation.45 | convolution fusion | flops 537264128 | bytes 7602176 | tf_op jit(solution)/shard_map/dot_general | solution.py:152
  122.4 5.9 %fusion.2 = f32[512,2048]{1,0:T(8,128)} fusion(bf16[512,2048]{1,0:T(8,128)(2,1)S(1)} %bitcast.71, f32[512,256]{1,0:T(8,128)} %fusion.51, bf16[1,256,2048]{2,1,0:T(8,128)(2,1)} %param.29, bf16[1,2048,256]{2,1,0:T(8,128)(2,1)} %param.28), kind=kOutput, calls=%fused_computation.10 | convolution fusion | flops 1074528256 | bytes 8912896 | tf_op jit(solution)/shard_map/dot_general | solution.py:152
  128.3 6.7 %fusion.15 = f32[512,2048]{1,0:T(8,128)} fusion(bf16[256,2048]{1,0:T(8,128)(2,1)} %collective-permute-done.2, f32[512,256]{1,0:T(8,128)} %fusion.70, bf16[512,2048]{1,0:T(8,128)(2,1)} %bitcast.72, bf16[2048,256]{1,0:T(8,128)(2,1)} %collective-permute-done.1), kind=kOutput, calls=%fused_computation.31 | convolution fusion | flops 1074528256 | bytes 8912896 | tf_op jit(solution)/shard_map/dot_general | solution.py:152
  135.0 3.5 %copy-done.1 = bf16[16896,256]{1,0:T(8,128)(2,1)S(1)} copy-done((bf16[16896,256]{1,0:T(8,128)(2,1)S(1)}, bf16[16896,256]{1,0:T(8,128)(2,1)}, u32[]{:S(2)}) %copy-start.1) | copy-done | bytes 8650776
  138.5 4.4 %shard_map.158 = bf16[512,2048]{1,0:T(8,128)(2,1)} custom-call(s32[1]{0:T(128)} %bitcast.own_ref, bf16[256,1024]{1,0:T(8,128)(2,1)S(1)} %pad_maximum_fusion.q_ref, bf16[256,2048]{1,0:T(8,128)(2,1)S(1)} %copy-done.2, bf16[32,528,256]{2,1,0:T(8,128)(2,1)S(1)} %bitcast.65), custom_call_target="tpu_custom_call" | custom-call | flops 8999999488 | bytes 12000000 | tf_op jit(solution)/shard_map/pallas_call | solution.py:114
  144.5 1.7 fusion.73
  146.2 5.9 %fusion.16 = f32[512,2048]{1,0:T(8,128)} fusion(bf16[256,2048]{1,0:T(8,128)(2,1)} %collective-permute-done.5, f32[512,256]{1,0:T(8,128)} %fusion.71, bf16[512,2048]{1,0:T(8,128)(2,1)S(1)} %bitcast.74, bf16[2048,256]{1,0:T(8,128)(2,1)} %collective-permute-done.4), kind=kOutput, calls=%fused_computation.32 | convolution fusion | flops 1074528256 | bytes 8912896 | tf_op jit(solution)/shard_map/dot_general | solution.py:152
  152.2 9.9 %add_convert_fusion = bf16[512,2048]{1,0:T(8,128)(2,1)} fusion(f32[512,2048]{1,0:T(8,128)} %fusion.24, f32[512,2048]{1,0:T(8,128)} %fusion.16, f32[512,2048]{1,0:T(8,128)} %fusion.2, f32[512,2048]{1,0:T(8,128)} %fusion.15, bf16[128,2048]{1,0:T(8,128)(2,1)} %collective-permute-done.11, f32[512,128]{1,0:T(8,128)S(1)} %fusion.73, ...), kind=kOutput, calls=%fused_computation | convolution fusion | flops 542507008 | bytes 22282240 | tf_op jit(solution)/shard_map/dot_general | solution.py:152
  162.0 68.1 %all-to-all-start.1 = ((bf16[32,16,2048]{2,1,0:T(8,128)(2,1)}), bf16[32,16,2048]{2,1,0:T(8,128)(2,1)S(1)}, u32[]{:S(2)}, u32[]{:S(2)}) async-start(bf16[32,16,2048]{2,1,0:T(8,128)(2,1)} %bitcast.79), calls=%async_computation.2 | async-start | bytes 4194304 | tf_op jit(solution)/shard_map/all_to_all | solution.py:221
  230.8 29.4 %all-to-all-done.1 = bf16[32,16,2048]{2,1,0:T(8,128)(2,1)S(1)} async-done(((bf16[32,16,2048]{2,1,0:T(8,128)(2,1)}), bf16[32,16,2048]{2,1,0:T(8,128)(2,1)S(1)}, u32[]{:S(2)}, u32[]{:S(2)}) %all-to-all-start.1) | async-done | bytes 2097184 | tf_op jit(solution)/shard_map/all_to_all | solution.py:221
  263.3 2.0 fusion.5
  (82 shorter events, 27.7 us)
Async XLA Ops:
  7.2 223.0 %copy-start = (bf16[2048,32]{0,1:T(8,128)(2,1)S(1)}, bf16[2048,32]{0,1:T(8,128)(2,1)}, u32[]{:S(2)}) copy-start(bf16[2048,32]{0,1:T(8,128)(2,1)} %param.24) | copy-start | bytes 393220
  7.2 127.8 %all-gather.2.cloned.1.call-start = ((), (), s32[]{:S(2)}) async-start(), calls=%async_computation.3 | async-start | bytes 8921088 | tf_op jit(solution)/shard_map/all_gather | solution.py:192
  11.8 27.6 %collective-permute-start = (bf16[2048,256]{1,0:T(8,128)(2,1)}, bf16[2048,256]{1,0:T(8,128)(2,1)}, u32[]{:S(2)}, u32[]{:S(2)}) collective-permute-start(bf16[2048,256]{1,0:T(8,128)(2,1)} %bitcast.90), channel_id=1, source_target_pairs={{0,1},{1,2},{2,3},{3,0},{4,5},{5,6},{6,7},{7,4},{8,9},{9,10},{10,1... | collective-permute-start | bytes 3145736 | tf_op jit(solution)/shard_map/ppermute | solution.py:138
  20.4 20.7 %copy-start.5 = (bf16[512,256]{1,0:T(8,128)(2,1)S(1)}, bf16[512,256]{1,0:T(8,128)(2,1)}, u32[]{:S(2)}) copy-start(bf16[512,256]{1,0:T(8,128)(2,1)} %param.15) | copy-start | bytes 786436
  20.4 83.3 %all-to-all-start = ((bf16[32,16,2048]{2,1,0:T(8,128)(2,1)}), bf16[32,16,2048]{2,1,0:T(8,128)(2,1)S(1)}, u32[]{:S(2)}, u32[]{:S(2)}) async-start(bf16[32,16,2048]{2,1,0:T(8,128)(2,1)} %bitcast.78), calls=%async_computation.1 | async-start | bytes 4194304 | tf_op jit(solution)/shard_map/all_to_all | solution.py:211
  28.9 233.2 %reduce-scatter.2.cloned.1.call-start = ((), (), s32[]{:S(2)}) async-start(), calls=%async_computation.4 | async-start | bytes 2621440 | tf_op jit(solution)/shard_map/reduce_scatter | solution.py:226
  28.9 26.4 %collective-permute-start.3 = (bf16[2048,256]{1,0:T(8,128)(2,1)}, bf16[2048,256]{1,0:T(8,128)(2,1)}, u32[]{:S(2)}, u32[]{:S(2)}) collective-permute-start(bf16[2048,256]{1,0:T(8,128)(2,1)} %bitcast.91), channel_id=1, source_target_pairs={{0,3},{1,0},{2,1},{3,2},{4,7},{5,4},{6,5},{7,6},{8,11},{9,8},{10,9... | collective-permute-start | bytes 3145736 | tf_op jit(solution)/shard_map/ppermute | solution.py:138
  30.7 31.2 %collective-permute-start.1 = (bf16[2048,256]{1,0:T(8,128)(2,1)}, bf16[2048,256]{1,0:T(8,128)(2,1)}, u32[]{:S(2)}, u32[]{:S(2)}) collective-permute-start(bf16[2048,256]{1,0:T(8,128)(2,1)} %bitcast.82), channel_id=1, source_target_pairs={{0,1},{1,2},{2,3},{3,0},{4,5},{5,6},{6,7},{7,4},{8,9},{9,10},{10,1... | collective-permute-start | bytes 3145736 | tf_op jit(solution)/shard_map/ppermute | solution.py:138
  31.0 46.8 %collective-permute-start.4 = (bf16[2048,256]{1,0:T(8,128)(2,1)}, bf16[2048,256]{1,0:T(8,128)(2,1)}, u32[]{:S(2)}, u32[]{:S(2)}) collective-permute-start(bf16[2048,256]{1,0:T(8,128)(2,1)} %bitcast.83), channel_id=1, source_target_pairs={{0,3},{1,0},{2,1},{3,2},{4,7},{5,4},{6,5},{7,6},{8,11},{9,8},{10,9... | collective-permute-start | bytes 3145736 | tf_op jit(solution)/shard_map/ppermute | solution.py:138
  34.0 50.4 %collective-permute-start.2 = (bf16[256,2048]{1,0:T(8,128)(2,1)}, bf16[256,2048]{1,0:T(8,128)(2,1)}, u32[]{:S(2)}, u32[]{:S(2)}) collective-permute-start(bf16[256,2048]{1,0:T(8,128)(2,1)} %bitcast.80), channel_id=1, source_target_pairs={{0,1},{1,2},{2,3},{3,0},{4,5},{5,6},{6,7},{7,4},{8,9},{9,10},{10,1... | collective-permute-start | bytes 3145736 | tf_op jit(solution)/shard_map/ppermute | solution.py:138
  39.5 60.8 %collective-permute-start.5 = (bf16[256,2048]{1,0:T(8,128)(2,1)}, bf16[256,2048]{1,0:T(8,128)(2,1)}, u32[]{:S(2)}, u32[]{:S(2)}) collective-permute-start(bf16[256,2048]{1,0:T(8,128)(2,1)} %bitcast.81), channel_id=1, source_target_pairs={{0,3},{1,0},{2,1},{3,2},{4,7},{5,4},{6,5},{7,6},{8,11},{9,8},{10,9... | collective-permute-start | bytes 3145736 | tf_op jit(solution)/shard_map/ppermute | solution.py:138
  55.3 54.6 %collective-permute-start.6 = (bf16[2048,128]{1,0:T(8,128)(2,1)}, bf16[2048,128]{1,0:T(8,128)(2,1)}, u32[]{:S(2)}, u32[]{:S(2)}) collective-permute-start(bf16[2048,128]{1,0:T(8,128)(2,1)} %slice.51), channel_id=1, source_target_pairs={{0,1},{1,2},{2,3},{3,0},{4,5},{5,6},{6,7},{7,4},{8,9},{9,10},{10,1... | collective-permute-start | bytes 1572872 | tf_op jit(solution)/shard_map/ppermute | solution.py:138
  61.9 81.0 %collective-permute-start.9 = (bf16[2048,128]{1,0:T(8,128)(2,1)}, bf16[2048,128]{1,0:T(8,128)(2,1)}, u32[]{:S(2)}, u32[]{:S(2)}) collective-permute-start(bf16[2048,128]{1,0:T(8,128)(2,1)} %slice.54), channel_id=1, source_target_pairs={{0,3},{1,0},{2,1},{3,2},{4,7},{5,4},{6,5},{7,6},{8,11},{9,8},{10,9... | collective-permute-start | bytes 1572872 | tf_op jit(solution)/shard_map/ppermute | solution.py:138
  77.8 38.3 %collective-permute-start.7 = (bf16[2048,128]{1,0:T(8,128)(2,1)}, bf16[2048,128]{1,0:T(8,128)(2,1)}, u32[]{:S(2)}, u32[]{:S(2)}) collective-permute-start(bf16[2048,128]{1,0:T(8,128)(2,1)} %slice.52), channel_id=1, source_target_pairs={{0,1},{1,2},{2,3},{3,0},{4,5},{5,6},{6,7},{7,4},{8,9},{9,10},{10,1... | collective-permute-start | bytes 1572872 | tf_op jit(solution)/shard_map/ppermute | solution.py:138
  84.4 67.8 %collective-permute-start.10 = (bf16[2048,128]{1,0:T(8,128)(2,1)}, bf16[2048,128]{1,0:T(8,128)(2,1)}, u32[]{:S(2)}, u32[]{:S(2)}) collective-permute-start(bf16[2048,128]{1,0:T(8,128)(2,1)} %slice.55), channel_id=1, source_target_pairs={{0,3},{1,0},{2,1},{3,2},{4,7},{5,4},{6,5},{7,6},{8,11},{9,8},{10,9... | collective-permute-start | bytes 1572872 | tf_op jit(solution)/shard_map/ppermute | solution.py:138
  100.3 16.6 %collective-permute-start.8 = (bf16[128,2048]{1,0:T(8,128)(2,1)}, bf16[128,2048]{1,0:T(8,128)(2,1)}, u32[]{:S(2)}, u32[]{:S(2)}) collective-permute-start(bf16[128,2048]{1,0:T(8,128)(2,1)} %slice.53), channel_id=1, source_target_pairs={{0,1},{1,2},{2,3},{3,0},{4,5},{5,6},{6,7},{7,4},{8,9},{9,10},{10,1... | collective-permute-start | bytes 1572872 | tf_op jit(solution)/shard_map/ppermute | solution.py:138
  103.7 18.7 %copy-start.3 = (bf16[32,16,2048]{2,1,0:T(8,128)(2,1)}, bf16[32,16,2048]{2,1,0:T(8,128)(2,1)S(1)}, u32[]{:S(2)}) copy-start(bf16[32,16,2048]{2,1,0:T(8,128)(2,1)S(1)} %all-to-all-done) | copy-start | bytes 6291460
  109.9 42.2 %collective-permute-start.11 = (bf16[128,2048]{1,0:T(8,128)(2,1)}, bf16[128,2048]{1,0:T(8,128)(2,1)}, u32[]{:S(2)}, u32[]{:S(2)}) collective-permute-start(bf16[128,2048]{1,0:T(8,128)(2,1)} %slice.56), channel_id=1, source_target_pairs={{0,3},{1,0},{2,1},{3,2},{4,7},{5,4},{6,5},{7,6},{8,11},{9,8},{10,9... | collective-permute-start | bytes 1572872 | tf_op jit(solution)/shard_map/ppermute | solution.py:138
  128.3 6.7 %copy-start.2 = (bf16[256,2048]{1,0:T(8,128)(2,1)S(1)}, bf16[256,2048]{1,0:T(8,128)(2,1)}, u32[]{:S(2)}) copy-start(bf16[256,2048]{1,0:T(8,128)(2,1)} %w_ref.1) | copy-start | bytes 3145732
  135.0 3.5 %copy-start.1 = (bf16[16896,256]{1,0:T(8,128)(2,1)S(1)}, bf16[16896,256]{1,0:T(8,128)(2,1)}, u32[]{:S(2)}) copy-start(bf16[16896,256]{1,0:T(8,128)(2,1)} %all-gather.2.cloned.1.call-done) | copy-start | bytes 25952260
  142.9 1.6 copy-start.4
  162.0 68.4 %copy-start.6 = (bf16[2048,4]{0,1:T(4,128)(2,1)S(1)}, bf16[2048,4]{0,1:T(4,128)(2,1)}, u32[]{:S(2)}) copy-start(bf16[2048,4]{0,1:T(4,128)(2,1)} %param.23) | copy-start | bytes 49156
  162.0 98.2 %all-to-all-start.1 = ((bf16[32,16,2048]{2,1,0:T(8,128)(2,1)}), bf16[32,16,2048]{2,1,0:T(8,128)(2,1)S(1)}, u32[]{:S(2)}, u32[]{:S(2)}) async-start(bf16[32,16,2048]{2,1,0:T(8,128)(2,1)} %bitcast.79), calls=%async_computation.2 | async-start | bytes 4194304 | tf_op jit(solution)/shard_map/all_to_all | solution.py:221
  260.7 2.6 copy-start.7
Sparse Core Ops, SparseCore 0:
  12.0 71.5 all-gather.1
  143.0 90.3 reduce-scatter.1

commit v2 on v1

--- a/solution.py
+++ b/solution.py
@@ -15,10 +15,13 @@
 QT = 256
 
 
-def attention_kernel(own_ref, q_ref, w_ref, kv_hbm, out_ref, buf, sems, top, gap, acc):
+def attention_kernel(
+    own_ref, q_ref, w_ref, kv_hbm, out_ref, buf, sems, even, odd, peak_even, peak_odd, top, gap, acc
+):
     own = own_ref[0]
     width = q_ref.shape[1]
     half = width // 2
+    tiles = [slice(t * QT, (t + 1) * QT) for t in range(width // QT)]
 
     def copy(j):
         return pltpu.make_async_copy(kv_hbm.at[j], buf.at[j], sems.at[j])
@@ -32,8 +35,7 @@
     gap[...] = jnp.zeros_like(gap)
     acc[...] = jnp.zeros_like(acc)
 
-    def block(j, masked):
-        copy(j).wait()
+    def keys_of(j):
         gates = buf[j, BLOCK:, :]
         gates = jnp.concatenate([gates, jnp.zeros((DH - 16, 2 * DH), jnp.bfloat16)], axis=0)
         turned = jnp.transpose(gates.astype(jnp.float32)).astype(jnp.bfloat16)
@@ -42,42 +44,71 @@
         extra = jnp.concatenate(
             [jnp.where(lane < 8, turned, zero), jnp.where(lane < 8, zero, turned)], axis=0
         )
-        keys = jnp.concatenate([buf[j, :BLOCK, :DH], extra], axis=1)
+        return jnp.concatenate([buf[j, :BLOCK, :DH], extra], axis=1)
+
+    def values_of(j):
         values = jnp.concatenate(
-            [buf[j, c * DH : (c + 1) * DH, DH:] for c in range(BLOCK // DH)]
-            , axis=1)
-        values = jnp.concatenate([values, jnp.ones((16, BLOCK), jnp.bfloat16)], axis=0)
-        if not masked:
-            last = buf[j, BLOCK:, 2 * DH - DH :].astype(jnp.float32)
-            for h in range(2):
-                total = (
-                    last[8 + 3 * h : 9 + 3 * h, DH - 1 : DH]
-                    + last[9 + 3 * h : 10 + 3 * h, DH - 1 : DH]
-                    + last[10 + 3 * h : 11 + 3 * h, DH - 1 : DH]
-                )
-                gap[:, h * half : (h + 1) * half] = gap[:, h * half : (h + 1) * half] + total
-        for t in range(width // QT):
-            cols = slice(t * QT, (t + 1) * QT)
-            s = jnp.dot(keys, q_ref[:, cols], preferred_element_type=jnp.float32)
-            if masked:
-                key_at = lax.broadcasted_iota(jnp.int32, s.shape, 0)
-                query_at = lax.broadcasted_iota(jnp.int32, s.shape, 1) + (t * QT) % half
-                s = jnp.where(key_at <= query_at, s, -1e30)
-            old = top[:, cols]
-            new = jnp.maximum(old, jnp.max(s, axis=0, keepdims=True) + gap[:, cols])
-            top[:, cols] = new
-            shift = (new - gap[:, cols]) * SCALE
-            p = jnp.exp2(s * SCALE - shift)
-            part = jnp.dot(values, p.astype(jnp.bfloat16), preferred_element_type=jnp.float32)
-            acc[:, cols] = acc[:, cols] * jnp.exp2((old - new) * SCALE) + part
-
-    block(own, True)
+            [buf[j, c * DH : (c + 1) * DH, DH:] for c in range(BLOCK // DH)], axis=1
+        )
+        return jnp.concatenate([values, jnp.ones((16, BLOCK), jnp.bfloat16)], axis=0)
+
+    def move_gap(j, alive):
+        last = buf[j, BLOCK:, DH:].astype(jnp.float32)
+        dead = jnp.where(alive, 0.0, -1e30)
+        for h in range(2):
+            total = (
+                last[8 + 3 * h : 9 + 3 * h, DH - 1 : DH]
+                + last[9 + 3 * h : 10 + 3 * h, DH - 1 : DH]
+                + last[10 + 3 * h : 11 + 3 * h, DH - 1 : DH]
+                + dead
+            )
+            gap[:, h * half : (h + 1) * half] = gap[:, h * half : (h + 1) * half] + total
+
+    def score(keys, t, into, peak, masked):
+        s = jnp.dot(keys, q_ref[:, tiles[t]], preferred_element_type=jnp.float32)
+        if masked:
+            key_at = lax.broadcasted_iota(jnp.int32, s.shape, 0)
+            query_at = lax.broadcasted_iota(jnp.int32, s.shape, 1) + (t * QT) % half
+            s = jnp.where(key_at <= query_at, s, -1e30)
+        into[:, tiles[t]] = s
+        peak[:, tiles[t]] = jnp.max(s, axis=0, keepdims=True)
+
+    def absorb(values, t, held, peak):
+        cols = tiles[t]
+        old = top[:, cols]
+        new = jnp.maximum(old, peak[:, cols] + gap[:, cols])
+        top[:, cols] = new
+        p = jnp.exp2(held[:, cols] * SCALE - (new - gap[:, cols]) * SCALE)
+        part = jnp.dot(values, p.astype(jnp.bfloat16), preferred_element_type=jnp.float32)
+        acc[:, cols] = acc[:, cols] * jnp.exp2((old - new) * SCALE) + part
+
+    def phase(now, later, held, held_peak, into, into_peak):
+        values = values_of(jnp.maximum(now, 0))
+        keys = keys_of(jnp.maximum(later, 0))
+        for t in range(len(tiles)):
+            score(keys, t, into, into_peak, False)
+            absorb(values, t, held, held_peak)
+        move_gap(jnp.maximum(later, 0), later >= 0)
+
+    def arrive(j):
+        @pl.when(j >= 0)
+        def _():
+            copy(j).wait()
+
+    copy(own).wait()
+    keys = keys_of(own)
+    for t in range(len(tiles)):
+        score(keys, t, even, peak_even, True)
 
     def step(i, carry):
-        block(own - i, False)
+        now = own - 2 * i
+        arrive(now - 1)
+        arrive(now - 2)
+        phase(now, now - 1, even, peak_even, odd, peak_odd)
+        phase(now - 1, now - 2, odd, peak_odd, even, peak_even)
         return carry
 
-    lax.fori_loop(1, own + 1, step, 0)
+    lax.fori_loop(0, lax.div(own + 2, 2), step, 0)
     total = acc[DH : DH + 1, :]
     attended = acc[:DH, :] / total
     stacked = jnp.concatenate([attended[:, :half], attended[:, half:]], axis=0)
@@ -118,19 +149,152 @@
             pl.BlockSpec(memory_space=pltpu.SMEM),
             pl.BlockSpec(memory_space=pltpu.VMEM),
             pl.BlockSpec(memory_space=pltpu.VMEM),
-            pl.BlockSpec(memory_space=pl.ANY),
+            pl.BlockSpec(memory_space=pltpu.HBM),
         ],
         out_specs=pl.BlockSpec(memory_space=pltpu.VMEM),
         scratch_shapes=[
             pltpu.VMEM(kv.shape, jnp.bfloat16),
             pltpu.SemaphoreType.DMA((n,)),
+            pltpu.VMEM((BLOCK, width), jnp.float32),
+            pltpu.VMEM((BLOCK, width), jnp.float32),
+            pltpu.VMEM((1, width), jnp.float32),
+            pltpu.VMEM((1, width), jnp.float32),
             pltpu.VMEM((1, width), jnp.float32),
             pltpu.VMEM((1, width), jnp.float32),
             pltpu.VMEM((DH + 16, width), jnp.float32),
         ],
-        compiler_params=pltpu.CompilerParams(vmem_limit_bytes=40 << 20),
         cost_estimate=pl.CostEstimate(flops=9_000_000_000, bytes_accessed=12_000_000, transcendentals=16_000_000),
     )(own, q, w, kv)
+
+
+def expert_hidden(x_ref, both, hidden_ref, at):
+    rows, ff = x_ref.shape[0], both.shape[1] // 2
+    for r in range(0, rows, 256):
+        lines = slice(r, r + 256)
+        pre = jnp.dot(x_ref[lines, :], both[...], preferred_element_type=jnp.float32)
+        gated, lifted = pre[:, :ff], pre[:, ff:]
+        hidden_ref[lines, at : at + ff] = (gated * jax.nn.sigmoid(gated) * lifted).astype(jnp.bfloat16)
+
+
+def column_tiles(width):
+    return [slice(n, n + 512) for n in range(0, width, 512)]
+
+
+def first_kernel(x_hbm, *refs):
+    count = (len(refs) - 7) // 3
+    weights, (out_hbm, x_ref, both, down, hidden, out, sems) = refs[: 3 * count], refs[3 * count :]
+    ff = down.shape[0] // count
+    rows = pltpu.make_async_copy(x_hbm, x_ref, sems.at[3 * count])
+    rows.start()
+    copies = []
+    for q in range(count):
+        gate, up, low = weights[3 * q : 3 * q + 3]
+        pairs = (
+            (gate, both.at[q, :, :ff]),
+            (up, both.at[q, :, ff:]),
+            (low, down.at[q * ff : (q + 1) * ff, :]),
+        )
+        for k, (src, dst) in enumerate(pairs):
+            copies.append(pltpu.make_async_copy(src, dst, sems.at[3 * q + k]))
+    for c in copies:
+        c.start()
+    rows.wait()
+    for q in range(count):
+        copies[3 * q].wait()
+        copies[3 * q + 1].wait()
+        expert_hidden(x_ref, both.at[q], hidden, q * ff)
+    for q in range(count):
+        copies[3 * q + 2].wait()
+    stores = []
+    for n, cols in enumerate(column_tiles(out.shape[1])):
+        out[:, cols] = jnp.dot(hidden[...], down[:, cols], preferred_element_type=jnp.float32)
+        stores.append(
+            pltpu.make_async_copy(out.at[:, cols], out_hbm.at[:, cols], sems.at[3 * count + 1 + n])
+        )
+        stores[-1].start()
+    for c in stores:
+        c.wait()
+
+
+def first_parts(x, weights):
+    rows, width = x.shape
+    count, ff = len(weights) // 3, weights[0].shape[1]
+    return pl.pallas_call(
+        first_kernel,
+        out_shape=jax.ShapeDtypeStruct((rows, width), jnp.float32),
+        in_specs=[pl.BlockSpec(memory_space=pltpu.HBM)] * (1 + len(weights)),
+        out_specs=pl.BlockSpec(memory_space=pltpu.HBM),
+        scratch_shapes=[
+            pltpu.VMEM((rows, width), jnp.bfloat16),
+            pltpu.VMEM((count, width, 2 * ff), jnp.bfloat16),
+            pltpu.VMEM((count * ff, width), jnp.bfloat16),
+            pltpu.VMEM((rows, count * ff), jnp.bfloat16),
+            pltpu.VMEM((rows, width), jnp.float32),
+            pltpu.SemaphoreType.DMA((3 * count + 1 + len(column_tiles(width)),)),
+        ],
+        cost_estimate=pl.CostEstimate(
+            flops=count * 6 * rows * width * ff,
+            bytes_accessed=count * 6 * width * ff,
+            transcendentals=rows * count * ff,
+        ),
+    )(x, *weights)
+
+
+def last_kernel(
+    x_hbm, part_hbm, gate, up, top_half, bottom_half, out_hbm, x_ref, part, both, down, hidden, out, sems
+):
+    ff = gate.shape[1]
+    pairs = (
+        (x_hbm, x_ref),
+        (gate, both.at[:, :ff]),
+        (up, both.at[:, ff:]),
+        (top_half, down.at[: ff // 2, :]),
+        (bottom_half, down.at[ff // 2 :, :]),
+        (part_hbm, part),
+    )
+    copies = [pltpu.make_async_copy(src, dst, sems.at[k]) for k, (src, dst) in enumerate(pairs)]
+    for c in copies:
+        c.start()
+    for c in copies[:3]:
+        c.wait()
+    expert_hidden(x_ref, both, hidden, 0)
+    for c in copies[3:]:
+        c.wait()
+    stores = []
+    for n, cols in enumerate(column_tiles(out.shape[1])):
+        out[:, cols] = (
+            part[:, cols]
+            + jnp.dot(hidden[...], down[:, cols], preferred_element_type=jnp.float32)
+        ).astype(jnp.bfloat16)
+        stores.append(
+            pltpu.make_async_copy(out.at[:, cols], out_hbm.at[:, cols], sems.at[len(pairs) + n])
+        )
+        stores[-1].start()
+    for c in stores:
+        c.wait()
+
+
+def last_part(x, part, gate, up, top_half, bottom_half):
+    rows, width = x.shape
+    ff = gate.shape[1]
+    return pl.pallas_call(
+        last_kernel,
+        out_shape=jax.ShapeDtypeStruct((rows, width), jnp.bfloat16),
+        in_specs=[pl.BlockSpec(memory_space=pltpu.HBM)] * 6,
+        out_specs=pl.BlockSpec(memory_space=pltpu.HBM),
+        scratch_shapes=[
+            pltpu.VMEM((rows, width), jnp.bfloat16),
+            pltpu.VMEM((rows, width), jnp.float32),
+            pltpu.VMEM((width, 2 * ff), jnp.bfloat16),
+            pltpu.VMEM((ff, width), jnp.bfloat16),
+            pltpu.VMEM((rows, ff), jnp.bfloat16),
+            pltpu.VMEM((rows, width), jnp.bfloat16),
+            pltpu.SemaphoreType.DMA((6 + len(column_tiles(width)),)),
+        ],
+        cost_estimate=pl.CostEstimate(
+            flops=6 * rows * width * ff, bytes_accessed=6 * width * ff, transcendentals=rows * ff
+        ),
+    )(x, part, gate, up, top_half, bottom_half)
 
 
 def shift(x, by):
@@ -145,14 +309,7 @@
     )
 
 
-def expert_part(rows, gate, up, down):
-    gated = jnp.dot(rows, gate, preferred_element_type=jnp.float32)
-    lifted = jnp.dot(rows, up, preferred_element_type=jnp.float32)
-    hidden = (jax.nn.silu(gated) * lifted).astype(jnp.bfloat16)
-    return jnp.dot(hidden, down, preferred_element_type=jnp.float32)
-
-
-def body(
+def inner(
     queries,
     key_rows,
     value_rows,
@@ -182,14 +339,17 @@
 
     gate, up, down = expert_gate[0], expert_up[0], expert_down[0]
     half = gate.shape[1] // 2
-    left = [shift(w, 1) for w in (gate, up, down)]
-    right = [shift(w, -1) for w in (gate, up, down)]
-    far_a = [shift(left[0][:, :half], 1), shift(left[1][:, :half], 1), shift(left[2][:half], 1)]
-    far_b = [shift(right[0][:, half:], -1), shift(right[1][:, half:], -1), shift(right[2][half:], -1)]
+    from_left = [shift(w, 1) for w in (gate, down, up)]
+    from_right = [shift(w, -1) for w in (up, down, gate)]
+    far_gate = shift(from_left[0], 1)
+    far_up = shift(from_right[0], -1)
+    far_top = shift(from_left[1][:half], 1)
+    far_bottom = shift(from_right[1][half:], -1)
 
     running = jnp.cumsum(jax.nn.log_sigmoid(forget_logit), axis=1)
     packed = pack(key_rows, value_rows, running)
-    gathered = lax.all_gather(packed, "ep", axis=0, tiled=True).reshape(ep_count, *packed.shape)
+    gathered = lax.all_gather(packed, "ep", axis=0, tiled=True)
+    gathered = gathered.reshape(ep_count, *packed.shape)
 
     own_first = tp_index * own_rows
     own_group = lax.dynamic_slice_in_dim(route_group, own_first, own_rows, 0)
@@ -208,21 +368,25 @@
     slot_at = jnp.arange(slots, dtype=jnp.int32)[:, None]
     sent = ((slot_at == target[None, :, 0]) | (slot_at == target[None, :, 1])).astype(jnp.bfloat16)
     outgoing = jnp.dot(sent, normed, preferred_element_type=jnp.float32).astype(jnp.bfloat16)
-    arrived = lax.all_to_all(
-        outgoing.reshape(experts, capacity, width_model), "ep", split_axis=0, concat_axis=0, tiled=True
-    ).reshape(slots, width_model)
-
-    total = expert_part(arrived, gate, up, down)
-    total = total + expert_part(arrived, *left)
-    total = total + expert_part(arrived, *right)
-    total = total + expert_part(arrived, *far_a)
-    total = total + expert_part(arrived, *far_b)
-    results = total.astype(jnp.bfloat16).reshape(experts, capacity, width_model)
+    outgoing = outgoing.reshape(experts, capacity, width_model)
+    arrived = lax.all_to_all(outgoing, "ep", split_axis=0, concat_axis=0, tiled=True)
+    arrived = arrived.reshape(slots, width_model)
+
+    part = first_parts(
+        arrived,
+        (gate, up, down)
+        + (from_left[0], from_left[2], from_left[1])
+        + (from_right[2], from_right[0], from_right[1]),
+    )
+    gathered, part = lax.optimization_barrier((gathered, part))
+    mixer_term = attention(ep_index.reshape(1), widen(queries), out_weight, gathered)
+    part, mixer_term = lax.optimization_barrier((part, mixer_term))
+    results = last_part(arrived, part, far_gate, far_up, far_top, far_bottom)
+    results = results.reshape(experts, capacity, width_model)
     returned = lax.all_to_all(results, "ep", split_axis=0, concat_axis=0, tiled=True).reshape(
         slots, width_model
     )
 
-    mixer_term = attention(ep_index.reshape(1), widen(queries), out_weight, gathered)
     mixer_summed = lax.psum_scatter(mixer_term, "tp", scatter_dimension=0, tiled=True)
     mixer_out = rms_scale(mixer_summed, out_gain).astype(jnp.bfloat16)
 
@@ -264,4 +428,4 @@
         P("ep", "tp", None),
     )
     out_specs = (P(("ep", "tp"), None), P(("ep", "tp"), None))
-    return jax.shard_map(body, mesh=mesh, in_specs=in_specs, out_specs=out_specs, check_vma=False)
+    return jax.shard_map(inner, mesh=mesh, in_specs=in_specs, out_specs=out_specs, check_vma=False)

time: 273 us -> 250 us (0.916)
  waiting for transfers between devices: 78.3 us -> 127 us
  matrix products: 51 us -> 4.62 us
  starting transfers between devices: 94.5 us -> 62 us
  Pallas kernels: 4.39 us -> 21.2 us
  local copies, waits for them, and re-layouts: 18.1 us -> 8.02 us
    ppermute x12 -> x10, waiting for transfers between devices: 48.9 us -> 97.4 us  [shift(): return lax.ppermute(x, 'tp', [(i, (i + by) % count) for i in range(count)])]
    dot_general x16 -> x6, matrix products: 51 us -> 4.62 us  [the longest x1 2.07 us: inner(): jnp.dot(sent, normed, preferred_element_type=jnp.float32)]
    all_to_all x2, starting transfers between devices: 76.5 us -> 46.5 us  [the longest x1 38.1 us: inner(): lax.all_to_all(results, 'ep', split_axis=0, concat_axis=0, tiled=True)]
    pallas_call x0 -> x2, Pallas kernels: none -> 14.5 us  [the longest x1 8.94 us: first_parts(): pl.pallas_call(first_kernel, out_shape=jax.ShapeDtypeStruct((rows, width)...]
    slice x7 -> x3, local copies, waits for them, and re-layouts: 11.5 us -> 2.31 us  [the longest x1 1.08 us: inner(): far_top = shift(from_left[1][:half], 1)]
    ppermute x12 -> x10, starting transfers between devices: 17.9 us -> 15.3 us  [shift(): return lax.ppermute(x, 'tp', [(i, (i + by) % count) for i in range(count)])]
  transfers between devices with their start and end apart: 16 -> 14, of which waited for: 8 -> 7; matrix products, arithmetic and copies ran while one was open for 25% -> 5% of each run, Pallas kernels for 2% -> 6%
where the time goes in v2:
time: 250 us; the launch traced here: 249 us
  waiting for transfers between devices  127 us (51%)
  starting transfers between devices  62 us (25%)
  Pallas kernels  21.2 us (8%)
  between operations  14.3 us (6%)
  other arithmetic  12.4 us (5%)
  local copies, waits for them, and re-layouts  8.02 us (3%)
  matrix products  4.62 us (2%)
    ppermute x10, waiting for transfers between devices, shift(): return lax.ppermute(x, 'tp', [(i, (i + by) % count) for i in range(count)])  97.4 us
    all_to_all x1, starting transfers between devices, inner(): lax.all_to_all(results, 'ep', split_axis=0, concat_axis=0, tiled=True)  38.1 us
    all_to_all x1, waiting for transfers between devices, inner(): lax.all_to_all(results, 'ep', split_axis=0, concat_axis=0, tiled=True)  29.4 us
    ppermute x10, starting transfers between devices, shift(): return lax.ppermute(x, 'tp', [(i, (i + by) % count) for i in range(count)])  15.3 us
    pallas_call x1, Pallas kernels, first_parts(): pl.pallas_call(first_kernel, out_shape=jax.ShapeDtypeStruct((rows, width)...  8.94 us
    all_to_all x1, starting transfers between devices, inner(): lax.all_to_all(outgoing, 'ep', split_axis=0, concat_axis=0, tiled=True)  8.46 us
    pallas_call x1, Pallas kernels, attention(): pl.pallas_call(attention_kernel, out_shape=jax.ShapeDtypeStruct((width //...  6.7 us
    pallas_call x1, Pallas kernels, last_part(): pl.pallas_call(last_kernel, out_shape=jax.ShapeDtypeStruct((rows, width),...  5.59 us
  transfers between devices with their start and end apart: 14, of which 7 were waited for; matrix products, arithmetic and copies ran while one was open for 5% of the time, Pallas kernels for 6%

profile of v2, /device:TPU:0, one launch (start us, length us, event | category | flops | bytes accessed | tf_op | source)
XLA Modules:
  0.0 249.3 jit_solution(949419521455225447)
XLA Ops:
  9.1 1.0 copy.42
  10.2 1.7 pad_maximum_fusion.1
  11.9 1.7 collective-permute-start
  13.5 1.2 fusion.1
  17.1 1.2 fusion.3
  18.3 2.1 convolution_convert_fusion
  20.4 8.5 %all-to-all-start = ((bf16[32,16,2048]{2,1,0:T(8,128)(2,1)}), bf16[32,16,2048]{2,1,0:T(8,128)(2,1)S(1)}, u32[]{:S(2)}, u32[]{:S(2)}) async-start(bf16[32,16,2048]{2,1,0:T(8,128)(2,1)} %bitcast.8), calls=%async_computation | async-start | bytes 4194304 | tf_op jit(solution)/shard_map/all_to_all | solution.py:372
  28.9 1.8 collective-permute-start.3
  31.0 1.5 collective-permute-start.2
  32.5 1.7 collective-permute-start.4
  34.3 5.2 %collective-permute-done.refs_3_ = bf16[2048,256]{1,0:T(8,128)(2,1)} collective-permute-done((bf16[2048,256]{1,0:T(8,128)(2,1)}, bf16[2048,256]{1,0:T(8,128)(2,1)}, u32[]{:S(2)}, u32[]{:S(2)}) %collective-permute-start) | collective-permute-done | bytes 1048608 | tf_op jit(solution)/shard_map/ppermute | solution.py:302
  39.5 1.7 collective-permute-start.5
  42.7 19.2 %collective-permute-done.1.refs_4_ = bf16[2048,256]{1,0:T(8,128)(2,1)} collective-permute-done((bf16[2048,256]{1,0:T(8,128)(2,1)}, bf16[2048,256]{1,0:T(8,128)(2,1)}, u32[]{:S(2)}, u32[]{:S(2)}) %collective-permute-start.1) | collective-permute-done | bytes 1048608 | tf_op jit(solution)/shard_map/ppermute | solution.py:302
  62.0 21.3 %collective-permute-done.2.refs_5_ = bf16[256,2048]{1,0:T(8,128)(2,1)} collective-permute-done((bf16[256,2048]{1,0:T(8,128)(2,1)}, bf16[256,2048]{1,0:T(8,128)(2,1)}, u32[]{:S(2)}, u32[]{:S(2)}) %collective-permute-start.2) | collective-permute-done | bytes 1048608 | tf_op jit(solution)/shard_map/ppermute | solution.py:302
  83.2 16.4 %collective-permute-done.5.refs_8_ = bf16[256,2048]{1,0:T(8,128)(2,1)} collective-permute-done((bf16[256,2048]{1,0:T(8,128)(2,1)}, bf16[256,2048]{1,0:T(8,128)(2,1)}, u32[]{:S(2)}, u32[]{:S(2)}) %collective-permute-start.5) | collective-permute-done | bytes 1048608 | tf_op jit(solution)/shard_map/ppermute | solution.py:302
  99.6 1.3 copy-done.1
  100.9 8.9 %shard_map.158.part_hbm = f32[512,2048]{1,0:T(8,128)} custom-call(bf16[512,2048]{1,0:T(8,128)(2,1)} %bitcast.38, bf16[2048,256]{1,0:T(8,128)(2,1)} %bitcast.50, bf16[2048,256]{1,0:T(8,128)(2,1)} %bitcast.53, bf16[256,2048]{1,0:T(8,128)(2,1)} %bitcast.56, bf16[2048,256]{1,0:T(8,128)(2,1)} %collective-permute-done.refs_3_, ...), custom_call_target="tpu_custom_call" | custom-call | flops 4831838208 | bytes 9437184 | tf_op jit(solution)/shard_map/pallas_call | solution.py:222
  109.9 6.7 %shard_map.159 = bf16[512,2048]{1,0:T(8,128)(2,1)} custom-call(s32[1]{0:T(128)} %bitcast.13.own_ref, bf16[256,1024]{1,0:T(8,128)(2,1)} %pad_maximum_fusion.q_ref, bf16[256,2048]{1,0:T(8,128)(2,1)} %w_ref.1, bf16[32,528,256]{2,1,0:T(8,128)(2,1)} %bitcast.47), custom_call_target="tpu_custom_call" | custom-call | flops 8999999488 | bytes 12000000 | tf_op jit(solution)/shard_map/pallas_call | solution.py:145
  116.6 1.6 collective-permute-start.6
  118.2 1.7 collective-permute-start.7
  119.9 1.1 slice.35
  121.3 1.1 slice.36
  122.4 3.0 %collective-permute-start.9 = (bf16[128,2048]{1,0:T(8,128)(2,1)S(1)}, bf16[128,2048]{1,0:T(8,128)(2,1)S(1)}, u32[]{:S(2)}, u32[]{:S(2)}) collective-permute-start(bf16[128,2048]{1,0:T(8,128)(2,1)S(1)} %slice.36), channel_id=1, source_target_pairs={{0,3},{1,0},{2,1},{3,2},{4,7},{5,4},{6,5},{7,6},{8,11},{9,8},{10,9... | collective-permute-start | bytes 1572872 | tf_op jit(solution)/shard_map/ppermute | solution.py:302
  125.4 33.0 %collective-permute-done.8.top_half = bf16[128,2048]{1,0:T(8,128)(2,1)S(1)} collective-permute-done((bf16[128,2048]{1,0:T(8,128)(2,1)S(1)}, bf16[128,2048]{1,0:T(8,128)(2,1)S(1)}, u32[]{:S(2)}, u32[]{:S(2)}) %collective-permute-start.8) | collective-permute-done | bytes 524320 | tf_op jit(solution)/shard_map/ppermute | solution.py:302
  158.4 2.4 collective-permute-done.9.bottom_half
  162.5 1.0 copy-done.3
  163.5 5.6 %shard_map.160 = bf16[512,2048]{1,0:T(8,128)(2,1)} custom-call(bf16[512,2048]{1,0:T(8,128)(2,1)} %bitcast.39, f32[512,2048]{1,0:T(8,128)} %shard_map.158.part_hbm, bf16[2048,256]{1,0:T(8,128)(2,1)} %copy-done.2, bf16[2048,256]{1,0:T(8,128)(2,1)} %copy-done.3, bf16[128,2048]{1,0:T(8,128)(2,1)} %copy-done.4, bf16[128,2048]{1,0:T(8,128)(2,1)} %copy-done.5), custom_call_target="tpu_custom_call" | custom-call | flops 1610612736 | bytes 3145728 | tf_op jit(solution)/shard_map/pallas_call | solution.py:280
  169.1 38.1 %all-to-all-start.1 = ((bf16[32,16,2048]{2,1,0:T(8,128)(2,1)}), bf16[32,16,2048]{2,1,0:T(8,128)(2,1)S(1)}, u32[]{:S(2)}, u32[]{:S(2)}) async-start(bf16[32,16,2048]{2,1,0:T(8,128)(2,1)} %bitcast.40), calls=%async_computation.2 | async-start | bytes 4194304 | tf_op jit(solution)/shard_map/all_to_all | solution.py:386
  207.9 29.4 %all-to-all-done.1 = bf16[32,16,2048]{2,1,0:T(8,128)(2,1)S(1)} async-done(((bf16[32,16,2048]{2,1,0:T(8,128)(2,1)}), bf16[32,16,2048]{2,1,0:T(8,128)(2,1)S(1)}, u32[]{:S(2)}, u32[]{:S(2)}) %all-to-all-start.1) | async-done | bytes 2097184 | tf_op jit(solution)/shard_map/all_to_all | solution.py:386
  237.8 1.4 fusion
  239.2 1.2 fusion.4
  240.4 2.0 fusion.6
  (68 shorter events, 9.5 us)
Async XLA Ops:
  7.2 200.1 %copy-start = (bf16[2048,32]{0,1:T(8,128)(2,1)S(1)}, bf16[2048,32]{0,1:T(8,128)(2,1)}, u32[]{:S(2)}) copy-start(bf16[2048,32]{0,1:T(8,128)(2,1)} %param.24) | copy-start | bytes 393220
  7.2 102.7 %all-gather.2.cloned.1.call-start = ((), (), s32[]{:S(2)}) async-start(), calls=%async_computation.3 | async-start | bytes 8921088 | tf_op jit(solution)/shard_map/all_gather | solution.py:351
  11.9 27.6 %collective-permute-start = (bf16[2048,256]{1,0:T(8,128)(2,1)}, bf16[2048,256]{1,0:T(8,128)(2,1)}, u32[]{:S(2)}, u32[]{:S(2)}) collective-permute-start(bf16[2048,256]{1,0:T(8,128)(2,1)} %bitcast.48), channel_id=1, source_target_pairs={{0,1},{1,2},{2,3},{3,0},{4,5},{5,6},{6,7},{7,4},{8,9},{9,10},{10,1... | collective-permute-start | bytes 3145736 | tf_op jit(solution)/shard_map/ppermute | solution.py:302
  20.4 20.7 %copy-start.6 = (bf16[512,256]{1,0:T(8,128)(2,1)S(1)}, bf16[512,256]{1,0:T(8,128)(2,1)}, u32[]{:S(2)}) copy-start(bf16[512,256]{1,0:T(8,128)(2,1)} %param.15) | copy-start | bytes 786436
  20.4 79.2 %all-to-all-start = ((bf16[32,16,2048]{2,1,0:T(8,128)(2,1)}), bf16[32,16,2048]{2,1,0:T(8,128)(2,1)S(1)}, u32[]{:S(2)}, u32[]{:S(2)}) async-start(bf16[32,16,2048]{2,1,0:T(8,128)(2,1)} %bitcast.8), calls=%async_computation | async-start | bytes 4194304 | tf_op jit(solution)/shard_map/all_to_all | solution.py:372
  28.9 210.3 %reduce-scatter.2.cloned.1.call-start = ((), (), s32[]{:S(2)}) async-start(), calls=%async_computation.4 | async-start | bytes 2621440 | tf_op jit(solution)/shard_map/reduce_scatter | solution.py:390
  28.9 54.3 %collective-permute-start.3 = (bf16[2048,256]{1,0:T(8,128)(2,1)}, bf16[2048,256]{1,0:T(8,128)(2,1)}, u32[]{:S(2)}, u32[]{:S(2)}) collective-permute-start(bf16[2048,256]{1,0:T(8,128)(2,1)} %bitcast.49), channel_id=1, source_target_pairs={{0,3},{1,0},{2,1},{3,2},{4,7},{5,4},{6,5},{7,6},{8,11},{9,8},{10,9... | collective-permute-start | bytes 3145736 | tf_op jit(solution)/shard_map/ppermute | solution.py:302
  30.7 31.2 %collective-permute-start.1 = (bf16[2048,256]{1,0:T(8,128)(2,1)}, bf16[2048,256]{1,0:T(8,128)(2,1)}, u32[]{:S(2)}, u32[]{:S(2)}) collective-permute-start(bf16[2048,256]{1,0:T(8,128)(2,1)} %bitcast.51), channel_id=1, source_target_pairs={{0,1},{1,2},{2,3},{3,0},{4,5},{5,6},{6,7},{7,4},{8,9},{9,10},{10,1... | collective-permute-start | bytes 3145736 | tf_op jit(solution)/shard_map/ppermute | solution.py:302
  31.0 52.2 %collective-permute-start.2 = (bf16[256,2048]{1,0:T(8,128)(2,1)}, bf16[256,2048]{1,0:T(8,128)(2,1)}, u32[]{:S(2)}, u32[]{:S(2)}) collective-permute-start(bf16[256,2048]{1,0:T(8,128)(2,1)} %bitcast.54), channel_id=1, source_target_pairs={{0,1},{1,2},{2,3},{3,0},{4,5},{5,6},{6,7},{7,4},{8,9},{9,10},{10,1... | collective-permute-start | bytes 3145736 | tf_op jit(solution)/shard_map/ppermute | solution.py:302
  32.5 50.7 %collective-permute-start.4 = (bf16[2048,256]{1,0:T(8,128)(2,1)}, bf16[2048,256]{1,0:T(8,128)(2,1)}, u32[]{:S(2)}, u32[]{:S(2)}) collective-permute-start(bf16[2048,256]{1,0:T(8,128)(2,1)} %bitcast.52), channel_id=1, source_target_pairs={{0,3},{1,0},{2,1},{3,2},{4,7},{5,4},{6,5},{7,6},{8,11},{9,8},{10,9... | collective-permute-start | bytes 3145736 | tf_op jit(solution)/shard_map/ppermute | solution.py:302
  39.5 60.1 %collective-permute-start.5 = (bf16[256,2048]{1,0:T(8,128)(2,1)}, bf16[256,2048]{1,0:T(8,128)(2,1)}, u32[]{:S(2)}, u32[]{:S(2)}) collective-permute-start(bf16[256,2048]{1,0:T(8,128)(2,1)} %bitcast.55), channel_id=1, source_target_pairs={{0,3},{1,0},{2,1},{3,2},{4,7},{5,4},{6,5},{7,6},{8,11},{9,8},{10,9... | collective-permute-start | bytes 3145736 | tf_op jit(solution)/shard_map/ppermute | solution.py:302
  99.6 1.3 copy-start.1
  116.6 44.2 %collective-permute-start.6 = (bf16[2048,256]{1,0:T(8,128)(2,1)}, bf16[2048,256]{1,0:T(8,128)(2,1)S(1)}, u32[]{:S(2)}, u32[]{:S(2)}) collective-permute-start(bf16[2048,256]{1,0:T(8,128)(2,1)} %collective-permute-done.refs_3_), channel_id=1, source_target_pairs={{0,1},{1,2},{2,3},{3,0},{4,5},{5,6},{6,7},{7,4},{8,9},{9,10},{10,1... | collective-permute-start | bytes 3145736 | tf_op jit(solution)/shard_map/ppermute | solution.py:302
  118.2 43.4 %collective-permute-start.7 = (bf16[2048,256]{1,0:T(8,128)(2,1)}, bf16[2048,256]{1,0:T(8,128)(2,1)S(1)}, u32[]{:S(2)}, u32[]{:S(2)}) collective-permute-start(bf16[2048,256]{1,0:T(8,128)(2,1)} %collective-permute-done.4.refs_7_), channel_id=1, source_target_pairs={{0,3},{1,0},{2,1},{3,2},{4,7},{5,4},{6,5},{7,6},{8,11},{9,8},{10,9... | collective-permute-start | bytes 3145736 | tf_op jit(solution)/shard_map/ppermute | solution.py:302
  121.0 37.4 %collective-permute-start.8 = (bf16[128,2048]{1,0:T(8,128)(2,1)S(1)}, bf16[128,2048]{1,0:T(8,128)(2,1)S(1)}, u32[]{:S(2)}, u32[]{:S(2)}) collective-permute-start(bf16[128,2048]{1,0:T(8,128)(2,1)S(1)} %slice.35), channel_id=1, source_target_pairs={{0,1},{1,2},{2,3},{3,0},{4,5},{5,6},{6,7},{7,4},{8,9},{9,10},{10,1... | collective-permute-start | bytes 1572872 | tf_op jit(solution)/shard_map/ppermute | solution.py:302
  122.4 38.3 %collective-permute-start.9 = (bf16[128,2048]{1,0:T(8,128)(2,1)S(1)}, bf16[128,2048]{1,0:T(8,128)(2,1)S(1)}, u32[]{:S(2)}, u32[]{:S(2)}) collective-permute-start(bf16[128,2048]{1,0:T(8,128)(2,1)S(1)} %slice.36), channel_id=1, source_target_pairs={{0,3},{1,0},{2,1},{3,2},{4,7},{5,4},{6,5},{7,6},{8,11},{9,8},{10,9... | collective-permute-start | bytes 1572872 | tf_op jit(solution)/shard_map/ppermute | solution.py:302
  158.4 3.2 %copy-start.4 = (bf16[128,2048]{1,0:T(8,128)(2,1)}, bf16[128,2048]{1,0:T(8,128)(2,1)S(1)}, u32[]{:S(2)}) copy-start(bf16[128,2048]{1,0:T(8,128)(2,1)S(1)} %collective-permute-done.8.top_half) | copy-start | bytes 1572868
  160.8 0.8 copy-start.5
  161.6 1.0 copy-start.2
  162.5 1.0 copy-start.3
  169.1 38.5 %copy-start.7 = (bf16[2048,4]{0,1:T(4,128)(2,1)S(1)}, bf16[2048,4]{0,1:T(4,128)(2,1)}, u32[]{:S(2)}) copy-start(bf16[2048,4]{0,1:T(4,128)(2,1)} %param.23) | copy-start | bytes 49156
  169.1 68.2 %all-to-all-start.1 = ((bf16[32,16,2048]{2,1,0:T(8,128)(2,1)}), bf16[32,16,2048]{2,1,0:T(8,128)(2,1)S(1)}, u32[]{:S(2)}, u32[]{:S(2)}) async-start(bf16[32,16,2048]{2,1,0:T(8,128)(2,1)} %bitcast.40), calls=%async_computation.2 | async-start | bytes 4194304 | tf_op jit(solution)/shard_map/all_to_all | solution.py:386
  237.8 2.6 %copy-start.8 = (f32[2048]{0:T(1024)S(1)}, f32[2048]{0:T(1024)}, u32[]{:S(2)}) copy-start(f32[2048]{0:T(1024)} %param.20) | copy-start | bytes 24580
Sparse Core Ops, SparseCore 0:
  12.0 71.4 all-gather.1
  116.7 55.2 reduce-scatter.1

commit v3 on v2

--- a/solution.py
+++ b/solution.py
@@ -9,111 +9,241 @@
 DH = 128
 GROUPS = 4
 BLOCK = 512
+PLANE = 8
+DEPTH = 4
 ROOT = math.sqrt(DH)
 LOG2E = 1.4426950408889634
 SCALE = LOG2E / ROOT
 QT = 256
 
 
-def attention_kernel(
-    own_ref, q_ref, w_ref, kv_hbm, out_ref, buf, sems, even, odd, peak_even, peak_odd, top, gap, acc
+def put_rows(stat, first, row, half):
+    for h in range(2):
+        rest = row[:, h * half : (h + 1) * half]
+        for p in range(3):
+            piece = rest.astype(jnp.bfloat16).astype(jnp.float32)
+            stat[first + 3 * h + p : first + 3 * h + p + 1, :] = piece
+            rest = rest - piece
+
+
+def attend_kernel(
+    pos_ref, q0, q1, q2, q3, kv_hbm, o0, o1, o2, o3,
+    kv, raw, sems, wide, keys, values, even, odd, peak_even, peak_odd, top, gap, acc, stat,
 ):
-    own = own_ref[0]
-    width = q_ref.shape[1]
+    own, ahead = pos_ref[0], DEPTH - 1 - pos_ref[1]
+    width = wide.shape[2]
     half = width // 2
     tiles = [slice(t * QT, (t + 1) * QT) for t in range(width // QT)]
-
-    def copy(j):
-        return pltpu.make_async_copy(kv_hbm.at[j], buf.at[j], sems.at[j])
-
-    def launch(i, carry):
-        copy(own - i).start()
+    arriving = [pltpu.make_async_copy(q, raw.at[s], sems.at[s]) for s, q in enumerate((q0, q1, q2, q3))]
+    arriving += [
+        pltpu.make_async_copy(kv_hbm.at[b], kv.at[b], sems.at[DEPTH + b]) for b in range(PLANE)
+    ]
+    for c in arriving:
+        c.start()
+    top[...] = jnp.full_like(top, -1e30)
+    acc[...] = jnp.zeros_like(acc)
+    line = lax.broadcasted_iota(jnp.int32, (DH, width), 0)
+    head = lax.broadcasted_iota(jnp.int32, (DH, width), 1) // half
+    index = line % 8
+    pick = (line < 16) & (index >= 3 * head) & (index < 3 * head + 3)
+    picks = jnp.where(pick, -1.0, 0.0).astype(jnp.bfloat16)
+    for s in range(DEPTH):
+        arriving[s].wait()
+
+    def turn(s, carry):
+        turned = jnp.transpose(raw[s].astype(jnp.float32)).astype(jnp.bfloat16)
+        for h in range(2):
+            wide[s, :DH, h * half : (h + 1) * half] = turned[h * DH : (h + 1) * DH, :]
+        wide[s, DH:, :] = picks
         return carry
 
-    lax.fori_loop(0, own + 1, launch, 0)
-    top[...] = jnp.full_like(top, -1e30)
-    gap[...] = jnp.zeros_like(gap)
-    acc[...] = jnp.zeros_like(acc)
-
-    def keys_of(j):
-        gates = buf[j, BLOCK:, :]
+    lax.fori_loop(0, ahead + 1, turn, 0)
+    for b in range(PLANE):
+        arriving[DEPTH + b].wait()
+    sums = jnp.zeros((1, width), jnp.float32)
+    first_total = None
+    for b in reversed(range(PLANE)):
+        gates = kv[b, BLOCK:, :]
+        last = gates[:, DH:].astype(jnp.float32)
+        total = jnp.concatenate(
+            [
+                jnp.broadcast_to(
+                    last[8 + 3 * h : 9 + 3 * h, DH - 1 : DH]
+                    + last[9 + 3 * h : 10 + 3 * h, DH - 1 : DH]
+                    + last[10 + 3 * h : 11 + 3 * h, DH - 1 : DH],
+                    (1, half),
+                )
+                for h in range(2)
+            ],
+            axis=1,
+        )
+        if b == PLANE - 1:
+            first_total = total
+        else:
+            sums = sums + total
+        gap[b] = sums
+
+    def prepare(b, carry):
+        gates = kv[b, BLOCK:, :]
         gates = jnp.concatenate([gates, jnp.zeros((DH - 16, 2 * DH), jnp.bfloat16)], axis=0)
         turned = jnp.transpose(gates.astype(jnp.float32)).astype(jnp.bfloat16)
         lane = lax.broadcasted_iota(jnp.int32, turned.shape, 1)
         zero = jnp.zeros_like(turned)
-        extra = jnp.concatenate(
-            [jnp.where(lane < 8, turned, zero), jnp.where(lane < 8, zero, turned)], axis=0
-        )
-        return jnp.concatenate([buf[j, :BLOCK, :DH], extra], axis=1)
-
-    def values_of(j):
-        values = jnp.concatenate(
-            [buf[j, c * DH : (c + 1) * DH, DH:] for c in range(BLOCK // DH)], axis=1
-        )
-        return jnp.concatenate([values, jnp.ones((16, BLOCK), jnp.bfloat16)], axis=0)
-
-    def move_gap(j, alive):
-        last = buf[j, BLOCK:, DH:].astype(jnp.float32)
-        dead = jnp.where(alive, 0.0, -1e30)
-        for h in range(2):
-            total = (
-                last[8 + 3 * h : 9 + 3 * h, DH - 1 : DH]
-                + last[9 + 3 * h : 10 + 3 * h, DH - 1 : DH]
-                + last[10 + 3 * h : 11 + 3 * h, DH - 1 : DH]
-                + dead
-            )
-            gap[:, h * half : (h + 1) * half] = gap[:, h * half : (h + 1) * half] + total
-
-    def score(keys, t, into, peak, masked):
-        s = jnp.dot(keys, q_ref[:, tiles[t]], preferred_element_type=jnp.float32)
+        keys[b, :, :DH] = kv[b, :BLOCK, :DH]
+        keys[b, : 2 * DH, DH:] = jnp.where(lane < 8, turned, zero)
+        keys[b, 2 * DH :, DH:] = jnp.where(lane < 8, zero, turned)
+        for c in range(BLOCK // DH):
+            values[b, :DH, c * DH : (c + 1) * DH] = kv[b, c * DH : (c + 1) * DH, DH:]
+        values[b, DH:, :] = jnp.ones((16, BLOCK), jnp.bfloat16)
+        return carry
+
+    lax.fori_loop(0, PLANE, prepare, 0)
+    steps = own + 1 + PLANE * ahead
+
+    def place(n):
+        m = jnp.maximum(n - (own + 1), 0)
+        mine = n <= own
+        s = jnp.where(mine, 0, jnp.minimum(1 + (m >> 3), DEPTH - 1))
+        b = jnp.where(mine, own - n, PLANE - 1 - (m & 7))
+        return s, b
+
+    def score(s, b, t, into, peak, masked):
+        scores = jnp.dot(keys[b], wide[s, :, tiles[t]], preferred_element_type=jnp.float32)
         if masked:
-            key_at = lax.broadcasted_iota(jnp.int32, s.shape, 0)
-            query_at = lax.broadcasted_iota(jnp.int32, s.shape, 1) + (t * QT) % half
-            s = jnp.where(key_at <= query_at, s, -1e30)
-        into[:, tiles[t]] = s
-        peak[:, tiles[t]] = jnp.max(s, axis=0, keepdims=True)
-
-    def absorb(values, t, held, peak):
+            key_at = lax.broadcasted_iota(jnp.int32, scores.shape, 0)
+            query_at = lax.broadcasted_iota(jnp.int32, scores.shape, 1) + (t * QT) % half
+            scores = jnp.where(key_at <= query_at, scores, -1e30)
+        into[:, tiles[t]] = scores
+        peak[:, tiles[t]] = jnp.max(scores, axis=0, keepdims=True)
+
+    def absorb(s, b, dead, t, held, peak):
         cols = tiles[t]
-        old = top[:, cols]
-        new = jnp.maximum(old, peak[:, cols] + gap[:, cols])
-        top[:, cols] = new
-        p = jnp.exp2(held[:, cols] * SCALE - (new - gap[:, cols]) * SCALE)
-        part = jnp.dot(values, p.astype(jnp.bfloat16), preferred_element_type=jnp.float32)
-        acc[:, cols] = acc[:, cols] * jnp.exp2((old - new) * SCALE) + part
-
-    def phase(now, later, held, held_peak, into, into_peak):
-        values = values_of(jnp.maximum(now, 0))
-        keys = keys_of(jnp.maximum(later, 0))
+        old = top[s, :, cols]
+        shift = gap[b, :, cols] + dead
+        new = jnp.maximum(old, peak[:, cols] + shift)
+        top[s, :, cols] = new
+        p = jnp.exp2(held[:, cols] * SCALE - (new - shift) * SCALE)
+        part = jnp.dot(values[b], p.astype(jnp.bfloat16), preferred_element_type=jnp.float32)
+        acc[s, :, cols] = acc[s, :, cols] * jnp.exp2((old - new) * SCALE) + part
+
+    def phase(n, held, held_peak, into, into_peak):
+        s, b = place(n)
+        dead = jnp.where(n < steps, 0.0, -1e30)
+        later_s, later_b = place(n + 1)
         for t in range(len(tiles)):
-            score(keys, t, into, into_peak, False)
-            absorb(values, t, held, held_peak)
-        move_gap(jnp.maximum(later, 0), later >= 0)
-
-    def arrive(j):
-        @pl.when(j >= 0)
+            score(later_s, later_b, t, into, into_peak, False)
+            absorb(s, b, dead, t, held, held_peak)
+
+    for t in range(len(tiles)):
+        score(0, own, t, even, peak_even, True)
+
+    def step(i, carry):
+        phase(2 * i, even, peak_even, odd, peak_odd)
+        phase(2 * i + 1, odd, peak_odd, even, peak_even)
+        return carry
+
+    lax.fori_loop(0, (steps + 1) >> 1, step, 0)
+    for s, out in enumerate((o0, o1, o2, o3)):
+
+        @pl.when(s <= ahead)
         def _():
-            copy(j).wait()
-
-    copy(own).wait()
-    keys = keys_of(own)
-    for t in range(len(tiles)):
-        score(keys, t, even, peak_even, True)
-
-    def step(i, carry):
-        now = own - 2 * i
-        arrive(now - 1)
-        arrive(now - 2)
-        phase(now, now - 1, even, peak_even, odd, peak_odd)
-        phase(now - 1, now - 2, odd, peak_odd, even, peak_even)
-        return carry
-
-    lax.fori_loop(0, lax.div(own + 2, 2), step, 0)
-    total = acc[DH : DH + 1, :]
-    attended = acc[:DH, :] / total
-    stacked = jnp.concatenate([attended[:, :half], attended[:, half:]], axis=0)
-    rows = jnp.transpose(stacked).astype(jnp.bfloat16)
-    out_ref[...] = jnp.dot(rows, w_ref[...], preferred_element_type=jnp.float32).astype(jnp.bfloat16)
+            weight = acc[s, DH : DH + 1, :]
+            mean = acc[s, :DH, :] / weight
+            for h in range(2):
+                out[h * DH : (h + 1) * DH, :] = mean[:, h * half : (h + 1) * half].astype(jnp.bfloat16)
+            level = top[s] * SCALE + jnp.log(weight) * LOG2E
+            if s == 0:
+                level = level - gap[own] * SCALE
+                passed = gap[0] - gap[own]
+            else:
+                level = level + first_total * SCALE
+                passed = gap[0] + first_total
+            stat[...] = jnp.zeros_like(stat)
+            put_rows(stat, 0, level, half)
+            put_rows(stat, 6, passed * SCALE, half)
+            out[2 * DH :, :] = stat[...].astype(jnp.bfloat16)
+
+
+def attend(pos, sets, kv):
+    rows = sets[0].shape[0]
+    width = 2 * rows
+    return pl.pallas_call(
+        attend_kernel,
+        out_shape=[jax.ShapeDtypeStruct((2 * DH + 16, rows), jnp.bfloat16)] * DEPTH,
+        in_specs=[pl.BlockSpec(memory_space=pltpu.SMEM)]
+        + [pl.BlockSpec(memory_space=pltpu.HBM)] * (DEPTH + 1),
+        out_specs=[pl.BlockSpec(memory_space=pltpu.VMEM)] * DEPTH,
+        scratch_shapes=[
+            pltpu.VMEM(kv.shape, jnp.bfloat16),
+            pltpu.VMEM((DEPTH, rows, 2 * DH), jnp.bfloat16),
+            pltpu.SemaphoreType.DMA((DEPTH + PLANE,)),
+            pltpu.VMEM((DEPTH, 2 * DH, width), jnp.bfloat16),
+            pltpu.VMEM((PLANE, BLOCK, 2 * DH), jnp.bfloat16),
+            pltpu.VMEM((PLANE, DH + 16, BLOCK), jnp.bfloat16),
+            pltpu.VMEM((BLOCK, width), jnp.float32),
+            pltpu.VMEM((BLOCK, width), jnp.float32),
+            pltpu.VMEM((1, width), jnp.float32),
+            pltpu.VMEM((1, width), jnp.float32),
+            pltpu.VMEM((DEPTH, 1, width), jnp.float32),
+            pltpu.VMEM((PLANE, 1, width), jnp.float32),
+            pltpu.VMEM((DEPTH, DH + 16, width), jnp.float32),
+            pltpu.VMEM((16, rows), jnp.float32),
+        ],
+        cost_estimate=pl.CostEstimate(
+            flops=9_000_000_000, bytes_accessed=4_000_000, transcendentals=16_000_000
+        ),
+    )(pos, *sets, kv)
+
+
+def merge_kernel(pos_ref, p0, p1, p2, p3, w_ref, out_ref):
+    depth = pos_ref[1]
+    parts = (p0, p1, p2, p3)
+
+    def read(ref, first):
+        stat = ref[2 * DH :, :].astype(jnp.float32)
+        return [
+            sum(stat[first + 3 * h + p : first + 3 * h + p + 1, :] for p in range(3)) for h in range(2)
+        ]
+
+    merged = []
+    passed = read(p0, 6)
+    levels = [read(p0, 0)]
+    for d in range(1, DEPTH):
+        own = read(parts[d], 0)
+        lost = jnp.where(d <= depth, 0.0, -1e30)
+        levels.append([own[h] + passed[h] + lost for h in range(2)])
+        more = read(parts[d], 6)
+        passed = [passed[h] + more[h] for h in range(2)]
+    for h in range(2):
+        high = levels[0][h]
+        for d in range(1, DEPTH):
+            high = jnp.maximum(high, levels[d][h])
+        weights = [jnp.exp2(levels[d][h] - high) for d in range(DEPTH)]
+        total = weights[0] + weights[1] + weights[2] + weights[3]
+        mixed = None
+        for d in range(DEPTH):
+            term = parts[d][h * DH : (h + 1) * DH, :].astype(jnp.float32) * (weights[d] / total)
+            mixed = term if mixed is None else mixed + term
+        merged.append(mixed)
+    attended = jnp.transpose(jnp.concatenate(merged, axis=0)).astype(jnp.bfloat16)
+    for n in range(0, out_ref.shape[1], 512):
+        out_ref[:, n : n + 512] = jnp.dot(
+            attended, w_ref[:, n : n + 512], preferred_element_type=jnp.float32
+        ).astype(jnp.bfloat16)
+
+
+def merge(pos, parts, w):
+    rows = parts[0].shape[1]
+    return pl.pallas_call(
+        merge_kernel,
+        out_shape=jax.ShapeDtypeStruct((rows, w.shape[1]), jnp.bfloat16),
+        in_specs=[pl.BlockSpec(memory_space=pltpu.SMEM)]
+        + [pl.BlockSpec(memory_space=pltpu.VMEM)] * (DEPTH + 1),
+        out_specs=pl.BlockSpec(memory_space=pltpu.VMEM),
+        cost_estimate=pl.CostEstimate(
+            flops=2 * rows * w.shape[0] * w.shape[1], bytes_accessed=4_000_000, transcendentals=8 * rows
+        ),
+    )(pos, *parts, w)
 
 
 def three(x):
@@ -127,44 +257,6 @@
     parts = three(gates * ROOT).reshape(6, 2, 2 * DH).transpose(1, 0, 2)
     parts = jnp.pad(parts, ((0, 0), (0, 2), (0, 0))).reshape(16, 2 * DH)
     return jnp.concatenate([jnp.concatenate([keys, turned], axis=1), parts], axis=0)
-
-
-def widen(queries):
-    rows = queries.shape[0]
-    q = queries.reshape(rows, 2, DH).transpose(2, 1, 0).reshape(DH, 2 * rows)
-    line = jnp.arange(DH, dtype=jnp.int32)[:, None]
-    head = (jnp.arange(2 * rows, dtype=jnp.int32) // rows)[None, :]
-    idx = line % 8
-    pick = (line < 16) & (idx >= 3 * head) & (idx < 3 * head + 3)
-    return jnp.concatenate([q, jnp.where(pick, -1.0, 0.0).astype(jnp.bfloat16)], axis=0)
-
-
-def attention(own, q, w, kv):
-    n = kv.shape[0]
-    width = q.shape[1]
-    return pl.pallas_call(
-        attention_kernel,
-        out_shape=jax.ShapeDtypeStruct((width // 2, w.shape[1]), jnp.bfloat16),
-        in_specs=[
-            pl.BlockSpec(memory_space=pltpu.SMEM),
-            pl.BlockSpec(memory_space=pltpu.VMEM),
-            pl.BlockSpec(memory_space=pltpu.VMEM),
-            pl.BlockSpec(memory_space=pltpu.HBM),
-        ],
-        out_specs=pl.BlockSpec(memory_space=pltpu.VMEM),
-        scratch_shapes=[
-            pltpu.VMEM(kv.shape, jnp.bfloat16),
-            pltpu.SemaphoreType.DMA((n,)),
-            pltpu.VMEM((BLOCK, width), jnp.float32),
-            pltpu.VMEM((BLOCK, width), jnp.float32),
-            pltpu.VMEM((1, width), jnp.float32),
-            pltpu.VMEM((1, width), jnp.float32),
-            pltpu.VMEM((1, width), jnp.float32),
-            pltpu.VMEM((1, width), jnp.float32),
-            pltpu.VMEM((DH + 16, width), jnp.float32),
-        ],
-        cost_estimate=pl.CostEstimate(flops=9_000_000_000, bytes_accessed=12_000_000, transcendentals=16_000_000),
-    )(own, q, w, kv)
 
 
 def expert_hidden(x_ref, both, hidden_ref, at):
@@ -348,8 +440,19 @@
 
     running = jnp.cumsum(jax.nn.log_sigmoid(forget_logit), axis=1)
     packed = pack(key_rows, value_rows, running)
-    gathered = lax.all_gather(packed, "ep", axis=0, tiled=True)
-    gathered = gathered.reshape(ep_count, *packed.shape)
+    planes = [[z * PLANE + i for i in range(PLANE)] for z in range(ep_count // PLANE)]
+    gathered = lax.all_gather(packed, "ep", axis=0, tiled=True, axis_index_groups=planes)
+    gathered = gathered.reshape(PLANE, *packed.shape)
+    place = jnp.stack([ep_index % PLANE, ep_index // PLANE])
+    asked = [queries]
+    for d in range(1, DEPTH):
+        pairs = [(i, i - PLANE * d) for i in range(PLANE * d, ep_count)]
+        asked.append(lax.ppermute(queries, "ep", pairs))
+    answers = attend(place, asked, gathered)
+    told = [answers[0]]
+    for d in range(1, DEPTH):
+        pairs = [(i, i + PLANE * d) for i in range(ep_count - PLANE * d)]
+        told.append(lax.ppermute(answers[d], "ep", pairs))
 
     own_first = tp_index * own_rows
     own_group = lax.dynamic_slice_in_dim(route_group, own_first, own_rows, 0)
@@ -357,8 +460,8 @@
     chosen = own_group[:, None] * per_group + own_pick
     expert_hit = chosen[:, :, None] == jnp.arange(experts, dtype=jnp.int32)
     usage = jnp.any(expert_hit, axis=1).astype(jnp.bfloat16)
-    place = jnp.arange(own_rows, dtype=jnp.int32)
-    earlier = (place[None, :] < place[:, None]).astype(jnp.bfloat16)
+    line = jnp.arange(own_rows, dtype=jnp.int32)
+    earlier = (line[None, :] < line[:, None]).astype(jnp.bfloat16)
     before = jnp.dot(earlier, usage, preferred_element_type=jnp.float32).astype(jnp.int32)
     ranks = jnp.sum(jnp.where(expert_hit, before[:, None, :], 0), axis=2)
     target = jnp.where(ranks < capacity, chosen * capacity + ranks, slots)
@@ -378,9 +481,7 @@
         + (from_left[0], from_left[2], from_left[1])
         + (from_right[2], from_right[0], from_right[1]),
     )
-    gathered, part = lax.optimization_barrier((gathered, part))
-    mixer_term = attention(ep_index.reshape(1), widen(queries), out_weight, gathered)
-    part, mixer_term = lax.optimization_barrier((part, mixer_term))
+    mixer_term = merge(place, told, out_weight)
     results = last_part(arrived, part, far_gate, far_up, far_top, far_bottom)
     results = results.reshape(experts, capacity, width_model)
     returned = lax.all_to_all(results, "ep", split_axis=0, concat_axis=0, tiled=True).reshape(

time: 250 us -> 231 us (0.924)
  waiting for transfers between devices: 127 us -> 103 us
  Pallas kernels: 21.2 us -> 42.1 us
  starting transfers between devices: 62 us -> 46.9 us
    ppermute x10, waiting for transfers between devices: 97.4 us -> 66.9 us  [shift(): return lax.ppermute(x, 'tp', [(i, (i + by) % count) for i in range(count)])]
    all_to_all x1, starting transfers between devices: 38.1 us -> 8.88 us  [inner(): lax.all_to_all(results, 'ep', split_axis=0, concat_axis=0, tiled=True)]
    pallas_call x1 -> x2, Pallas kernels: 6.7 us -> 27.7 us  [the longest x1 23.8 us: attend(): pl.pallas_call(attend_kernel, out_shape=[jax.ShapeDtypeStruct((2 * DH + 1...]
    ppermute x0 -> x6, starting transfers between devices: none -> 8.49 us  [the longest x3 4.61 us: inner(): told.append(lax.ppermute(answers[d], 'ep', pairs))]
    ppermute x0 -> x6, waiting for transfers between devices: none -> 4.16 us  [the longest x3 4.15 us: inner(): told.append(lax.ppermute(answers[d], 'ep', pairs))]
    ppermute x10, starting transfers between devices: 15.3 us -> 19.2 us  [shift(): return lax.ppermute(x, 'tp', [(i, (i + by) % count) for i in range(count)])]
    unnamed x20 -> x21, local copies, waits for them, and re-layouts: 4.13 us -> 1.36 us
  transfers between devices with their start and end apart: 14 -> 20, of which waited for: 7 -> 9; matrix products, arithmetic and copies ran while one was open for 5% -> 6% of each run, Pallas kernels for 6% -> 18%
where the time goes in v3:
time: 231 us; the launch traced here: 229 us
  waiting for transfers between devices  103 us (45%)
  starting transfers between devices  46.9 us (20%)
  Pallas kernels  42.1 us (18%)
  between operations  14.3 us (6%)
  other arithmetic  11.9 us (5%)
  local copies, waits for them, and re-layouts  6.41 us (3%)
  matrix products  4.54 us (2%)
    ppermute x10, waiting for transfers between devices, shift(): return lax.ppermute(x, 'tp', [(i, (i + by) % count) for i in range(count)])  66.9 us
    all_to_all x1, waiting for transfers between devices, inner(): lax.all_to_all(results, 'ep', split_axis=0, concat_axis=0, tiled=True)  29.4 us
    pallas_call x1, Pallas kernels, attend(): pl.pallas_call(attend_kernel, out_shape=[jax.ShapeDtypeStruct((2 * DH + 1...  23.8 us
    ppermute x10, starting transfers between devices, shift(): return lax.ppermute(x, 'tp', [(i, (i + by) % count) for i in range(count)])  19.2 us
    all_to_all x1, starting transfers between devices, inner(): lax.all_to_all(outgoing, 'ep', split_axis=0, concat_axis=0, tiled=True)  10.2 us
    pallas_call x1, Pallas kernels, first_parts(): pl.pallas_call(first_kernel, out_shape=jax.ShapeDtypeStruct((rows, width)...  8.9 us
    all_to_all x1, starting transfers between devices, inner(): lax.all_to_all(results, 'ep', split_axis=0, concat_axis=0, tiled=True)  8.88 us
    pallas_call x1, Pallas kernels, last_part(): pl.pallas_call(last_kernel, out_shape=jax.ShapeDtypeStruct((rows, width),...  5.51 us
  transfers between devices with their start and end apart: 20, of which 9 were waited for; matrix products, arithmetic and copies ran while one was open for 6% of the time, Pallas kernels for 18%

profile of v3, /device:TPU:0, one launch (start us, length us, event | category | flops | bytes accessed | tf_op | source)
XLA Modules:
  0.0 229.2 jit_solution(8866878927118503630)
XLA Ops:
  10.2 1.6 pad_maximum_fusion
  11.8 1.3 collective-permute-start
  13.1 1.3 collective-permute-start.1
  14.4 1.3 collective-permute-start.2
  15.7 2.9 %collective-permute-start.10 = (bf16[2048,256]{1,0:T(8,128)(2,1)}, bf16[2048,256]{1,0:T(8,128)(2,1)}, u32[]{:S(2)}, u32[]{:S(2)}) collective-permute-start(bf16[2048,256]{1,0:T(8,128)(2,1)} %bitcast.47), channel_id=1, source_target_pairs={{0,3},{1,0},{2,1},{3,2},{4,7},{5,4},{6,5},{7,6},{8,11},{9,8},{10,9... | collective-permute-start | bytes 3145736 | tf_op jit(solution)/shard_map/ppermute | solution.py:394
  23.5 2.0 convolution_convert_fusion
  25.5 10.2 %all-to-all-start = ((bf16[32,16,2048]{2,1,0:T(8,128)(2,1)}), bf16[32,16,2048]{2,1,0:T(8,128)(2,1)S(1)}, u32[]{:S(2)}, u32[]{:S(2)}) async-start(bf16[32,16,2048]{2,1,0:T(8,128)(2,1)} %bitcast.12), calls=%async_computation.1 | async-start | bytes 4194304 | tf_op jit(solution)/shard_map/all_to_all | solution.py:475
  37.3 2.5 %all-gather.2.cloned.1.call-done = bf16[4224,256]{1,0:T(8,128)(2,1)} async-done(((bf16[528,256]{1,0:T(8,128)(2,1)}), bf16[4224,256]{1,0:T(8,128)(2,1)}) %all-gather.2.cloned.1.call-update) | async-done | bytes 2162704 | tf_op jit(solution)/shard_map/all_gather | solution.py:444
  39.9 23.8 %shard_map.158 = (bf16[272,512]{1,0:T(8,128)(2,1)}, bf16[272,512]{1,0:T(8,128)(2,1)}, bf16[272,512]{1,0:T(8,128)(2,1)}, bf16[272,512]{1,0:T(8,128)(2,1)}) custom-call(s32[2]{0:T(128)} %pad_add_fusion.pos_ref, bf16[512,256]{1,0:T(8,128)(2,1)} %q0.1, bf16[512,256]{1,0:T(8,128)(2,1)} %copy-done.7, bf16[512,256]{1,0:T(8,128)(2,1)} %copy-done.8, ...), custom_call_target="tpu_custom_call" | custom-call | flops 8999999488 | bytes 4000000 | tf_op jit(solution)/shard_map/pallas_call | solution.py:170
  63.6 1.3 collective-permute-start.3
  65.0 1.3 collective-permute-start.4
  66.3 2.0 collective-permute-start.5
  68.3 4.0 %collective-permute-done.3.p1 = bf16[272,512]{1,0:T(8,128)(2,1)S(1)} collective-permute-done((bf16[272,512]{1,0:T(8,128)(2,1)}, bf16[272,512]{1,0:T(8,128)(2,1)S(1)}, u32[]{:S(2)}, u32[]{:S(2)}) %collective-permute-start.3) | collective-permute-done | bytes 278560 | tf_op jit(solution)/shard_map/ppermute | solution.py:455
  72.3 5.4 %collective-permute-start.11 = (bf16[256,2048]{1,0:T(8,128)(2,1)}, bf16[256,2048]{1,0:T(8,128)(2,1)}, u32[]{:S(2)}, u32[]{:S(2)}) collective-permute-start(bf16[256,2048]{1,0:T(8,128)(2,1)} %bitcast.51), channel_id=1, source_target_pairs={{0,3},{1,0},{2,1},{3,2},{4,7},{5,4},{6,5},{7,6},{8,11},{9,8},{10,9... | collective-permute-start | bytes 3145736 | tf_op jit(solution)/shard_map/ppermute | solution.py:394
  77.8 4.3 %collective-permute-start.7 = (bf16[2048,256]{1,0:T(8,128)(2,1)}, bf16[2048,256]{1,0:T(8,128)(2,1)}, u32[]{:S(2)}, u32[]{:S(2)}) collective-permute-start(bf16[2048,256]{1,0:T(8,128)(2,1)} %bitcast.48), channel_id=1, source_target_pairs={{0,1},{1,2},{2,3},{3,0},{4,5},{5,6},{6,7},{7,4},{8,9},{9,10},{10,1... | collective-permute-start | bytes 3145736 | tf_op jit(solution)/shard_map/ppermute | solution.py:394
  83.2 3.9 %shard_map.159 = bf16[512,2048]{1,0:T(8,128)(2,1)} custom-call(s32[2]{0:T(128)} %pad_add_fusion.pos_ref, bf16[272,512]{1,0:T(8,128)(2,1)} %get-tuple-element.6.p0, bf16[272,512]{1,0:T(8,128)(2,1)} %copy-done.3, bf16[272,512]{1,0:T(8,128)(2,1)} %copy-done.4, bf16[272,512]{1,0:T(8,128)(2,1)} %collective-permute-done.5.p3, bf16[256,2048]{1,0:T(8,128)(2,1)} %w_ref.1), custom_call_target="tpu_custom_call" | custom-call | flops 536870912 | bytes 4000000 | tf_op jit(solution)/shard_map/pallas_call | solution.py:237
  88.1 2.4 %collective-permute-start.13 = (bf16[2048,256]{1,0:T(8,128)(2,1)}, bf16[2048,256]{1,0:T(8,128)(2,1)}, u32[]{:S(2)}, u32[]{:S(2)}) collective-permute-start(bf16[2048,256]{1,0:T(8,128)(2,1)} %collective-permute-done.10.refs_7_), channel_id=1, source_target_pairs={{0,3},{1,0},{2,1},{3,2},{4,7},{5,4},{6,5},{7,6},{8,11},{9,8},{10,9... | collective-permute-start | bytes 3145736 | tf_op jit(solution)/shard_map/ppermute | solution.py:394
  90.5 1.9 slice.35
  92.4 10.8 %collective-permute-done.11.refs_8_ = bf16[256,2048]{1,0:T(8,128)(2,1)} collective-permute-done((bf16[256,2048]{1,0:T(8,128)(2,1)}, bf16[256,2048]{1,0:T(8,128)(2,1)}, u32[]{:S(2)}, u32[]{:S(2)}) %collective-permute-start.11) | collective-permute-done | bytes 1048608 | tf_op jit(solution)/shard_map/ppermute | solution.py:394
  103.1 1.9 slice.36
  105.0 8.6 %collective-permute-done.7.refs_4_ = bf16[2048,256]{1,0:T(8,128)(2,1)} collective-permute-done((bf16[2048,256]{1,0:T(8,128)(2,1)}, bf16[2048,256]{1,0:T(8,128)(2,1)}, u32[]{:S(2)}, u32[]{:S(2)}) %collective-permute-start.7) | collective-permute-done | bytes 1048608 | tf_op jit(solution)/shard_map/ppermute | solution.py:394
  113.6 1.4 collective-permute-start.15
  115.0 25.9 %collective-permute-done.9.refs_6_ = bf16[2048,256]{1,0:T(8,128)(2,1)} collective-permute-done((bf16[2048,256]{1,0:T(8,128)(2,1)}, bf16[2048,256]{1,0:T(8,128)(2,1)}, u32[]{:S(2)}, u32[]{:S(2)}) %collective-permute-start.9) | collective-permute-done | bytes 1048608 | tf_op jit(solution)/shard_map/ppermute | solution.py:394
  140.8 1.3 copy-done.1
  142.1 8.9 %shard_map.160.part_hbm = f32[512,2048]{1,0:T(8,128)} custom-call(bf16[512,2048]{1,0:T(8,128)(2,1)} %bitcast.36, bf16[2048,256]{1,0:T(8,128)(2,1)} %bitcast.46, bf16[2048,256]{1,0:T(8,128)(2,1)} %bitcast.49, bf16[256,2048]{1,0:T(8,128)(2,1)} %bitcast.52, bf16[2048,256]{1,0:T(8,128)(2,1)} %collective-permute-done.6.refs_3_, ...), custom_call_target="tpu_custom_call" | custom-call | flops 4831838208 | bytes 9437184 | tf_op jit(solution)/shard_map/pallas_call | solution.py:314
  151.1 7.1 %collective-permute-done.14.top_half = bf16[128,2048]{1,0:T(8,128)(2,1)S(1)} collective-permute-done((bf16[128,2048]{1,0:T(8,128)(2,1)}, bf16[128,2048]{1,0:T(8,128)(2,1)S(1)}, u32[]{:S(2)}, u32[]{:S(2)}) %collective-permute-start.14) | collective-permute-done | bytes 524320 | tf_op jit(solution)/shard_map/ppermute | solution.py:394
  158.1 14.6 %collective-permute-done.15.bottom_half = bf16[128,2048]{1,0:T(8,128)(2,1)} collective-permute-done((bf16[128,2048]{1,0:T(8,128)(2,1)}, bf16[128,2048]{1,0:T(8,128)(2,1)}, u32[]{:S(2)}, u32[]{:S(2)}) %collective-permute-start.15) | collective-permute-done | bytes 524320 | tf_op jit(solution)/shard_map/ppermute | solution.py:394
  172.8 5.5 %shard_map.161 = bf16[512,2048]{1,0:T(8,128)(2,1)} custom-call(bf16[512,2048]{1,0:T(8,128)(2,1)} %bitcast.37, f32[512,2048]{1,0:T(8,128)} %shard_map.160.part_hbm, bf16[2048,256]{1,0:T(8,128)(2,1)} %collective-permute-done.12.gate, bf16[2048,256]{1,0:T(8,128)(2,1)} %collective-permute-done.13.up, bf16[128,2048]{1,0:T(8,128)(2,1)} %copy-done.2, ...), custom_call_target="tpu_custom_call" | custom-call | flops 1610612736 | bytes 3145728 | tf_op jit(solution)/shard_map/pallas_call | solution.py:372
  178.3 8.9 %all-to-all-start.1 = ((bf16[32,16,2048]{2,1,0:T(8,128)(2,1)}), bf16[32,16,2048]{2,1,0:T(8,128)(2,1)S(1)}, u32[]{:S(2)}, u32[]{:S(2)}) async-start(bf16[32,16,2048]{2,1,0:T(8,128)(2,1)} %bitcast.38), calls=%async_computation.2 | async-start | bytes 4194304 | tf_op jit(solution)/shard_map/all_to_all | solution.py:487
  187.9 29.4 %all-to-all-done.1 = bf16[32,16,2048]{2,1,0:T(8,128)(2,1)S(1)} async-done(((bf16[32,16,2048]{2,1,0:T(8,128)(2,1)}), bf16[32,16,2048]{2,1,0:T(8,128)(2,1)S(1)}, u32[]{:S(2)}, u32[]{:S(2)}) %all-to-all-start.1) | async-done | bytes 2097184 | tf_op jit(solution)/shard_map/all_to_all | solution.py:487
  217.8 1.3 fusion
  220.4 2.0 fusion.3
  (76 shorter events, 14.0 us)
Async XLA Ops:
  7.2 180.0 %copy-start = (bf16[2048,32]{0,1:T(8,128)(2,1)S(1)}, bf16[2048,32]{0,1:T(8,128)(2,1)}, u32[]{:S(2)}) copy-start(bf16[2048,32]{0,1:T(8,128)(2,1)} %param.24) | copy-start | bytes 393220
  7.2 32.7 %all-gather.2.cloned.1.call-start = ((), (), s32[]{:S(2)}) async-start(), calls=%async_computation.3 | async-start | bytes 2433024 | tf_op jit(solution)/shard_map/all_gather | solution.py:444
  11.8 24.8 %collective-permute-start = (bf16[512,256]{1,0:T(8,128)(2,1)}, bf16[512,256]{1,0:T(8,128)(2,1)S(1)}, u32[]{:S(2)}, u32[]{:S(2)}) collective-permute-start(bf16[512,256]{1,0:T(8,128)(2,1)} %q0.1), channel_id=1, source_target_pairs={{32,0},{36,4},{40,8},{44,12},{48,16},{52,20},{56,24},{60,28},{64,3... | collective-permute-start | bytes 786440 | tf_op jit(solution)/shard_map/ppermute | solution.py:450
  13.1 24.2 %collective-permute-start.1 = (bf16[512,256]{1,0:T(8,128)(2,1)}, bf16[512,256]{1,0:T(8,128)(2,1)S(1)}, u32[]{:S(2)}, u32[]{:S(2)}) collective-permute-start(bf16[512,256]{1,0:T(8,128)(2,1)} %q0.1), channel_id=1, source_target_pairs={{64,0},{68,4},{72,8},{76,12},{80,16},{84,20},{88,24},{92,28},{96,3... | collective-permute-start | bytes 786440 | tf_op jit(solution)/shard_map/ppermute | solution.py:450
  14.4 22.9 %collective-permute-start.2 = (bf16[512,256]{1,0:T(8,128)(2,1)}, bf16[512,256]{1,0:T(8,128)(2,1)S(1)}, u32[]{:S(2)}, u32[]{:S(2)}) collective-permute-start(bf16[512,256]{1,0:T(8,128)(2,1)} %q0.1), channel_id=1, source_target_pairs={{96,0},{100,4},{104,8},{108,12},{112,16},{116,20},{120,24},{124,28... | collective-permute-start | bytes 786440 | tf_op jit(solution)/shard_map/ppermute | solution.py:450
  15.7 50.5 %collective-permute-start.10 = (bf16[2048,256]{1,0:T(8,128)(2,1)}, bf16[2048,256]{1,0:T(8,128)(2,1)}, u32[]{:S(2)}, u32[]{:S(2)}) collective-permute-start(bf16[2048,256]{1,0:T(8,128)(2,1)} %bitcast.47), channel_id=1, source_target_pairs={{0,3},{1,0},{2,1},{3,2},{4,7},{5,4},{6,5},{7,6},{8,11},{9,8},{10,9... | collective-permute-start | bytes 3145736 | tf_op jit(solution)/shard_map/ppermute | solution.py:394
  25.5 115.3 %all-to-all-start = ((bf16[32,16,2048]{2,1,0:T(8,128)(2,1)}), bf16[32,16,2048]{2,1,0:T(8,128)(2,1)S(1)}, u32[]{:S(2)}, u32[]{:S(2)}) async-start(bf16[32,16,2048]{2,1,0:T(8,128)(2,1)} %bitcast.12), calls=%async_computation.1 | async-start | bytes 4194304 | tf_op jit(solution)/shard_map/all_to_all | solution.py:475
  35.8 183.3 %reduce-scatter.2.cloned.1.call-start = ((), (), s32[]{:S(2)}) async-start(), calls=%async_computation.4 | async-start | bytes 2621440 | tf_op jit(solution)/shard_map/reduce_scatter | solution.py:491
  35.8 51.4 %collective-permute-start.6 = (bf16[2048,256]{1,0:T(8,128)(2,1)}, bf16[2048,256]{1,0:T(8,128)(2,1)}, u32[]{:S(2)}, u32[]{:S(2)}) collective-permute-start(bf16[2048,256]{1,0:T(8,128)(2,1)} %bitcast.44), channel_id=1, source_target_pairs={{0,1},{1,2},{2,3},{3,0},{4,5},{5,6},{6,7},{7,4},{8,9},{9,10},{10,1... | collective-permute-start | bytes 3145736 | tf_op jit(solution)/shard_map/ppermute | solution.py:394
  36.6 3.3 %copy-start.7 = (bf16[512,256]{1,0:T(8,128)(2,1)}, bf16[512,256]{1,0:T(8,128)(2,1)S(1)}, u32[]{:S(2)}) copy-start(bf16[512,256]{1,0:T(8,128)(2,1)S(1)} %collective-permute-done.q1) | copy-start | bytes 786436
  36.6 51.6 %collective-permute-start.8 = (bf16[256,2048]{1,0:T(8,128)(2,1)}, bf16[256,2048]{1,0:T(8,128)(2,1)}, u32[]{:S(2)}, u32[]{:S(2)}) collective-permute-start(bf16[256,2048]{1,0:T(8,128)(2,1)} %bitcast.50), channel_id=1, source_target_pairs={{0,1},{1,2},{2,3},{3,0},{4,5},{5,6},{6,7},{7,4},{8,9},{9,10},{10,1... | collective-permute-start | bytes 3145736 | tf_op jit(solution)/shard_map/ppermute | solution.py:394
  37.3 2.5 %copy-start.8 = (bf16[512,256]{1,0:T(8,128)(2,1)}, bf16[512,256]{1,0:T(8,128)(2,1)S(1)}, u32[]{:S(2)}) copy-start(bf16[512,256]{1,0:T(8,128)(2,1)S(1)} %collective-permute-done.1.q2) | copy-start | bytes 786436
  37.3 2.5 %copy-start.9 = (bf16[512,256]{1,0:T(8,128)(2,1)}, bf16[512,256]{1,0:T(8,128)(2,1)S(1)}, u32[]{:S(2)}) copy-start(bf16[512,256]{1,0:T(8,128)(2,1)S(1)} %collective-permute-done.2.q3) | copy-start | bytes 786436
  63.6 8.6 %collective-permute-start.3 = (bf16[272,512]{1,0:T(8,128)(2,1)}, bf16[272,512]{1,0:T(8,128)(2,1)S(1)}, u32[]{:S(2)}, u32[]{:S(2)}) collective-permute-start(bf16[272,512]{1,0:T(8,128)(2,1)} %get-tuple-element.7), channel_id=1, source_target_pairs={{0,32},{4,36},{8,40},{12,44},{16,48},{20,52},{24,56},{28,60},{32,6... | collective-permute-start | bytes 835592 | tf_op jit(solution)/shard_map/ppermute | solution.py:455
  65.0 12.8 %collective-permute-start.4 = (bf16[272,512]{1,0:T(8,128)(2,1)}, bf16[272,512]{1,0:T(8,128)(2,1)S(1)}, u32[]{:S(2)}, u32[]{:S(2)}) collective-permute-start(bf16[272,512]{1,0:T(8,128)(2,1)} %get-tuple-element.8), channel_id=1, source_target_pairs={{0,64},{4,68},{8,72},{12,76},{16,80},{20,84},{24,88},{28,92},{32,9... | collective-permute-start | bytes 835592 | tf_op jit(solution)/shard_map/ppermute | solution.py:455
  66.3 15.8 %collective-permute-start.5 = (bf16[272,512]{1,0:T(8,128)(2,1)}, bf16[272,512]{1,0:T(8,128)(2,1)}, u32[]{:S(2)}, u32[]{:S(2)}) collective-permute-start(bf16[272,512]{1,0:T(8,128)(2,1)} %get-tuple-element.9), channel_id=1, source_target_pairs={{0,96},{4,100},{8,104},{12,108},{16,112},{20,116},{24,120},{28,124... | collective-permute-start | bytes 835592 | tf_op jit(solution)/shard_map/ppermute | solution.py:455
  72.3 10.9 %copy-start.3 = (bf16[272,512]{1,0:T(8,128)(2,1)}, bf16[272,512]{1,0:T(8,128)(2,1)S(1)}, u32[]{:S(2)}) copy-start(bf16[272,512]{1,0:T(8,128)(2,1)S(1)} %collective-permute-done.3.p1) | copy-start | bytes 835588
  72.3 30.9 %collective-permute-start.11 = (bf16[256,2048]{1,0:T(8,128)(2,1)}, bf16[256,2048]{1,0:T(8,128)(2,1)}, u32[]{:S(2)}, u32[]{:S(2)}) collective-permute-start(bf16[256,2048]{1,0:T(8,128)(2,1)} %bitcast.51), channel_id=1, source_target_pairs={{0,3},{1,0},{2,1},{3,2},{4,7},{5,4},{6,5},{7,6},{8,11},{9,8},{10,9... | collective-permute-start | bytes 3145736 | tf_op jit(solution)/shard_map/ppermute | solution.py:394
  77.8 5.4 %copy-start.4 = (bf16[272,512]{1,0:T(8,128)(2,1)}, bf16[272,512]{1,0:T(8,128)(2,1)S(1)}, u32[]{:S(2)}) copy-start(bf16[272,512]{1,0:T(8,128)(2,1)S(1)} %collective-permute-done.4.p2) | copy-start | bytes 835588
  77.8 35.8 %collective-permute-start.7 = (bf16[2048,256]{1,0:T(8,128)(2,1)}, bf16[2048,256]{1,0:T(8,128)(2,1)}, u32[]{:S(2)}, u32[]{:S(2)}) collective-permute-start(bf16[2048,256]{1,0:T(8,128)(2,1)} %bitcast.48), channel_id=1, source_target_pairs={{0,1},{1,2},{2,3},{3,0},{4,5},{5,6},{6,7},{7,4},{8,9},{9,10},{10,1... | collective-permute-start | bytes 3145736 | tf_op jit(solution)/shard_map/ppermute | solution.py:394
  82.1 58.8 %collective-permute-start.9 = (bf16[2048,256]{1,0:T(8,128)(2,1)}, bf16[2048,256]{1,0:T(8,128)(2,1)}, u32[]{:S(2)}, u32[]{:S(2)}) collective-permute-start(bf16[2048,256]{1,0:T(8,128)(2,1)} %bitcast.45), channel_id=1, source_target_pairs={{0,3},{1,0},{2,1},{3,2},{4,7},{5,4},{6,5},{7,6},{8,11},{9,8},{10,9... | collective-permute-start | bytes 3145736 | tf_op jit(solution)/shard_map/ppermute | solution.py:394
  87.2 85.6 %collective-permute-start.12 = (bf16[2048,256]{1,0:T(8,128)(2,1)}, bf16[2048,256]{1,0:T(8,128)(2,1)}, u32[]{:S(2)}, u32[]{:S(2)}) collective-permute-start(bf16[2048,256]{1,0:T(8,128)(2,1)} %collective-permute-done.6.refs_3_), channel_id=1, source_target_pairs={{0,1},{1,2},{2,3},{3,0},{4,5},{5,6},{6,7},{7,4},{8,9},{9,10},{10,1... | collective-permute-start | bytes 3145736 | tf_op jit(solution)/shard_map/ppermute | solution.py:394
  88.1 84.6 %collective-permute-start.13 = (bf16[2048,256]{1,0:T(8,128)(2,1)}, bf16[2048,256]{1,0:T(8,128)(2,1)}, u32[]{:S(2)}, u32[]{:S(2)}) collective-permute-start(bf16[2048,256]{1,0:T(8,128)(2,1)} %collective-permute-done.10.refs_7_), channel_id=1, source_target_pairs={{0,3},{1,0},{2,1},{3,2},{4,7},{5,4},{6,5},{7,6},{8,11},{9,8},{10,9... | collective-permute-start | bytes 3145736 | tf_op jit(solution)/shard_map/ppermute | solution.py:394
  103.1 55.0 %collective-permute-start.14 = (bf16[128,2048]{1,0:T(8,128)(2,1)}, bf16[128,2048]{1,0:T(8,128)(2,1)S(1)}, u32[]{:S(2)}, u32[]{:S(2)}) collective-permute-start(bf16[128,2048]{1,0:T(8,128)(2,1)} %slice.35), channel_id=1, source_target_pairs={{0,1},{1,2},{2,3},{3,0},{4,5},{5,6},{6,7},{7,4},{8,9},{9,10},{10,1... | collective-permute-start | bytes 1572872 | tf_op jit(solution)/shard_map/ppermute | solution.py:394
  113.6 59.2 %collective-permute-start.15 = (bf16[128,2048]{1,0:T(8,128)(2,1)}, bf16[128,2048]{1,0:T(8,128)(2,1)}, u32[]{:S(2)}, u32[]{:S(2)}) collective-permute-start(bf16[128,2048]{1,0:T(8,128)(2,1)} %slice.36), channel_id=1, source_target_pairs={{0,3},{1,0},{2,1},{3,2},{4,7},{5,4},{6,5},{7,6},{8,11},{9,8},{10,9... | collective-permute-start | bytes 1572872 | tf_op jit(solution)/shard_map/ppermute | solution.py:394
  140.8 1.3 copy-start.1
  158.1 14.6 %copy-start.2 = (bf16[128,2048]{1,0:T(8,128)(2,1)}, bf16[128,2048]{1,0:T(8,128)(2,1)S(1)}, u32[]{:S(2)}) copy-start(bf16[128,2048]{1,0:T(8,128)(2,1)S(1)} %collective-permute-done.14.top_half) | copy-start | bytes 1572868
  178.3 9.3 %copy-start.5 = (bf16[2048,4]{0,1:T(4,128)(2,1)S(1)}, bf16[2048,4]{0,1:T(4,128)(2,1)}, u32[]{:S(2)}) copy-start(bf16[2048,4]{0,1:T(4,128)(2,1)} %param.23) | copy-start | bytes 49156
  178.3 39.0 %all-to-all-start.1 = ((bf16[32,16,2048]{2,1,0:T(8,128)(2,1)}), bf16[32,16,2048]{2,1,0:T(8,128)(2,1)S(1)}, u32[]{:S(2)}, u32[]{:S(2)}) async-start(bf16[32,16,2048]{2,1,0:T(8,128)(2,1)} %bitcast.38), calls=%async_computation.2 | async-start | bytes 4194304 | tf_op jit(solution)/shard_map/all_to_all | solution.py:487
  217.8 2.6 %copy-start.6 = (f32[2048]{0:T(1024)S(1)}, f32[2048]{0:T(1024)}, u32[]{:S(2)}) copy-start(f32[2048]{0:T(1024)} %param.20) | copy-start | bytes 24580
Sparse Core Ops, SparseCore 0:
  11.9 27.8 all-gather.1
  87.3 50.6 reduce-scatter.1

commit v4 on v3

--- a/solution.py
+++ b/solution.py
@@ -273,35 +273,38 @@
 
 
 def first_kernel(x_hbm, *refs):
-    count = (len(refs) - 7) // 3
-    weights, (out_hbm, x_ref, both, down, hidden, out, sems) = refs[: 3 * count], refs[3 * count :]
+    count = (len(refs) - 7) // 4
+    weights, (out_hbm, x_ref, both, down, hidden, out, sems) = refs[: 4 * count], refs[4 * count :]
     ff = down.shape[0] // count
-    rows = pltpu.make_async_copy(x_hbm, x_ref, sems.at[3 * count])
+    rows = pltpu.make_async_copy(x_hbm, x_ref, sems.at[4 * count])
     rows.start()
     copies = []
     for q in range(count):
-        gate, up, low = weights[3 * q : 3 * q + 3]
+        gate, up, upper, lower = weights[4 * q : 4 * q + 4]
+        middle = q * ff + ff // 2
         pairs = (
             (gate, both.at[q, :, :ff]),
             (up, both.at[q, :, ff:]),
-            (low, down.at[q * ff : (q + 1) * ff, :]),
+            (upper, down.at[q * ff : middle, :]),
+            (lower, down.at[middle : (q + 1) * ff, :]),
         )
         for k, (src, dst) in enumerate(pairs):
-            copies.append(pltpu.make_async_copy(src, dst, sems.at[3 * q + k]))
+            copies.append(pltpu.make_async_copy(src, dst, sems.at[4 * q + k]))
     for c in copies:
         c.start()
     rows.wait()
     for q in range(count):
-        copies[3 * q].wait()
-        copies[3 * q + 1].wait()
+        copies[4 * q].wait()
+        copies[4 * q + 1].wait()
         expert_hidden(x_ref, both.at[q], hidden, q * ff)
     for q in range(count):
-        copies[3 * q + 2].wait()
+        copies[4 * q + 2].wait()
+        copies[4 * q + 3].wait()
     stores = []
     for n, cols in enumerate(column_tiles(out.shape[1])):
         out[:, cols] = jnp.dot(hidden[...], down[:, cols], preferred_element_type=jnp.float32)
         stores.append(
-            pltpu.make_async_copy(out.at[:, cols], out_hbm.at[:, cols], sems.at[3 * count + 1 + n])
+            pltpu.make_async_copy(out.at[:, cols], out_hbm.at[:, cols], sems.at[4 * count + 1 + n])
         )
         stores[-1].start()
     for c in stores:
@@ -310,7 +313,7 @@
 
 def first_parts(x, weights):
     rows, width = x.shape
-    count, ff = len(weights) // 3, weights[0].shape[1]
+    count, ff = len(weights) // 4, weights[0].shape[1]
     return pl.pallas_call(
         first_kernel,
         out_shape=jax.ShapeDtypeStruct((rows, width), jnp.float32),
@@ -322,7 +325,7 @@
             pltpu.VMEM((count * ff, width), jnp.bfloat16),
             pltpu.VMEM((rows, count * ff), jnp.bfloat16),
             pltpu.VMEM((rows, width), jnp.float32),
-            pltpu.SemaphoreType.DMA((3 * count + 1 + len(column_tiles(width)),)),
+            pltpu.SemaphoreType.DMA((4 * count + 1 + len(column_tiles(width)),)),
         ],
         cost_estimate=pl.CostEstimate(
             flops=count * 6 * rows * width * ff,
@@ -431,12 +434,14 @@
 
     gate, up, down = expert_gate[0], expert_up[0], expert_down[0]
     half = gate.shape[1] // 2
-    from_left = [shift(w, 1) for w in (gate, down, up)]
-    from_right = [shift(w, -1) for w in (up, down, gate)]
-    far_gate = shift(from_left[0], 1)
-    far_up = shift(from_right[0], -1)
-    far_top = shift(from_left[1][:half], 1)
-    far_bottom = shift(from_right[1][half:], -1)
+    upper, lower = down[:half], down[half:]
+    own = {"gate": gate, "upper": upper, "up": up, "lower": lower}
+    first, second = ("gate", "upper"), ("up", "lower")
+    left = {n: shift(own[n], 1) for n in first + second}
+    right = {n: shift(own[n], -1) for n in second + first}
+    far = {n: shift(left[n], 1) for n in first}
+    far |= {n: shift(right[n], -1) for n in second}
+    names = ("gate", "up", "upper", "lower")
 
     running = jnp.cumsum(jax.nn.log_sigmoid(forget_logit), axis=1)
     packed = pack(key_rows, value_rows, running)
@@ -475,18 +480,13 @@
     arrived = lax.all_to_all(outgoing, "ep", split_axis=0, concat_axis=0, tiled=True)
     arrived = arrived.reshape(slots, width_model)
 
-    part = first_parts(
-        arrived,
-        (gate, up, down)
-        + (from_left[0], from_left[2], from_left[1])
-        + (from_right[2], from_right[0], from_right[1]),
-    )
+    part = first_parts(arrived, [q[n] for q in (own, left, right) for n in names])
+    results = last_part(arrived, part, *[far[n] for n in names])
+    results, told[0] = lax.optimization_barrier((results, told[0]))
     mixer_term = merge(place, told, out_weight)
-    results = last_part(arrived, part, far_gate, far_up, far_top, far_bottom)
     results = results.reshape(experts, capacity, width_model)
-    returned = lax.all_to_all(results, "ep", split_axis=0, concat_axis=0, tiled=True).reshape(
-        slots, width_model
-    )
+    returned = lax.all_to_all(results, "ep", split_axis=0, concat_axis=0, tiled=True)
+    returned = returned.reshape(slots, width_model)
 
     mixer_summed = lax.psum_scatter(mixer_term, "tp", scatter_dimension=0, tiled=True)
     mixer_out = rms_scale(mixer_summed, out_gain).astype(jnp.bfloat16)

time: 231 us -> 217 us (0.939)
  waiting for transfers between devices: 103 us -> 90 us
  other arithmetic: 11.9 us -> 8.89 us
  starting transfers between devices: 46.9 us -> 49.3 us
    ppermute x10 -> x12, waiting for transfers between devices: 66.9 us -> 60.6 us  [shift(): return lax.ppermute(x, 'tp', [(i, (i + by) % count) for i in range(count)])]
    ppermute x3, starting transfers between devices: 4.61 us -> 9.52 us  [inner(): told.append(lax.ppermute(answers[d], 'ep', pairs))]
    ppermute x3, waiting for transfers between devices: 4.15 us -> 0.01 us  [inner(): told.append(lax.ppermute(answers[d], 'ep', pairs))]
    all_gather x1, waiting for transfers between devices: 2.51 us -> 0.01 us  [inner(): lax.all_gather(packed, 'ep', axis=0, tiled=True, axis_index_groups=planes)]
    ppermute x10 -> x12, starting transfers between devices: 19.2 us -> 17 us  [shift(): return lax.ppermute(x, 'tp', [(i, (i + by) % count) for i in range(count)])]
  transfers between devices with their start and end apart: 20 -> 22, of which waited for: 9 -> 5; matrix products, arithmetic and copies ran while one was open for 6% -> 6% of each run, Pallas kernels for 18% -> 18%
where the time goes in v4:
time: 217 us; the launch traced here: 216 us
  waiting for transfers between devices  90 us (41%)
  starting transfers between devices  49.3 us (23%)
  Pallas kernels  42.1 us (19%)
  between operations  14.4 us (7%)
  other arithmetic  8.89 us (4%)
  local copies, waits for them, and re-layouts  6.92 us (3%)
  matrix products  4.54 us (2%)
    ppermute x12, waiting for transfers between devices, shift(): return lax.ppermute(x, 'tp', [(i, (i + by) % count) for i in range(count)])  60.6 us
    all_to_all x1, waiting for transfers between devices, inner(): lax.all_to_all(results, 'ep', split_axis=0, concat_axis=0, tiled=True)  29.4 us
    pallas_call x1, Pallas kernels, attend(): pl.pallas_call(attend_kernel, out_shape=[jax.ShapeDtypeStruct((2 * DH + 1...  23.8 us
    ppermute x12, starting transfers between devices, shift(): return lax.ppermute(x, 'tp', [(i, (i + by) % count) for i in range(count)])  17 us
    all_to_all x1, starting transfers between devices, inner(): lax.all_to_all(outgoing, 'ep', split_axis=0, concat_axis=0, tiled=True)  11.6 us
    ppermute x3, starting transfers between devices, inner(): told.append(lax.ppermute(answers[d], 'ep', pairs))  9.52 us
    pallas_call x1, Pallas kernels, first_parts(): pl.pallas_call(first_kernel, out_shape=jax.ShapeDtypeStruct((rows, width)...  8.95 us
    all_to_all x1, starting transfers between devices, inner(): lax.all_to_all(results, 'ep', split_axis=0, concat_axis=0, tiled=True)  7.09 us
  transfers between devices with their start and end apart: 22, of which 5 were waited for; matrix products, arithmetic and copies ran while one was open for 6% of the time, Pallas kernels for 18%

profile of v4, /device:TPU:0, one launch (start us, length us, event | category | flops | bytes accessed | tf_op | source)
XLA Modules:
  0.0 216.2 jit_solution(17224439898565029194)
XLA Ops:
  7.3 1.4 collective-permute-start.12
  8.7 1.3 collective-permute-start.13
  10.0 1.3 collective-permute-start.14
  14.2 1.6 pad_maximum_fusion
  15.9 2.1 slice_bitcast_fusion
  17.9 1.6 collective-permute-start.2
  19.7 1.3 broadcast_multiply_fusion
  22.1 2.0 convolution_convert_fusion
  24.1 11.6 %all-to-all-start = ((bf16[32,16,2048]{2,1,0:T(8,128)(2,1)}), bf16[32,16,2048]{2,1,0:T(8,128)(2,1)S(1)}, u32[]{:S(2)}, u32[]{:S(2)}) async-start(bf16[32,16,2048]{2,1,0:T(8,128)(2,1)} %bitcast.4), calls=%async_computation | async-start | bytes 4194304 | tf_op jit(solution)/shard_map/all_to_all | solution.py:480
  35.8 1.8 collective-permute-start.7
  37.9 3.0 %collective-permute-start.5 = (bf16[2048,256]{1,0:T(8,128)(2,1)}, bf16[2048,256]{1,0:T(8,128)(2,1)}, u32[]{:S(2)}, u32[]{:S(2)}) collective-permute-start(bf16[2048,256]{1,0:T(8,128)(2,1)} %bitcast.50), channel_id=1, source_target_pairs={{0,3},{1,0},{2,1},{3,2},{4,7},{5,4},{6,5},{7,6},{8,11},{9,8},{10,9... | collective-permute-start | bytes 3145736 | tf_op jit(solution)/shard_map/ppermute | solution.py:397
  41.4 9.2 %collective-permute-done.7.refs_11_ = bf16[128,2048]{1,0:T(8,128)(2,1)S(1)} collective-permute-done((bf16[128,2048]{1,0:T(8,128)(2,1)S(1)}, bf16[128,2048]{1,0:T(8,128)(2,1)S(1)}, u32[]{:S(2)}, u32[]{:S(2)}) %collective-permute-start.7) | collective-permute-done | bytes 524320 | tf_op jit(solution)/shard_map/ppermute | solution.py:397
  50.6 3.0 %collective-permute-start.6 = (bf16[128,2048]{1,0:T(8,128)(2,1)}, bf16[128,2048]{1,0:T(8,128)(2,1)}, u32[]{:S(2)}, u32[]{:S(2)}) collective-permute-start(bf16[128,2048]{1,0:T(8,128)(2,1)} %get-tuple-element.19.refs_2_), channel_id=1, source_target_pairs={{0,3},{1,0},{2,1},{3,2},{4,7},{5,4},{6,5},{7,6},{8,11},{9,8},{10,9... | collective-permute-start | bytes 1572872 | tf_op jit(solution)/shard_map/ppermute | solution.py:397
  53.6 44.2 %collective-permute-done.3.refs_7_ = bf16[128,2048]{1,0:T(8,128)(2,1)S(1)} collective-permute-done((bf16[128,2048]{1,0:T(8,128)(2,1)S(1)}, bf16[128,2048]{1,0:T(8,128)(2,1)S(1)}, u32[]{:S(2)}, u32[]{:S(2)}) %collective-permute-start.3) | collective-permute-done | bytes 524320 | tf_op jit(solution)/shard_map/ppermute | solution.py:397
  99.5 1.7 collective-permute-start.10
  101.2 1.5 collective-permute-start.11
  103.2 2.8 %collective-permute-start.9 = (bf16[2048,256]{1,0:T(8,128)(2,1)}, bf16[2048,256]{1,0:T(8,128)(2,1)}, u32[]{:S(2)}, u32[]{:S(2)}) collective-permute-start(bf16[2048,256]{1,0:T(8,128)(2,1)} %collective-permute-done.5.refs_9_), channel_id=1, source_target_pairs={{0,3},{1,0},{2,1},{3,2},{4,7},{5,4},{6,5},{7,6},{8,11},{9,8},{10,9... | collective-permute-start | bytes 3145736 | tf_op jit(solution)/shard_map/ppermute | solution.py:397
  106.0 23.8 %shard_map.160 = (bf16[272,512]{1,0:T(8,128)(2,1)}, bf16[272,512]{1,0:T(8,128)(2,1)}, bf16[272,512]{1,0:T(8,128)(2,1)}, bf16[272,512]{1,0:T(8,128)(2,1)}) custom-call(s32[2]{0:T(128)} %pad_add_fusion.pos_ref, bf16[512,256]{1,0:T(8,128)(2,1)} %q0.1, bf16[512,256]{1,0:T(8,128)(2,1)} %copy-done.19, bf16[512,256]{1,0:T(8,128)(2,1)} %collective-permute-done.13.q2, ...), custom_call_target="tpu_custom_call" | custom-call | flops 8999999488 | bytes 4000000 | tf_op jit(solution)/shard_map/pallas_call | solution.py:170
  129.8 1.3 collective-permute-start.15
  131.1 2.7 %collective-permute-start.16 = (bf16[272,512]{1,0:T(8,128)(2,1)}, bf16[272,512]{1,0:T(8,128)(2,1)}, u32[]{:S(2)}, u32[]{:S(2)}) collective-permute-start(bf16[272,512]{1,0:T(8,128)(2,1)} %get-tuple-element.11), channel_id=1, source_target_pairs={{0,64},{4,68},{8,72},{12,76},{16,80},{20,84},{24,88},{28,92},{32,9... | collective-permute-start | bytes 835592 | tf_op jit(solution)/shard_map/ppermute | solution.py:460
  133.8 2.3 %collective-permute-done.11.bottom_half = bf16[128,2048]{1,0:T(8,128)(2,1)} collective-permute-done((bf16[128,2048]{1,0:T(8,128)(2,1)}, bf16[128,2048]{1,0:T(8,128)(2,1)}, u32[]{:S(2)}, u32[]{:S(2)}) %collective-permute-start.11) | collective-permute-done | bytes 524320 | tf_op jit(solution)/shard_map/ppermute | solution.py:397
  136.2 5.5 %collective-permute-start.17 = (bf16[272,512]{1,0:T(8,128)(2,1)}, bf16[272,512]{1,0:T(8,128)(2,1)}, u32[]{:S(2)}, u32[]{:S(2)}) collective-permute-start(bf16[272,512]{1,0:T(8,128)(2,1)} %get-tuple-element.12), channel_id=1, source_target_pairs={{0,96},{4,100},{8,104},{12,108},{16,112},{20,116},{24,120},{28,124... | collective-permute-start | bytes 835592 | tf_op jit(solution)/shard_map/ppermute | solution.py:460
  141.7 1.4 copy-done.1
  143.0 8.9 %shard_map.158.part_hbm = f32[512,2048]{1,0:T(8,128)} custom-call(bf16[512,2048]{1,0:T(8,128)(2,1)} %bitcast.39, bf16[2048,256]{1,0:T(8,128)(2,1)} %bitcast.49, bf16[2048,256]{1,0:T(8,128)(2,1)} %bitcast.52, bf16[128,2048]{1,0:T(8,128)(2,1)} %get-tuple-element.19.refs_2_, bf16[128,2048]{1,0:T(8,128)(2,1)} %copy-done.4, ...), custom_call_target="tpu_custom_call" | custom-call | flops 4831838208 | bytes 9437184 | tf_op jit(solution)/shard_map/pallas_call | solution.py:317
  152.0 4.8 %collective-permute-done.9.up = bf16[2048,256]{1,0:T(8,128)(2,1)} collective-permute-done((bf16[2048,256]{1,0:T(8,128)(2,1)}, bf16[2048,256]{1,0:T(8,128)(2,1)}, u32[]{:S(2)}, u32[]{:S(2)}) %collective-permute-start.9) | collective-permute-done | bytes 1048608 | tf_op jit(solution)/shard_map/ppermute | solution.py:397
  156.8 5.5 %shard_map.159 = bf16[512,2048]{1,0:T(8,128)(2,1)} custom-call(bf16[512,2048]{1,0:T(8,128)(2,1)} %bitcast.40, f32[512,2048]{1,0:T(8,128)} %shard_map.158.part_hbm, bf16[2048,256]{1,0:T(8,128)(2,1)} %collective-permute-done.8.gate, bf16[2048,256]{1,0:T(8,128)(2,1)} %collective-permute-done.9.up, bf16[128,2048]{1,0:T(8,128)(2,1)} %copy-done.2, ...), custom_call_target="tpu_custom_call" | custom-call | flops 1610612736 | bytes 3145728 | tf_op jit(solution)/shard_map/pallas_call | solution.py:375
  163.1 3.9 %shard_map.161 = bf16[512,2048]{1,0:T(8,128)(2,1)} custom-call(s32[2]{0:T(128)} %pad_add_fusion.pos_ref, bf16[272,512]{1,0:T(8,128)(2,1)} %get-tuple-element.9.p0, bf16[272,512]{1,0:T(8,128)(2,1)} %copy-done.5, bf16[272,512]{1,0:T(8,128)(2,1)} %collective-permute-done.16.p2, bf16[272,512]{1,0:T(8,128)(2,1)} %collective-permute-done.17.p3, ...), custom_call_target="tpu_custom_call" | custom-call | flops 536870912 | bytes 4000000 | tf_op jit(solution)/shard_map/pallas_call | solution.py:237
  167.0 7.1 %all-to-all-start.1 = ((bf16[32,16,2048]{2,1,0:T(8,128)(2,1)}), bf16[32,16,2048]{2,1,0:T(8,128)(2,1)S(1)}, u32[]{:S(2)}, u32[]{:S(2)}) async-start(bf16[32,16,2048]{2,1,0:T(8,128)(2,1)} %bitcast.41), calls=%async_computation.2 | async-start | bytes 4194304 | tf_op jit(solution)/shard_map/all_to_all | solution.py:488
  174.8 29.4 %all-to-all-done.1 = bf16[32,16,2048]{2,1,0:T(8,128)(2,1)S(1)} async-done(((bf16[32,16,2048]{2,1,0:T(8,128)(2,1)}), bf16[32,16,2048]{2,1,0:T(8,128)(2,1)S(1)}, u32[]{:S(2)}, u32[]{:S(2)}) %all-to-all-start.1) | async-done | bytes 2097184 | tf_op jit(solution)/shard_map/all_to_all | solution.py:488
  204.7 1.3 fusion
  206.1 1.2 fusion.4
  207.3 2.0 fusion.6
  (99 shorter events, 9.2 us)
Async XLA Ops:
  7.2 167.0 %copy-start = (bf16[2048,32]{0,1:T(8,128)(2,1)S(1)}, bf16[2048,32]{0,1:T(8,128)(2,1)}, u32[]{:S(2)}) copy-start(bf16[2048,32]{0,1:T(8,128)(2,1)} %param.24) | copy-start | bytes 393220
  7.2 12.4 %copy-start.3 = (bf16[512,2048]{1,0:T(8,128)(2,1)S(1)}, bf16[512,2048]{1,0:T(8,128)(2,1)}, u32[]{:S(2)}) copy-start(bf16[512,2048]{1,0:T(8,128)(2,1)} %param.21) | copy-start | bytes 6291460
  7.2 13.8 %copy-start.16 = (s32[512,2]{0,1:T(2,128)S(1)}, s32[512,2]{0,1:T(2,128)}, u32[]{:S(2)}) copy-start(s32[512,2]{0,1:T(2,128)} %param.26) | copy-start | bytes 12292
  7.2 14.4 %copy-start.9 = (f32[2048]{0:T(1024)S(1)}, f32[2048]{0:T(1024)}, u32[]{:S(2)}) copy-start(f32[2048]{0:T(1024)} %param.22) | copy-start | bytes 24580
  7.2 98.8 %all-gather.2.cloned.1.call-start = ((), (), s32[]{:S(2)}) async-start(), calls=%async_computation.3 | async-start | bytes 2433024 | tf_op jit(solution)/shard_map/all_gather | solution.py:449
  7.3 30.3 %collective-permute-start.12 = (bf16[512,256]{1,0:T(8,128)(2,1)}, bf16[512,256]{1,0:T(8,128)(2,1)S(1)}, u32[]{:S(2)}, u32[]{:S(2)}) collective-permute-start(bf16[512,256]{1,0:T(8,128)(2,1)} %q0.1), channel_id=1, source_target_pairs={{32,0},{36,4},{40,8},{44,12},{48,16},{52,20},{56,24},{60,28},{64,3... | collective-permute-start | bytes 786440 | tf_op jit(solution)/shard_map/ppermute | solution.py:455
  8.7 29.2 %collective-permute-start.13 = (bf16[512,256]{1,0:T(8,128)(2,1)}, bf16[512,256]{1,0:T(8,128)(2,1)}, u32[]{:S(2)}, u32[]{:S(2)}) collective-permute-start(bf16[512,256]{1,0:T(8,128)(2,1)} %q0.1), channel_id=1, source_target_pairs={{64,0},{68,4},{72,8},{76,12},{80,16},{84,20},{88,24},{92,28},{96,3... | collective-permute-start | bytes 786440 | tf_op jit(solution)/shard_map/ppermute | solution.py:455
  10.0 30.8 %collective-permute-start.14 = (bf16[512,256]{1,0:T(8,128)(2,1)}, bf16[512,256]{1,0:T(8,128)(2,1)}, u32[]{:S(2)}, u32[]{:S(2)}) collective-permute-start(bf16[512,256]{1,0:T(8,128)(2,1)} %q0.1), channel_id=1, source_target_pairs={{96,0},{100,4},{104,8},{108,12},{112,16},{116,20},{120,24},{124,28... | collective-permute-start | bytes 786440 | tf_op jit(solution)/shard_map/ppermute | solution.py:455
  17.9 22.9 %copy-start.4 = (bf16[128,2048]{1,0:T(8,128)(2,1)}, bf16[128,2048]{1,0:T(8,128)(2,1)S(1)}, u32[]{:S(2)}) copy-start(bf16[128,2048]{1,0:T(8,128)(2,1)S(1)} %get-tuple-element.18.refs_3_) | copy-start | bytes 1572868
  17.9 22.9 %collective-permute-start.2 = (bf16[128,2048]{1,0:T(8,128)(2,1)}, bf16[128,2048]{1,0:T(8,128)(2,1)}, u32[]{:S(2)}, u32[]{:S(2)}) collective-permute-start(bf16[128,2048]{1,0:T(8,128)(2,1)} %get-tuple-element.19.refs_2_), channel_id=1, source_target_pairs={{0,1},{1,2},{2,3},{3,0},{4,5},{5,6},{6,7},{7,4},{8,9},{9,10},{10,1... | collective-permute-start | bytes 1572872 | tf_op jit(solution)/shard_map/ppermute | solution.py:397
  24.1 117.6 %all-to-all-start = ((bf16[32,16,2048]{2,1,0:T(8,128)(2,1)}), bf16[32,16,2048]{2,1,0:T(8,128)(2,1)S(1)}, u32[]{:S(2)}, u32[]{:S(2)}) async-start(bf16[32,16,2048]{2,1,0:T(8,128)(2,1)} %bitcast.4), calls=%async_computation | async-start | bytes 4194304 | tf_op jit(solution)/shard_map/all_to_all | solution.py:480
  35.7 170.4 %reduce-scatter.2.cloned.1.call-start = ((), (), s32[]{:S(2)}) async-start(), calls=%async_computation.4 | async-start | bytes 2621440 | tf_op jit(solution)/shard_map/reduce_scatter | solution.py:491
  35.8 14.9 %collective-permute-start.7 = (bf16[128,2048]{1,0:T(8,128)(2,1)S(1)}, bf16[128,2048]{1,0:T(8,128)(2,1)S(1)}, u32[]{:S(2)}, u32[]{:S(2)}) collective-permute-start(bf16[128,2048]{1,0:T(8,128)(2,1)S(1)} %get-tuple-element.18.refs_3_), channel_id=1, source_target_pairs={{0,3},{1,0},{2,1},{3,2},{4,7},{5,4},{6,5},{7,6},{8,11},{9,8},{10,9... | collective-permute-start | bytes 1572872 | tf_op jit(solution)/shard_map/ppermute | solution.py:397
  37.6 68.4 %copy-start.19 = (bf16[512,256]{1,0:T(8,128)(2,1)}, bf16[512,256]{1,0:T(8,128)(2,1)S(1)}, u32[]{:S(2)}) copy-start(bf16[512,256]{1,0:T(8,128)(2,1)S(1)} %collective-permute-done.12.q1) | copy-start | bytes 786436
  37.6 63.6 %collective-permute-start = (bf16[2048,256]{1,0:T(8,128)(2,1)}, bf16[2048,256]{1,0:T(8,128)(2,1)}, u32[]{:S(2)}, u32[]{:S(2)}) collective-permute-start(bf16[2048,256]{1,0:T(8,128)(2,1)} %bitcast.47), channel_id=1, source_target_pairs={{0,1},{1,2},{2,3},{3,0},{4,5},{5,6},{6,7},{7,4},{8,9},{9,10},{10,1... | collective-permute-start | bytes 3145736 | tf_op jit(solution)/shard_map/ppermute | solution.py:397
  37.9 64.9 %collective-permute-start.5 = (bf16[2048,256]{1,0:T(8,128)(2,1)}, bf16[2048,256]{1,0:T(8,128)(2,1)}, u32[]{:S(2)}, u32[]{:S(2)}) collective-permute-start(bf16[2048,256]{1,0:T(8,128)(2,1)} %bitcast.50), channel_id=1, source_target_pairs={{0,3},{1,0},{2,1},{3,2},{4,7},{5,4},{6,5},{7,6},{8,11},{9,8},{10,9... | collective-permute-start | bytes 3145736 | tf_op jit(solution)/shard_map/ppermute | solution.py:397
  40.8 62.4 %collective-permute-start.1 = (bf16[2048,256]{1,0:T(8,128)(2,1)}, bf16[2048,256]{1,0:T(8,128)(2,1)}, u32[]{:S(2)}, u32[]{:S(2)}) collective-permute-start(bf16[2048,256]{1,0:T(8,128)(2,1)} %bitcast.51), channel_id=1, source_target_pairs={{0,1},{1,2},{2,3},{3,0},{4,5},{5,6},{6,7},{7,4},{8,9},{9,10},{10,1... | collective-permute-start | bytes 3145736 | tf_op jit(solution)/shard_map/ppermute | solution.py:397
  40.8 56.9 %collective-permute-start.3 = (bf16[128,2048]{1,0:T(8,128)(2,1)S(1)}, bf16[128,2048]{1,0:T(8,128)(2,1)S(1)}, u32[]{:S(2)}, u32[]{:S(2)}) collective-permute-start(bf16[128,2048]{1,0:T(8,128)(2,1)S(1)} %get-tuple-element.18.refs_3_), channel_id=1, source_target_pairs={{0,1},{1,2},{2,3},{3,0},{4,5},{5,6},{6,7},{7,4},{8,9},{9,10},{10,1... | collective-permute-start | bytes 1572872 | tf_op jit(solution)/shard_map/ppermute | solution.py:397
  50.6 47.1 %copy-start.17 = (bf16[128,2048]{1,0:T(8,128)(2,1)}, bf16[128,2048]{1,0:T(8,128)(2,1)S(1)}, u32[]{:S(2)}) copy-start(bf16[128,2048]{1,0:T(8,128)(2,1)S(1)} %collective-permute-done.7.refs_11_) | copy-start | bytes 1572868
  50.6 48.9 %collective-permute-start.6 = (bf16[128,2048]{1,0:T(8,128)(2,1)}, bf16[128,2048]{1,0:T(8,128)(2,1)}, u32[]{:S(2)}, u32[]{:S(2)}) collective-permute-start(bf16[128,2048]{1,0:T(8,128)(2,1)} %get-tuple-element.19.refs_2_), channel_id=1, source_target_pairs={{0,3},{1,0},{2,1},{3,2},{4,7},{5,4},{6,5},{7,6},{8,11},{9,8},{10,9... | collective-permute-start | bytes 1572872 | tf_op jit(solution)/shard_map/ppermute | solution.py:397
  98.6 31.2 %collective-permute-start.4 = (bf16[2048,256]{1,0:T(8,128)(2,1)}, bf16[2048,256]{1,0:T(8,128)(2,1)}, u32[]{:S(2)}, u32[]{:S(2)}) collective-permute-start(bf16[2048,256]{1,0:T(8,128)(2,1)} %bitcast.48), channel_id=1, source_target_pairs={{0,3},{1,0},{2,1},{3,2},{4,7},{5,4},{6,5},{7,6},{8,11},{9,8},{10,9... | collective-permute-start | bytes 3145736 | tf_op jit(solution)/shard_map/ppermute | solution.py:397
  99.5 31.6 %collective-permute-start.10 = (bf16[128,2048]{1,0:T(8,128)(2,1)}, bf16[128,2048]{1,0:T(8,128)(2,1)S(1)}, u32[]{:S(2)}, u32[]{:S(2)}) collective-permute-start(bf16[128,2048]{1,0:T(8,128)(2,1)} %collective-permute-done.2.refs_6_), channel_id=1, source_target_pairs={{0,1},{1,2},{2,3},{3,0},{4,5},{5,6},{6,7},{7,4},{8,9},{9,10},{10,1... | collective-permute-start | bytes 1572872 | tf_op jit(solution)/shard_map/ppermute | solution.py:397
  101.2 35.0 %collective-permute-start.11 = (bf16[128,2048]{1,0:T(8,128)(2,1)}, bf16[128,2048]{1,0:T(8,128)(2,1)}, u32[]{:S(2)}, u32[]{:S(2)}) collective-permute-start(bf16[128,2048]{1,0:T(8,128)(2,1)} %copy-done.17), channel_id=1, source_target_pairs={{0,3},{1,0},{2,1},{3,2},{4,7},{5,4},{6,5},{7,6},{8,11},{9,8},{10,9... | collective-permute-start | bytes 1572872 | tf_op jit(solution)/shard_map/ppermute | solution.py:397
  102.7 49.3 %collective-permute-start.8 = (bf16[2048,256]{1,0:T(8,128)(2,1)}, bf16[2048,256]{1,0:T(8,128)(2,1)}, u32[]{:S(2)}, u32[]{:S(2)}) collective-permute-start(bf16[2048,256]{1,0:T(8,128)(2,1)} %collective-permute-done.refs_4_), channel_id=1, source_target_pairs={{0,1},{1,2},{2,3},{3,0},{4,5},{5,6},{6,7},{7,4},{8,9},{9,10},{10,1... | collective-permute-start | bytes 3145736 | tf_op jit(solution)/shard_map/ppermute | solution.py:397
  103.2 53.6 %collective-permute-start.9 = (bf16[2048,256]{1,0:T(8,128)(2,1)}, bf16[2048,256]{1,0:T(8,128)(2,1)}, u32[]{:S(2)}, u32[]{:S(2)}) collective-permute-start(bf16[2048,256]{1,0:T(8,128)(2,1)} %collective-permute-done.5.refs_9_), channel_id=1, source_target_pairs={{0,3},{1,0},{2,1},{3,2},{4,7},{5,4},{6,5},{7,6},{8,11},{9,8},{10,9... | collective-permute-start | bytes 3145736 | tf_op jit(solution)/shard_map/ppermute | solution.py:397
  129.8 32.6 %collective-permute-start.15 = (bf16[272,512]{1,0:T(8,128)(2,1)}, bf16[272,512]{1,0:T(8,128)(2,1)S(1)}, u32[]{:S(2)}, u32[]{:S(2)}) collective-permute-start(bf16[272,512]{1,0:T(8,128)(2,1)} %get-tuple-element.10), channel_id=1, source_target_pairs={{0,32},{4,36},{8,40},{12,44},{16,48},{20,52},{24,56},{28,60},{32,6... | collective-permute-start | bytes 835592 | tf_op jit(solution)/shard_map/ppermute | solution.py:460
  131.1 20.9 %copy-start.2 = (bf16[128,2048]{1,0:T(8,128)(2,1)}, bf16[128,2048]{1,0:T(8,128)(2,1)S(1)}, u32[]{:S(2)}) copy-start(bf16[128,2048]{1,0:T(8,128)(2,1)S(1)} %collective-permute-done.10.top_half) | copy-start | bytes 1572868
  131.1 31.2 %collective-permute-start.16 = (bf16[272,512]{1,0:T(8,128)(2,1)}, bf16[272,512]{1,0:T(8,128)(2,1)}, u32[]{:S(2)}, u32[]{:S(2)}) collective-permute-start(bf16[272,512]{1,0:T(8,128)(2,1)} %get-tuple-element.11), channel_id=1, source_target_pairs={{0,64},{4,68},{8,72},{12,76},{16,80},{20,84},{24,88},{28,92},{32,9... | collective-permute-start | bytes 835592 | tf_op jit(solution)/shard_map/ppermute | solution.py:460
  136.2 26.2 %collective-permute-start.17 = (bf16[272,512]{1,0:T(8,128)(2,1)}, bf16[272,512]{1,0:T(8,128)(2,1)}, u32[]{:S(2)}, u32[]{:S(2)}) collective-permute-start(bf16[272,512]{1,0:T(8,128)(2,1)} %get-tuple-element.12), channel_id=1, source_target_pairs={{0,96},{4,100},{8,104},{12,108},{16,112},{20,116},{24,120},{28,124... | collective-permute-start | bytes 835592 | tf_op jit(solution)/shard_map/ppermute | solution.py:460
  167.0 37.2 %copy-start.12 = (s32[128]{0:T(128)S(1)}, s32[128]{0:T(128)}, u32[]{:S(2)}) copy-start(s32[128]{0:T(128)} %copy-done.11) | copy-start | bytes 1540
  167.0 37.2 %copy-start.14 = (s32[128]{0:T(128)S(1)}, s32[128]{0:T(128)}, u32[]{:S(2)}) copy-start(s32[128]{0:T(128)} %copy-done.13) | copy-start | bytes 1540
  167.0 37.2 %all-to-all-start.1 = ((bf16[32,16,2048]{2,1,0:T(8,128)(2,1)}), bf16[32,16,2048]{2,1,0:T(8,128)(2,1)S(1)}, u32[]{:S(2)}, u32[]{:S(2)}) async-start(bf16[32,16,2048]{2,1,0:T(8,128)(2,1)} %bitcast.41), calls=%async_computation.2 | async-start | bytes 4194304 | tf_op jit(solution)/shard_map/all_to_all | solution.py:488
  (10 other events, 31.7 us)
Sparse Core Ops, SparseCore 0:
  16.0 40.4 all-gather.1
  167.1 29.2 reduce-scatter.1

commit v5 on v4

--- a/solution.py
+++ b/solution.py
@@ -1,3 +1,4 @@
+import functools
 import math
 import jax
 import jax.numpy as jnp
@@ -259,142 +260,159 @@
     return jnp.concatenate([jnp.concatenate([keys, turned], axis=1), parts], axis=0)
 
 
-def expert_hidden(x_ref, both, hidden_ref, at):
-    rows, ff = x_ref.shape[0], both.shape[1] // 2
-    for r in range(0, rows, 256):
-        lines = slice(r, r + 256)
-        pre = jnp.dot(x_ref[lines, :], both[...], preferred_element_type=jnp.float32)
-        gated, lifted = pre[:, :ff], pre[:, ff:]
-        hidden_ref[lines, at : at + ff] = (gated * jax.nn.sigmoid(gated) * lifted).astype(jnp.bfloat16)
-
-
 def column_tiles(width):
     return [slice(n, n + 512) for n in range(0, width, 512)]
 
 
-def first_kernel(x_hbm, *refs):
-    count = (len(refs) - 7) // 4
-    weights, (out_hbm, x_ref, both, down, hidden, out, sems) = refs[: 4 * count], refs[4 * count :]
-    ff = down.shape[0] // count
-    rows = pltpu.make_async_copy(x_hbm, x_ref, sems.at[4 * count])
-    rows.start()
-    copies = []
-    for q in range(count):
-        gate, up, upper, lower = weights[4 * q : 4 * q + 4]
-        middle = q * ff + ff // 2
-        pairs = (
-            (gate, both.at[q, :, :ff]),
-            (up, both.at[q, :, ff:]),
-            (upper, down.at[q * ff : middle, :]),
-            (lower, down.at[middle : (q + 1) * ff, :]),
-        )
-        for k, (src, dst) in enumerate(pairs):
-            copies.append(pltpu.make_async_copy(src, dst, sems.at[4 * q + k]))
+def fold_kernel(gate_hbm, up_hbm, down_hbm, one_hbm, two_hbm, gate, up, down, sems):
+    outs, ff = (one_hbm, two_hbm), gate.shape[1] // 2
+    blocks = down.shape[1] // DH
+    sources = ((gate_hbm, gate), (up_hbm, up), (down_hbm, down))
+    copies = [pltpu.make_async_copy(src, dst, sems.at[k]) for k, (src, dst) in enumerate(sources)]
     for c in copies:
         c.start()
-    rows.wait()
-    for q in range(count):
-        copies[4 * q].wait()
-        copies[4 * q + 1].wait()
-        expert_hidden(x_ref, both.at[q], hidden, q * ff)
-    for q in range(count):
-        copies[4 * q + 2].wait()
-        copies[4 * q + 3].wait()
+    stores = []
+
+    def store(src, dst):
+        stores.append(pltpu.make_async_copy(src, dst, sems.at[len(sources) + len(stores)]))
+        stores[-1].start()
+
+    for k, held in enumerate((gate, up)):
+        copies[k].wait()
+        for i, out in enumerate(outs):
+            store(held.at[:, i * ff : (i + 1) * ff], out.at[:, k * ff : (k + 1) * ff])
+    copies[2].wait()
+    for i, out in enumerate(outs):
+        for b in range(blocks):
+            store(
+                down.at[i * ff : (i + 1) * ff, b * DH : (b + 1) * DH],
+                out.at[b * ff : (b + 1) * ff, 2 * ff : 3 * ff],
+            )
+    for c in stores:
+        c.wait()
+
+
+def fold(gate, up, down):
+    width, ff = gate.shape
+    shape = jax.ShapeDtypeStruct((width, 3 * ff // 2), jnp.bfloat16)
+    return pl.pallas_call(
+        fold_kernel,
+        out_shape=[shape] * 2,
+        in_specs=[pl.BlockSpec(memory_space=pltpu.HBM)] * 3,
+        out_specs=[pl.BlockSpec(memory_space=pltpu.HBM)] * 2,
+        scratch_shapes=[
+            pltpu.VMEM(gate.shape, jnp.bfloat16),
+            pltpu.VMEM(up.shape, jnp.bfloat16),
+            pltpu.VMEM(down.shape, jnp.bfloat16),
+            pltpu.SemaphoreType.DMA((7 + 2 * (width // DH),)),
+        ],
+        cost_estimate=pl.CostEstimate(flops=1_000_000, bytes_accessed=12 * width * ff, transcendentals=0),
+    )(gate, up, down)
+
+
+def expert_kernel(count, joins, *refs):
+    holds, x_hbm, pieces, twins = refs[0], refs[1], refs[2 : 2 + count], refs[2 + count : 2 + 2 * count]
+    refs = refs[2 + 2 * count :]
+    if joins:
+        part_hbm, refs = refs[0], refs[1:]
+    out_hbm, x_ref, held, hidden, out, sems = refs[:6]
+    ff = held.shape[2] // 3
+    copies = [pltpu.make_async_copy(x_hbm, x_ref, sems.at[0])]
+    copies += [pltpu.make_async_copy(p, held.at[i], sems.at[1 + i]) for i, p in enumerate(pieces)]
+    copies[0].start()
+
+    @pl.when(holds[0] == 1)
+    def _():
+        for i in range(count):
+            copies[1 + i].start()
+
+    @pl.when(holds[0] == 0)
+    def _():
+        for i in range(count):
+            pltpu.make_async_copy(twins[i], held.at[i], sems.at[1 + i]).start()
+
+    if joins:
+        part = refs[6]
+        copies.append(pltpu.make_async_copy(part_hbm, part, sems.at[1 + count]))
+        copies[1 + count].start()
+    copies[0].wait()
+    for i in range(count):
+        copies[1 + i].wait()
+        for r in range(0, x_ref.shape[0], 256):
+            lines = slice(r, r + 256)
+            pre = jnp.dot(x_ref[lines, :], held[i, :, : 2 * ff], preferred_element_type=jnp.float32)
+            gated, lifted = pre[:, :ff], pre[:, ff:]
+            hidden[lines, i * ff : (i + 1) * ff] = (gated * jax.nn.sigmoid(gated) * lifted).astype(
+                jnp.bfloat16
+            )
+    if joins:
+        copies[1 + count].wait()
     stores = []
     for n, cols in enumerate(column_tiles(out.shape[1])):
-        out[:, cols] = jnp.dot(hidden[...], down[:, cols], preferred_element_type=jnp.float32)
+        weights = jnp.concatenate(
+            [
+                jnp.concatenate(
+                    [held[i, b * ff : (b + 1) * ff, 2 * ff :] for b in range(4 * n, 4 * n + 4)], axis=1
+                )
+                for i in range(count)
+            ],
+            axis=0,
+        )
+        total = jnp.dot(hidden[...], weights, preferred_element_type=jnp.float32)
+        if joins:
+            total = total + part[:, cols]
+        out[:, cols] = total.astype(out.dtype)
         stores.append(
-            pltpu.make_async_copy(out.at[:, cols], out_hbm.at[:, cols], sems.at[4 * count + 1 + n])
+            pltpu.make_async_copy(out.at[:, cols], out_hbm.at[:, cols], sems.at[2 + count + n])
         )
         stores[-1].start()
     for c in stores:
         c.wait()
 
 
-def first_parts(x, weights):
+def expert_parts(holds, x, pieces, part, out_type):
     rows, width = x.shape
-    count, ff = len(weights) // 4, weights[0].shape[1]
+    count, ff = len(pieces), pieces[0][0].shape[1] // 3
+    joined = [] if part is None else [part]
     return pl.pallas_call(
-        first_kernel,
-        out_shape=jax.ShapeDtypeStruct((rows, width), jnp.float32),
-        in_specs=[pl.BlockSpec(memory_space=pltpu.HBM)] * (1 + len(weights)),
+        functools.partial(expert_kernel, count, part is not None),
+        out_shape=jax.ShapeDtypeStruct((rows, width), out_type),
+        in_specs=[pl.BlockSpec(memory_space=pltpu.SMEM)]
+        + [pl.BlockSpec(memory_space=pltpu.HBM)] * (1 + 2 * count + len(joined)),
         out_specs=pl.BlockSpec(memory_space=pltpu.HBM),
         scratch_shapes=[
             pltpu.VMEM((rows, width), jnp.bfloat16),
-            pltpu.VMEM((count, width, 2 * ff), jnp.bfloat16),
-            pltpu.VMEM((count * ff, width), jnp.bfloat16),
+            pltpu.VMEM((count, width, 3 * ff), jnp.bfloat16),
             pltpu.VMEM((rows, count * ff), jnp.bfloat16),
-            pltpu.VMEM((rows, width), jnp.float32),
-            pltpu.SemaphoreType.DMA((4 * count + 1 + len(column_tiles(width)),)),
-        ],
+            pltpu.VMEM((rows, width), out_type),
+            pltpu.SemaphoreType.DMA((2 + count + len(column_tiles(width)),)),
+        ]
+        + [pltpu.VMEM((rows, width), jnp.float32)] * len(joined),
         cost_estimate=pl.CostEstimate(
             flops=count * 6 * rows * width * ff,
             bytes_accessed=count * 6 * width * ff,
             transcendentals=rows * count * ff,
         ),
-    )(x, *weights)
-
-
-def last_kernel(
-    x_hbm, part_hbm, gate, up, top_half, bottom_half, out_hbm, x_ref, part, both, down, hidden, out, sems
-):
-    ff = gate.shape[1]
-    pairs = (
-        (x_hbm, x_ref),
-        (gate, both.at[:, :ff]),
-        (up, both.at[:, ff:]),
-        (top_half, down.at[: ff // 2, :]),
-        (bottom_half, down.at[ff // 2 :, :]),
-        (part_hbm, part),
-    )
-    copies = [pltpu.make_async_copy(src, dst, sems.at[k]) for k, (src, dst) in enumerate(pairs)]
-    for c in copies:
-        c.start()
-    for c in copies[:3]:
-        c.wait()
-    expert_hidden(x_ref, both, hidden, 0)
-    for c in copies[3:]:
-        c.wait()
-    stores = []
-    for n, cols in enumerate(column_tiles(out.shape[1])):
-        out[:, cols] = (
-            part[:, cols]
-            + jnp.dot(hidden[...], down[:, cols], preferred_element_type=jnp.float32)
-        ).astype(jnp.bfloat16)
-        stores.append(
-            pltpu.make_async_copy(out.at[:, cols], out_hbm.at[:, cols], sems.at[len(pairs) + n])
-        )
-        stores[-1].start()
-    for c in stores:
-        c.wait()
-
-
-def last_part(x, part, gate, up, top_half, bottom_half):
-    rows, width = x.shape
-    ff = gate.shape[1]
-    return pl.pallas_call(
-        last_kernel,
-        out_shape=jax.ShapeDtypeStruct((rows, width), jnp.bfloat16),
-        in_specs=[pl.BlockSpec(memory_space=pltpu.HBM)] * 6,
-        out_specs=pl.BlockSpec(memory_space=pltpu.HBM),
-        scratch_shapes=[
-            pltpu.VMEM((rows, width), jnp.bfloat16),
-            pltpu.VMEM((rows, width), jnp.float32),
-            pltpu.VMEM((width, 2 * ff), jnp.bfloat16),
-            pltpu.VMEM((ff, width), jnp.bfloat16),
-            pltpu.VMEM((rows, ff), jnp.bfloat16),
-            pltpu.VMEM((rows, width), jnp.bfloat16),
-            pltpu.SemaphoreType.DMA((6 + len(column_tiles(width)),)),
-        ],
-        cost_estimate=pl.CostEstimate(
-            flops=6 * rows * width * ff, bytes_accessed=6 * width * ff, transcendentals=rows * ff
-        ),
-    )(x, part, gate, up, top_half, bottom_half)
-
-
-def shift(x, by):
-    count = lax.axis_size("tp")
-    return lax.ppermute(x, "tp", [(i, (i + by) % count) for i in range(count)])
+    )(holds, x, *[p[0] for p in pieces], *[p[1] for p in pieces], *joined)
+
+
+def shift(x, by, relays=False):
+    eps, tps = lax.axis_size("ep"), lax.axis_size("tp")
+    pairs = [
+        (e * tps + t, e * tps + (t + by) % tps)
+        for e in range(eps)
+        for t in range(tps)
+        if not relays or t % 2 != e % 2
+    ]
+    return lax.ppermute(x, ("ep", "tp"), pairs)
+
+
+def to_sibling(x):
+    eps, tps = lax.axis_size("ep"), lax.axis_size("tp")
+    pairs = [
+        (e * tps + t, (e ^ 1) * tps + t) for e in range(eps) for t in range(tps) if t % 2 == e % 2
+    ]
+    return lax.ppermute(x, ("ep", "tp"), pairs)
 
 
 def rms_scale(row_block, scale_gain):
@@ -432,16 +450,16 @@
     capacity = tp_count * own_rows // experts
     slots = experts * capacity
 
-    gate, up, down = expert_gate[0], expert_up[0], expert_down[0]
-    half = gate.shape[1] // 2
-    upper, lower = down[:half], down[half:]
-    own = {"gate": gate, "upper": upper, "up": up, "lower": lower}
-    first, second = ("gate", "upper"), ("up", "lower")
-    left = {n: shift(own[n], 1) for n in first + second}
-    right = {n: shift(own[n], -1) for n in second + first}
-    far = {n: shift(left[n], 1) for n in first}
-    far |= {n: shift(right[n], -1) for n in second}
-    names = ("gate", "up", "upper", "lower")
+    one, two = fold(expert_gate[0], expert_up[0], expert_down[0])
+    east, west = shift(one, 1), shift(two, -1)
+    east_more, west_more = shift(two, 1, True), shift(one, -1, True)
+    far_east, far_west = shift(east, 1, True), shift(west, -1, True)
+    mine = {
+        "one": one, "two": two, "east": east, "west": west,
+        "east_more": east_more, "west_more": west_more, "far_east": far_east, "far_west": far_west,
+    }
+    holds = (ep_index % 2 == tp_index % 2).astype(jnp.int32).reshape(1)
+    pieces = [(a, to_sibling(a)) for a in mine.values()]
 
     running = jnp.cumsum(jax.nn.log_sigmoid(forget_logit), axis=1)
     packed = pack(key_rows, value_rows, running)
@@ -459,19 +477,25 @@
         pairs = [(i, i + PLANE * d) for i in range(ep_count - PLANE * d)]
         told.append(lax.ppermute(answers[d], "ep", pairs))
 
-    own_first = tp_index * own_rows
-    own_group = lax.dynamic_slice_in_dim(route_group, own_first, own_rows, 0)
-    own_pick = lax.dynamic_slice_in_dim(route_pick, own_first, own_rows, 0)
-    chosen = own_group[:, None] * per_group + own_pick
+    pair_rows = 2 * own_rows
+    parity = tp_index % 2
+    pair_first = (tp_index // 2) * pair_rows
+    pair_group = lax.dynamic_slice_in_dim(route_group, pair_first, pair_rows, 0)
+    pair_pick = lax.dynamic_slice_in_dim(route_pick, pair_first, pair_rows, 0)
+    chosen = pair_group[:, None] * per_group + pair_pick
     expert_hit = chosen[:, :, None] == jnp.arange(experts, dtype=jnp.int32)
     usage = jnp.any(expert_hit, axis=1).astype(jnp.bfloat16)
-    line = jnp.arange(own_rows, dtype=jnp.int32)
-    earlier = (line[None, :] < line[:, None]).astype(jnp.bfloat16)
-    before = jnp.dot(earlier, usage, preferred_element_type=jnp.float32).astype(jnp.int32)
+    line = jnp.arange(pair_rows, dtype=jnp.int32)
+    side = line // own_rows
+    earlier = (line[None, :] < line[:, None]) & (side[None, :] == side[:, None])
+    before = jnp.dot(
+        earlier.astype(jnp.bfloat16), usage, preferred_element_type=jnp.float32
+    ).astype(jnp.int32)
     ranks = jnp.sum(jnp.where(expert_hit, before[:, None, :], 0), axis=2)
-    target = jnp.where(ranks < capacity, chosen * capacity + ranks, slots)
+    goes = (ranks < capacity) & (chosen % 2 == parity)
+    target = jnp.where(goes, (chosen - parity + side[:, None]) * capacity + ranks, slots)
     normed = rms_scale(
-        lax.dynamic_slice_in_dim(moe_input, own_first, own_rows, 0), moe_gain
+        lax.dynamic_slice_in_dim(moe_input, pair_first, pair_rows, 0), moe_gain
     ).astype(jnp.bfloat16)
     slot_at = jnp.arange(slots, dtype=jnp.int32)[:, None]
     sent = ((slot_at == target[None, :, 0]) | (slot_at == target[None, :, 1])).astype(jnp.bfloat16)
@@ -480,8 +504,8 @@
     arrived = lax.all_to_all(outgoing, "ep", split_axis=0, concat_axis=0, tiled=True)
     arrived = arrived.reshape(slots, width_model)
 
-    part = first_parts(arrived, [q[n] for q in (own, left, right) for n in names])
-    results = last_part(arrived, part, *[far[n] for n in names])
+    part = expert_parts(holds, arrived, pieces[:6], None, jnp.float32)
+    results = expert_parts(holds, arrived, pieces[6:], part, jnp.bfloat16)
     results, told[0] = lax.optimization_barrier((results, told[0]))
     mixer_term = merge(place, told, out_weight)
     results = results.reshape(experts, capacity, width_model)
@@ -495,7 +519,7 @@
     expert_logits = jnp.dot(normed, router_expert, preferred_element_type=jnp.float32)
     group_top = jnp.max(group_logits, axis=1, keepdims=True)
     group_exp = jnp.exp(group_logits - group_top)
-    group_hit = jnp.arange(GROUPS, dtype=jnp.int32)[None, :] == own_group[:, None]
+    group_hit = jnp.arange(GROUPS, dtype=jnp.int32)[None, :] == pair_group[:, None]
     group_share = jnp.sum(jnp.where(group_hit, group_exp, 0.0), axis=1) / jnp.sum(group_exp, axis=1)
     picked_logits = jnp.sum(jnp.where(expert_hit, expert_logits[:, None, :], 0.0), axis=2)
     shares = group_share[:, None] * jax.nn.sigmoid(picked_logits - picked_logits[:, ::-1])
@@ -503,10 +527,18 @@
     weight = jnp.where(column == target[:, :1], shares[:, :1], 0.0) + jnp.where(
         column == target[:, 1:], shares[:, 1:], 0.0
     )
-    high = lax.reduce_precision(weight, 8, 7)
-    moe_out = jnp.dot(
-        high.astype(jnp.bfloat16), returned, preferred_element_type=jnp.float32
-    ) + jnp.dot((weight - high).astype(jnp.bfloat16), returned, preferred_element_type=jnp.float32)
+
+    def combine(block):
+        lines = lax.dynamic_slice_in_dim(weight, block * own_rows, own_rows, 0)
+        high = lax.reduce_precision(lines, 8, 7)
+        both = jnp.concatenate([high, lines - high], axis=1).astype(jnp.bfloat16)
+        twice = jnp.concatenate([returned, returned], axis=0)
+        return jnp.dot(both, twice, preferred_element_type=jnp.float32)
+
+    other = lax.ppermute(
+        combine(1 - parity).astype(jnp.bfloat16), "tp", [(t, t ^ 1) for t in range(tp_count)]
+    )
+    moe_out = combine(parity) + other.astype(jnp.float32)
     return (mixer_out, moe_out.astype(jnp.bfloat16))
 
 

time: 217 us -> 211 us (0.972)
  waiting for transfers between devices: 90 us -> 72.9 us
  starting transfers between devices: 49.3 us -> 60.9 us
  local copies, waits for them, and re-layouts: 6.92 us -> 2.6 us
  Pallas kernels: 42.1 us -> 45.7 us
    ppermute x12 -> x15, waiting for transfers between devices: 60.6 us -> 16.1 us  [the longest x1 10.9 us: inner(): lax.ppermute(combine(1 - parity).astype(jnp.bfloat16), 'tp', [(t, t ^ 1)...]
    ppermute x3, waiting for transfers between devices: 0.01 us -> 28.2 us  [inner(): asked.append(lax.ppermute(queries, 'ep', pairs))]
    ppermute x12 -> x15, starting transfers between devices: 17 us -> 31.8 us  [the longest x8 21.2 us: to_sibling(): return lax.ppermute(x, ('ep', 'tp'), pairs)]
    ppermute x3, starting transfers between devices: 9.52 us -> 5.32 us  [inner(): told.append(lax.ppermute(answers[d], 'ep', pairs))]
    pallas_call x2 -> x3, Pallas kernels: 14.5 us -> 18.1 us  [the longest x2 14.6 us: expert_parts(): pl.pallas_call(functools.partial(expert_kernel, count, part is not None),...]
  transfers between devices with their start and end apart: 22 -> 25, of which waited for: 5 -> 6; matrix products, arithmetic and copies ran while one was open for 6% -> 5% of each run, Pallas kernels for 18% -> 18%
where the time goes in v5:
time: 211 us; the launch traced here: 209 us
  waiting for transfers between devices  72.9 us (35%)
  starting transfers between devices  60.9 us (29%)
  Pallas kernels  45.7 us (22%)
  between operations  14.7 us (7%)
  other arithmetic  7.23 us (3%)
  matrix products  5.34 us (3%)
  local copies, waits for them, and re-layouts  2.6 us (1%)
    all_to_all x1, waiting for transfers between devices, inner(): lax.all_to_all(results, 'ep', split_axis=0, concat_axis=0, tiled=True)  28.6 us
    ppermute x3, waiting for transfers between devices, inner(): asked.append(lax.ppermute(queries, 'ep', pairs))  28.2 us
    pallas_call x1, Pallas kernels, attend(): pl.pallas_call(attend_kernel, out_shape=[jax.ShapeDtypeStruct((2 * DH + 1...  23.7 us
    ppermute x8, starting transfers between devices, to_sibling(): return lax.ppermute(x, ('ep', 'tp'), pairs)  21.2 us
    pallas_call x2, Pallas kernels, expert_parts(): pl.pallas_call(functools.partial(expert_kernel, count, part is not None),...  14.6 us
    all_to_all x1, starting transfers between devices, inner(): lax.all_to_all(outgoing, 'ep', split_axis=0, concat_axis=0, tiled=True)  11.1 us
    ppermute x1, waiting for transfers between devices, inner(): lax.ppermute(combine(1 - parity).astype(jnp.bfloat16), 'tp', [(t, t ^ 1)...  10.9 us
    all_to_all x1, starting transfers between devices, inner(): lax.all_to_all(results, 'ep', split_axis=0, concat_axis=0, tiled=True)  8.75 us
  transfers between devices with their start and end apart: 25, of which 6 were waited for; matrix products, arithmetic and copies ran while one was open for 5% of the time, Pallas kernels for 18%

profile of v5, /device:TPU:0, one launch (start us, length us, event | category | flops | bytes accessed | tf_op | source)
XLA Modules:
  0.0 209.4 jit_solution(14677923244318689477)
XLA Ops:
  7.3 3.5 %shard_map.158 = (bf16[2048,384]{1,0:T(8,128)(2,1)}, bf16[2048,384]{1,0:T(8,128)(2,1)}) custom-call(bf16[2048,256]{1,0:T(8,128)(2,1)} %bitcast.34, bf16[2048,256]{1,0:T(8,128)(2,1)} %bitcast.35, bf16[256,2048]{1,0:T(8,128)(2,1)} %bitcast.36), custom_call_target="tpu_custom_call" | custom-call | flops 1000000 | bytes 6291456 | tf_op jit(solution)/shard_map/pallas_call | solution.py:298
  10.8 1.7 collective-permute-start
  12.5 1.6 collective-permute-start.2
  16.2 1.3 collective-permute-start.6
  20.8 7.5 %collective-permute-done.14.q1 = bf16[512,256]{1,0:T(8,128)(2,1)S(1)} collective-permute-done((bf16[512,256]{1,0:T(8,128)(2,1)S(1)}, bf16[512,256]{1,0:T(8,128)(2,1)S(1)}, u32[]{:S(2)}, u32[]{:S(2)}) %collective-permute-start.14) | collective-permute-done | bytes 262176 | tf_op jit(solution)/shard_map/ppermute | solution.py:473
  29.9 10.2 %collective-permute-done.15.q2 = bf16[512,256]{1,0:T(8,128)(2,1)S(1)} collective-permute-done((bf16[512,256]{1,0:T(8,128)(2,1)S(1)}, bf16[512,256]{1,0:T(8,128)(2,1)S(1)}, u32[]{:S(2)}, u32[]{:S(2)}) %collective-permute-start.15) | collective-permute-done | bytes 262176 | tf_op jit(solution)/shard_map/ppermute | solution.py:473
  41.7 10.4 %collective-permute-done.16.q3 = bf16[512,256]{1,0:T(8,128)(2,1)S(1)} collective-permute-done((bf16[512,256]{1,0:T(8,128)(2,1)S(1)}, bf16[512,256]{1,0:T(8,128)(2,1)S(1)}, u32[]{:S(2)}, u32[]{:S(2)}) %collective-permute-start.16) | collective-permute-done | bytes 262176 | tf_op jit(solution)/shard_map/ppermute | solution.py:473
  52.2 3.0 %collective-permute-start.8 = (bf16[2048,384]{1,0:T(8,128)(2,1)}, bf16[2048,384]{1,0:T(8,128)(2,1)}, u32[]{:S(2)}, u32[]{:S(2)}) collective-permute-start(bf16[2048,384]{1,0:T(8,128)(2,1)} %get-tuple-element.10.refs_2_), channel_id=1, source_target_pairs={{0,4},{2,6},{5,1},{7,3},{8,12},{10,14},{13,9},{15,11},{16,20},{18,... | collective-permute-start | bytes 4718600 | tf_op jit(solution)/shard_map/ppermute | solution.py:415
  55.2 2.4 %collective-permute-start.9 = (bf16[2048,384]{1,0:T(8,128)(2,1)}, bf16[2048,384]{1,0:T(8,128)(2,1)}, u32[]{:S(2)}, u32[]{:S(2)}) collective-permute-start(bf16[2048,384]{1,0:T(8,128)(2,1)} %get-tuple-element.11.refs_3_), channel_id=1, source_target_pairs={{0,4},{2,6},{5,1},{7,3},{8,12},{10,14},{13,9},{15,11},{16,20},{18,... | collective-permute-start | bytes 4718600 | tf_op jit(solution)/shard_map/ppermute | solution.py:415
  57.7 2.5 %collective-permute-start.10 = (bf16[2048,384]{1,0:T(8,128)(2,1)}, bf16[2048,384]{1,0:T(8,128)(2,1)}, u32[]{:S(2)}, u32[]{:S(2)}) collective-permute-start(bf16[2048,384]{1,0:T(8,128)(2,1)} %collective-permute-done.refs_4_), channel_id=1, source_target_pairs={{0,4},{2,6},{5,1},{7,3},{8,12},{10,14},{13,9},{15,11},{16,20},{18,... | collective-permute-start | bytes 4718600 | tf_op jit(solution)/shard_map/ppermute | solution.py:415
  60.1 5.2 %collective-permute-done.6.refs_6_ = bf16[2048,384]{1,0:T(8,128)(2,1)} collective-permute-done((bf16[2048,384]{1,0:T(8,128)(2,1)}, bf16[2048,384]{1,0:T(8,128)(2,1)}, u32[]{:S(2)}, u32[]{:S(2)}) %collective-permute-start.6) | collective-permute-done | bytes 1572896 | tf_op jit(solution)/shard_map/ppermute | solution.py:407
  68.3 2.0 convolution_convert_fusion
  70.3 11.1 %all-to-all-start = ((bf16[32,16,2048]{2,1,0:T(8,128)(2,1)}), bf16[32,16,2048]{2,1,0:T(8,128)(2,1)S(1)}, u32[]{:S(2)}, u32[]{:S(2)}) async-start(bf16[32,16,2048]{2,1,0:T(8,128)(2,1)} %bitcast.31), calls=%async_computation | async-start | bytes 4194304 | tf_op jit(solution)/shard_map/all_to_all | solution.py:504
  81.5 3.3 %collective-permute-start.11 = (bf16[2048,384]{1,0:T(8,128)(2,1)}, bf16[2048,384]{1,0:T(8,128)(2,1)}, u32[]{:S(2)}, u32[]{:S(2)}) collective-permute-start(bf16[2048,384]{1,0:T(8,128)(2,1)} %collective-permute-done.2.refs_5_), channel_id=1, source_target_pairs={{0,4},{2,6},{5,1},{7,3},{8,12},{10,14},{13,9},{15,11},{16,20},{18,... | collective-permute-start | bytes 4718600 | tf_op jit(solution)/shard_map/ppermute | solution.py:415
  84.8 2.5 %collective-permute-start.12 = (bf16[2048,384]{1,0:T(8,128)(2,1)}, bf16[2048,384]{1,0:T(8,128)(2,1)}, u32[]{:S(2)}, u32[]{:S(2)}) collective-permute-start(bf16[2048,384]{1,0:T(8,128)(2,1)} %collective-permute-done.6.refs_6_), channel_id=1, source_target_pairs={{0,4},{2,6},{5,1},{7,3},{8,12},{10,14},{13,9},{15,11},{16,20},{18,... | collective-permute-start | bytes 4718600 | tf_op jit(solution)/shard_map/ppermute | solution.py:415
  87.3 2.4 %collective-permute-start.13 = (bf16[2048,384]{1,0:T(8,128)(2,1)}, bf16[2048,384]{1,0:T(8,128)(2,1)}, u32[]{:S(2)}, u32[]{:S(2)}) collective-permute-start(bf16[2048,384]{1,0:T(8,128)(2,1)} %collective-permute-done.7.refs_7_), channel_id=1, source_target_pairs={{0,4},{2,6},{5,1},{7,3},{8,12},{10,14},{13,9},{15,11},{16,20},{18,... | collective-permute-start | bytes 4718600 | tf_op jit(solution)/shard_map/ppermute | solution.py:415
  89.7 2.5 %collective-permute-start.4 = (bf16[2048,384]{1,0:T(8,128)(2,1)}, bf16[2048,384]{1,0:T(8,128)(2,1)}, u32[]{:S(2)}, u32[]{:S(2)}) collective-permute-start(bf16[2048,384]{1,0:T(8,128)(2,1)} %collective-permute-done.1.refs_2_), channel_id=1, source_target_pairs={{0,4},{2,6},{5,1},{7,3},{8,12},{10,14},{13,9},{15,11},{16,20},{18,... | collective-permute-start | bytes 4718600 | tf_op jit(solution)/shard_map/ppermute | solution.py:415
  92.3 2.5 %collective-permute-start.5 = (bf16[2048,384]{1,0:T(8,128)(2,1)}, bf16[2048,384]{1,0:T(8,128)(2,1)}, u32[]{:S(2)}, u32[]{:S(2)}) collective-permute-start(bf16[2048,384]{1,0:T(8,128)(2,1)} %collective-permute-done.3.refs_3_), channel_id=1, source_target_pairs={{0,4},{2,6},{5,1},{7,3},{8,12},{10,14},{13,9},{15,11},{16,20},{18,... | collective-permute-start | bytes 4718600 | tf_op jit(solution)/shard_map/ppermute | solution.py:415
  95.4 23.7 %shard_map.161 = (bf16[272,512]{1,0:T(8,128)(2,1)}, bf16[272,512]{1,0:T(8,128)(2,1)}, bf16[272,512]{1,0:T(8,128)(2,1)}, bf16[272,512]{1,0:T(8,128)(2,1)}) custom-call(s32[2]{0:T(128)} %pad_add_fusion.pos_ref, bf16[512,256]{1,0:T(8,128)(2,1)} %q0.1, bf16[512,256]{1,0:T(8,128)(2,1)} %copy-done.20, bf16[512,256]{1,0:T(8,128)(2,1)} %copy-done.21, ...), custom_call_target="tpu_custom_call" | custom-call | flops 8999999488 | bytes 4000000 | tf_op jit(solution)/shard_map/pallas_call | solution.py:171
  119.2 1.3 collective-permute-start.17
  120.5 2.0 collective-permute-start.18
  122.5 2.0 collective-permute-start.19
  124.5 1.4 copy-done.1
  125.9 9.1 %shard_map.159.refs_6_ = f32[512,2048]{1,0:T(8,128)} custom-call(s32[1]{0:T(128)} %bitcast.2.refs_0_, bf16[512,2048]{1,0:T(8,128)(2,1)} %bitcast.29, bf16[2048,384]{1,0:T(8,128)(2,1)} %get-tuple-element.10.refs_2_, bf16[2048,384]{1,0:T(8,128)(2,1)} %get-tuple-element.11.refs_3_, bf16[2048,384]{1,0:T(8,128)(2,1)} %collective-permute-done.refs_4_, ...), custom_call_target="tpu_custom_call" | custom-call | flops 4831838208 | bytes 9437184 | tf_op jit(solution)/shard_map/pallas_call | solution.py:377
  135.0 5.5 %shard_map.160 = bf16[512,2048]{1,0:T(8,128)(2,1)} custom-call(s32[1]{0:T(128)} %bitcast.2.refs_0_, bf16[512,2048]{1,0:T(8,128)(2,1)} %bitcast.30, bf16[2048,384]{1,0:T(8,128)(2,1)} %collective-permute-done.1.refs_2_, bf16[2048,384]{1,0:T(8,128)(2,1)} %collective-permute-done.3.refs_3_, bf16[2048,384]{1,0:T(8,128)(2,1)} %collective-permute-done.4.refs_4_, ...), custom_call_target="tpu_custom_call" | custom-call | flops 1610612736 | bytes 3145728 | tf_op jit(solution)/shard_map/pallas_call | solution.py:377
  141.2 3.9 %shard_map.162 = bf16[512,2048]{1,0:T(8,128)(2,1)} custom-call(s32[2]{0:T(128)} %pad_add_fusion.pos_ref, bf16[272,512]{1,0:T(8,128)(2,1)} %get-tuple-element.13.p0, bf16[272,512]{1,0:T(8,128)(2,1)} %copy-done.3, bf16[272,512]{1,0:T(8,128)(2,1)} %collective-permute-done.18.p2, bf16[272,512]{1,0:T(8,128)(2,1)} %collective-permute-done.19.p3, ...), custom_call_target="tpu_custom_call" | custom-call | flops 536870912 | bytes 4000000 | tf_op jit(solution)/shard_map/pallas_call | solution.py:238
  145.2 8.8 %all-to-all-start.1 = ((bf16[32,16,2048]{2,1,0:T(8,128)(2,1)}), bf16[32,16,2048]{2,1,0:T(8,128)(2,1)S(1)}, u32[]{:S(2)}, u32[]{:S(2)}) async-start(bf16[32,16,2048]{2,1,0:T(8,128)(2,1)} %bitcast.18), calls=%async_computation.2 | async-start | bytes 4194304 | tf_op jit(solution)/shard_map/all_to_all | solution.py:512
  155.4 28.6 %all-to-all-done.1 = bf16[32,16,2048]{2,1,0:T(8,128)(2,1)S(1)} async-done(((bf16[32,16,2048]{2,1,0:T(8,128)(2,1)}), bf16[32,16,2048]{2,1,0:T(8,128)(2,1)S(1)}, u32[]{:S(2)}, u32[]{:S(2)}) %all-to-all-start.1) | async-done | bytes 2097184 | tf_op jit(solution)/shard_map/all_to_all | solution.py:512
  184.7 2.1 %collective-permute-start.20 = (bf16[128,2048]{1,0:T(8,128)(2,1)S(1)}, bf16[128,2048]{1,0:T(8,128)(2,1)S(1)}, u32[]{:S(2)}, u32[]{:S(2)}) collective-permute-start(bf16[128,2048]{1,0:T(8,128)(2,1)S(1)} %fusion.2), channel_id=1, source_target_pairs={{0,1},{1,0},{2,3},{3,2},{4,5},{5,4},{6,7},{7,6},{8,9},{9,8},{10,11... | collective-permute-start | bytes 1572872 | tf_op jit(solution)/shard_map/ppermute | solution.py:538
  186.9 10.9 %collective-permute-done.20 = bf16[128,2048]{1,0:T(8,128)(2,1)S(1)} collective-permute-done((bf16[128,2048]{1,0:T(8,128)(2,1)S(1)}, bf16[128,2048]{1,0:T(8,128)(2,1)S(1)}, u32[]{:S(2)}, u32[]{:S(2)}) %collective-permute-start.20) | collective-permute-done | bytes 524320 | tf_op jit(solution)/shard_map/ppermute | solution.py:538
  197.8 1.5 add_convert_fusion
  200.6 2.0 fusion.8
  (114 shorter events, 16.1 us)
Async XLA Ops:
  7.2 146.8 %copy-start = (bf16[2048,32]{0,1:T(8,128)(2,1)S(1)}, bf16[2048,32]{0,1:T(8,128)(2,1)}, u32[]{:S(2)}) copy-start(bf16[2048,32]{0,1:T(8,128)(2,1)} %param.24) | copy-start | bytes 393220
  7.2 88.2 %all-gather.2.cloned.1.call-start = ((), (), s32[]{:S(2)}) async-start(), calls=%async_computation.3 | async-start | bytes 2433024 | tf_op jit(solution)/shard_map/all_gather | solution.py:467
  7.3 34.1 %copy-start.2 = (bf16[512,2048]{1,0:T(8,128)(2,1)S(1)}, bf16[512,2048]{1,0:T(8,128)(2,1)}, u32[]{:S(2)}) copy-start(bf16[512,2048]{1,0:T(8,128)(2,1)} %param.21) | copy-start | bytes 6291460
  10.8 57.2 %copy-start.13 = (f32[2048]{0:T(1024)S(1)}, f32[2048]{0:T(1024)}, u32[]{:S(2)}) copy-start(f32[2048]{0:T(1024)} %param.22) | copy-start | bytes 24580
  10.8 44.4 %collective-permute-start = (bf16[2048,384]{1,0:T(8,128)(2,1)}, bf16[2048,384]{1,0:T(8,128)(2,1)}, u32[]{:S(2)}, u32[]{:S(2)}) collective-permute-start(bf16[2048,384]{1,0:T(8,128)(2,1)} %get-tuple-element.10.refs_2_), channel_id=1, source_target_pairs={{0,1},{1,2},{2,3},{3,0},{4,5},{5,6},{6,7},{7,4},{8,9},{9,10},{10,1... | collective-permute-start | bytes 4718600 | tf_op jit(solution)/shard_map/ppermute | solution.py:407
  12.5 45.2 %collective-permute-start.2 = (bf16[2048,384]{1,0:T(8,128)(2,1)}, bf16[2048,384]{1,0:T(8,128)(2,1)}, u32[]{:S(2)}, u32[]{:S(2)}) collective-permute-start(bf16[2048,384]{1,0:T(8,128)(2,1)} %get-tuple-element.11.refs_3_), channel_id=1, source_target_pairs={{0,3},{1,0},{2,1},{3,2},{4,7},{5,4},{6,5},{7,6},{8,11},{9,8},{10,9... | collective-permute-start | bytes 4718600 | tf_op jit(solution)/shard_map/ppermute | solution.py:407
  16.2 49.1 %collective-permute-start.6 = (bf16[2048,384]{1,0:T(8,128)(2,1)}, bf16[2048,384]{1,0:T(8,128)(2,1)}, u32[]{:S(2)}, u32[]{:S(2)}) collective-permute-start(bf16[2048,384]{1,0:T(8,128)(2,1)} %get-tuple-element.11.refs_3_), channel_id=1, source_target_pairs={{1,2},{3,0},{4,5},{6,7},{9,10},{11,8},{12,13},{14,15},{17,18},{19,... | collective-permute-start | bytes 4718600 | tf_op jit(solution)/shard_map/ppermute | solution.py:407
  17.5 49.1 %collective-permute-start.7 = (bf16[2048,384]{1,0:T(8,128)(2,1)}, bf16[2048,384]{1,0:T(8,128)(2,1)}, u32[]{:S(2)}, u32[]{:S(2)}) collective-permute-start(bf16[2048,384]{1,0:T(8,128)(2,1)} %get-tuple-element.10.refs_2_), channel_id=1, source_target_pairs={{1,0},{3,2},{4,7},{6,5},{9,8},{11,10},{12,15},{14,13},{17,16},{19,... | collective-permute-start | bytes 4718600 | tf_op jit(solution)/shard_map/ppermute | solution.py:407
  18.8 9.5 %collective-permute-start.14 = (bf16[512,256]{1,0:T(8,128)(2,1)S(1)}, bf16[512,256]{1,0:T(8,128)(2,1)S(1)}, u32[]{:S(2)}, u32[]{:S(2)}) collective-permute-start(bf16[512,256]{1,0:T(8,128)(2,1)S(1)} %copy-done.19), channel_id=1, source_target_pairs={{32,0},{36,4},{40,8},{44,12},{48,16},{52,20},{56,24},{60,28},{64,3... | collective-permute-start | bytes 786440 | tf_op jit(solution)/shard_map/ppermute | solution.py:473
  20.8 45.8 %copy-start.6 = (s32[256,2]{0,1:T(2,128)}, s32[256,2]{0,1:T(2,128)S(1)}, u32[]{:S(2)}) copy-start(s32[256,2]{0,1:T(2,128)S(1)} %dynamic-slice_add_fusion) | copy-start | bytes 6148
  28.3 38.3 %copy-start.20 = (bf16[512,256]{1,0:T(8,128)(2,1)}, bf16[512,256]{1,0:T(8,128)(2,1)S(1)}, u32[]{:S(2)}) copy-start(bf16[512,256]{1,0:T(8,128)(2,1)S(1)} %collective-permute-done.14.q1) | copy-start | bytes 786436
  28.3 11.8 %collective-permute-start.15 = (bf16[512,256]{1,0:T(8,128)(2,1)S(1)}, bf16[512,256]{1,0:T(8,128)(2,1)S(1)}, u32[]{:S(2)}, u32[]{:S(2)}) collective-permute-start(bf16[512,256]{1,0:T(8,128)(2,1)S(1)} %copy-done.19), channel_id=1, source_target_pairs={{64,0},{68,4},{72,8},{76,12},{80,16},{84,20},{88,24},{92,28},{96,3... | collective-permute-start | bytes 786440 | tf_op jit(solution)/shard_map/ppermute | solution.py:473
  40.1 26.5 %copy-start.21 = (bf16[512,256]{1,0:T(8,128)(2,1)}, bf16[512,256]{1,0:T(8,128)(2,1)S(1)}, u32[]{:S(2)}) copy-start(bf16[512,256]{1,0:T(8,128)(2,1)S(1)} %collective-permute-done.15.q2) | copy-start | bytes 786436
  40.1 12.1 %collective-permute-start.16 = (bf16[512,256]{1,0:T(8,128)(2,1)S(1)}, bf16[512,256]{1,0:T(8,128)(2,1)S(1)}, u32[]{:S(2)}, u32[]{:S(2)}) collective-permute-start(bf16[512,256]{1,0:T(8,128)(2,1)S(1)} %copy-done.19), channel_id=1, source_target_pairs={{96,0},{100,4},{104,8},{108,12},{112,16},{116,20},{120,24},{124,28... | collective-permute-start | bytes 786440 | tf_op jit(solution)/shard_map/ppermute | solution.py:473
  52.2 14.5 %copy-start.22 = (bf16[512,256]{1,0:T(8,128)(2,1)}, bf16[512,256]{1,0:T(8,128)(2,1)S(1)}, u32[]{:S(2)}) copy-start(bf16[512,256]{1,0:T(8,128)(2,1)S(1)} %collective-permute-done.16.q3) | copy-start | bytes 786436
  52.2 29.3 %collective-permute-start.8 = (bf16[2048,384]{1,0:T(8,128)(2,1)}, bf16[2048,384]{1,0:T(8,128)(2,1)}, u32[]{:S(2)}, u32[]{:S(2)}) collective-permute-start(bf16[2048,384]{1,0:T(8,128)(2,1)} %get-tuple-element.10.refs_2_), channel_id=1, source_target_pairs={{0,4},{2,6},{5,1},{7,3},{8,12},{10,14},{13,9},{15,11},{16,20},{18,... | collective-permute-start | bytes 4718600 | tf_op jit(solution)/shard_map/ppermute | solution.py:415
  55.2 29.6 %collective-permute-start.9 = (bf16[2048,384]{1,0:T(8,128)(2,1)}, bf16[2048,384]{1,0:T(8,128)(2,1)}, u32[]{:S(2)}, u32[]{:S(2)}) collective-permute-start(bf16[2048,384]{1,0:T(8,128)(2,1)} %get-tuple-element.11.refs_3_), channel_id=1, source_target_pairs={{0,4},{2,6},{5,1},{7,3},{8,12},{10,14},{13,9},{15,11},{16,20},{18,... | collective-permute-start | bytes 4718600 | tf_op jit(solution)/shard_map/ppermute | solution.py:415
  57.7 29.7 %collective-permute-start.10 = (bf16[2048,384]{1,0:T(8,128)(2,1)}, bf16[2048,384]{1,0:T(8,128)(2,1)}, u32[]{:S(2)}, u32[]{:S(2)}) collective-permute-start(bf16[2048,384]{1,0:T(8,128)(2,1)} %collective-permute-done.refs_4_), channel_id=1, source_target_pairs={{0,4},{2,6},{5,1},{7,3},{8,12},{10,14},{13,9},{15,11},{16,20},{18,... | collective-permute-start | bytes 4718600 | tf_op jit(solution)/shard_map/ppermute | solution.py:415
  65.3 24.4 %collective-permute-start.1 = (bf16[2048,384]{1,0:T(8,128)(2,1)}, bf16[2048,384]{1,0:T(8,128)(2,1)}, u32[]{:S(2)}, u32[]{:S(2)}) collective-permute-start(bf16[2048,384]{1,0:T(8,128)(2,1)} %collective-permute-done.refs_4_), channel_id=1, source_target_pairs={{1,2},{3,0},{4,5},{6,7},{9,10},{11,8},{12,13},{14,15},{17,18},{19,... | collective-permute-start | bytes 4718600 | tf_op jit(solution)/shard_map/ppermute | solution.py:407
  66.7 25.6 %collective-permute-start.3 = (bf16[2048,384]{1,0:T(8,128)(2,1)}, bf16[2048,384]{1,0:T(8,128)(2,1)}, u32[]{:S(2)}, u32[]{:S(2)}) collective-permute-start(bf16[2048,384]{1,0:T(8,128)(2,1)} %collective-permute-done.2.refs_5_), channel_id=1, source_target_pairs={{1,0},{3,2},{4,7},{6,5},{9,8},{11,10},{12,15},{14,13},{17,16},{19,... | collective-permute-start | bytes 4718600 | tf_op jit(solution)/shard_map/ppermute | solution.py:407
  70.3 54.2 %all-to-all-start = ((bf16[32,16,2048]{2,1,0:T(8,128)(2,1)}), bf16[32,16,2048]{2,1,0:T(8,128)(2,1)S(1)}, u32[]{:S(2)}, u32[]{:S(2)}) async-start(bf16[32,16,2048]{2,1,0:T(8,128)(2,1)} %bitcast.31), calls=%async_computation | async-start | bytes 4194304 | tf_op jit(solution)/shard_map/all_to_all | solution.py:504
  81.4 117.9 %reduce-scatter.2.cloned.1.call-start = ((), (), s32[]{:S(2)}) async-start(), calls=%async_computation.4 | async-start | bytes 2621440 | tf_op jit(solution)/shard_map/reduce_scatter | solution.py:515
  81.5 37.7 %collective-permute-start.11 = (bf16[2048,384]{1,0:T(8,128)(2,1)}, bf16[2048,384]{1,0:T(8,128)(2,1)}, u32[]{:S(2)}, u32[]{:S(2)}) collective-permute-start(bf16[2048,384]{1,0:T(8,128)(2,1)} %collective-permute-done.2.refs_5_), channel_id=1, source_target_pairs={{0,4},{2,6},{5,1},{7,3},{8,12},{10,14},{13,9},{15,11},{16,20},{18,... | collective-permute-start | bytes 4718600 | tf_op jit(solution)/shard_map/ppermute | solution.py:415
  84.8 35.7 %collective-permute-start.12 = (bf16[2048,384]{1,0:T(8,128)(2,1)}, bf16[2048,384]{1,0:T(8,128)(2,1)}, u32[]{:S(2)}, u32[]{:S(2)}) collective-permute-start(bf16[2048,384]{1,0:T(8,128)(2,1)} %collective-permute-done.6.refs_6_), channel_id=1, source_target_pairs={{0,4},{2,6},{5,1},{7,3},{8,12},{10,14},{13,9},{15,11},{16,20},{18,... | collective-permute-start | bytes 4718600 | tf_op jit(solution)/shard_map/ppermute | solution.py:415
  87.3 35.2 %collective-permute-start.13 = (bf16[2048,384]{1,0:T(8,128)(2,1)}, bf16[2048,384]{1,0:T(8,128)(2,1)}, u32[]{:S(2)}, u32[]{:S(2)}) collective-permute-start(bf16[2048,384]{1,0:T(8,128)(2,1)} %collective-permute-done.7.refs_7_), channel_id=1, source_target_pairs={{0,4},{2,6},{5,1},{7,3},{8,12},{10,14},{13,9},{15,11},{16,20},{18,... | collective-permute-start | bytes 4718600 | tf_op jit(solution)/shard_map/ppermute | solution.py:415
  89.7 45.2 %collective-permute-start.4 = (bf16[2048,384]{1,0:T(8,128)(2,1)}, bf16[2048,384]{1,0:T(8,128)(2,1)}, u32[]{:S(2)}, u32[]{:S(2)}) collective-permute-start(bf16[2048,384]{1,0:T(8,128)(2,1)} %collective-permute-done.1.refs_2_), channel_id=1, source_target_pairs={{0,4},{2,6},{5,1},{7,3},{8,12},{10,14},{13,9},{15,11},{16,20},{18,... | collective-permute-start | bytes 4718600 | tf_op jit(solution)/shard_map/ppermute | solution.py:415
  92.3 42.7 %collective-permute-start.5 = (bf16[2048,384]{1,0:T(8,128)(2,1)}, bf16[2048,384]{1,0:T(8,128)(2,1)}, u32[]{:S(2)}, u32[]{:S(2)}) collective-permute-start(bf16[2048,384]{1,0:T(8,128)(2,1)} %collective-permute-done.3.refs_3_), channel_id=1, source_target_pairs={{0,4},{2,6},{5,1},{7,3},{8,12},{10,14},{13,9},{15,11},{16,20},{18,... | collective-permute-start | bytes 4718600 | tf_op jit(solution)/shard_map/ppermute | solution.py:415
  119.2 21.3 %collective-permute-start.17 = (bf16[272,512]{1,0:T(8,128)(2,1)}, bf16[272,512]{1,0:T(8,128)(2,1)S(1)}, u32[]{:S(2)}, u32[]{:S(2)}) collective-permute-start(bf16[272,512]{1,0:T(8,128)(2,1)} %get-tuple-element.14), channel_id=1, source_target_pairs={{0,32},{4,36},{8,40},{12,44},{16,48},{20,52},{24,56},{28,60},{32,6... | collective-permute-start | bytes 835592 | tf_op jit(solution)/shard_map/ppermute | solution.py:478
  120.5 20.0 %collective-permute-start.18 = (bf16[272,512]{1,0:T(8,128)(2,1)}, bf16[272,512]{1,0:T(8,128)(2,1)}, u32[]{:S(2)}, u32[]{:S(2)}) collective-permute-start(bf16[272,512]{1,0:T(8,128)(2,1)} %get-tuple-element.15), channel_id=1, source_target_pairs={{0,64},{4,68},{8,72},{12,76},{16,80},{20,84},{24,88},{28,92},{32,9... | collective-permute-start | bytes 835592 | tf_op jit(solution)/shard_map/ppermute | solution.py:478
  122.5 18.0 %collective-permute-start.19 = (bf16[272,512]{1,0:T(8,128)(2,1)}, bf16[272,512]{1,0:T(8,128)(2,1)}, u32[]{:S(2)}, u32[]{:S(2)}) collective-permute-start(bf16[272,512]{1,0:T(8,128)(2,1)} %get-tuple-element.16), channel_id=1, source_target_pairs={{0,96},{4,100},{8,104},{12,108},{16,112},{20,116},{24,120},{28,124... | collective-permute-start | bytes 835592 | tf_op jit(solution)/shard_map/ppermute | solution.py:478
  145.2 38.8 %all-to-all-start.1 = ((bf16[32,16,2048]{2,1,0:T(8,128)(2,1)}), bf16[32,16,2048]{2,1,0:T(8,128)(2,1)S(1)}, u32[]{:S(2)}, u32[]{:S(2)}) async-start(bf16[32,16,2048]{2,1,0:T(8,128)(2,1)} %bitcast.18), calls=%async_computation.2 | async-start | bytes 4194304 | tf_op jit(solution)/shard_map/all_to_all | solution.py:512
  184.7 13.0 %collective-permute-start.20 = (bf16[128,2048]{1,0:T(8,128)(2,1)S(1)}, bf16[128,2048]{1,0:T(8,128)(2,1)S(1)}, u32[]{:S(2)}, u32[]{:S(2)}) collective-permute-start(bf16[128,2048]{1,0:T(8,128)(2,1)S(1)} %fusion.2), channel_id=1, source_target_pairs={{0,1},{1,0},{2,3},{3,2},{4,5},{5,4},{6,7},{7,6},{8,9},{9,8},{10,11... | collective-permute-start | bytes 1572872 | tf_op jit(solution)/shard_map/ppermute | solution.py:538
  (16 other events, 108.3 us)
Sparse Core Ops, SparseCore 0:
  16.3 26.6 all-gather.1
  145.3 33.0 reduce-scatter.1

commit v6 on v5

--- a/solution.py
+++ b/solution.py
@@ -1,4 +1,3 @@
-import functools
 import math
 import jax
 import jax.numpy as jnp
@@ -310,109 +309,146 @@
     )(gate, up, down)
 
 
-def expert_kernel(count, joins, *refs):
-    holds, x_hbm, pieces, twins = refs[0], refs[1], refs[2 : 2 + count], refs[2 + count : 2 + 2 * count]
-    refs = refs[2 + 2 * count :]
-    if joins:
-        part_hbm, refs = refs[0], refs[1:]
-    out_hbm, x_ref, held, hidden, out, sems = refs[:6]
-    ff = held.shape[2] // 3
-    copies = [pltpu.make_async_copy(x_hbm, x_ref, sems.at[0])]
-    copies += [pltpu.make_async_copy(p, held.at[i], sems.at[1 + i]) for i, p in enumerate(pieces)]
-    copies[0].start()
-
+def fetch(holds, held, other, dst, sem):
     @pl.when(holds[0] == 1)
     def _():
-        for i in range(count):
-            copies[1 + i].start()
+        pltpu.make_async_copy(held, dst, sem).start()
 
     @pl.when(holds[0] == 0)
     def _():
-        for i in range(count):
-            pltpu.make_async_copy(twins[i], held.at[i], sems.at[1 + i]).start()
-
-    if joins:
-        part = refs[6]
-        copies.append(pltpu.make_async_copy(part_hbm, part, sems.at[1 + count]))
-        copies[1 + count].start()
-    copies[0].wait()
-    for i in range(count):
-        copies[1 + i].wait()
-        for r in range(0, x_ref.shape[0], 256):
-            lines = slice(r, r + 256)
-            pre = jnp.dot(x_ref[lines, :], held[i, :, : 2 * ff], preferred_element_type=jnp.float32)
-            gated, lifted = pre[:, :ff], pre[:, ff:]
-            hidden[lines, i * ff : (i + 1) * ff] = (gated * jax.nn.sigmoid(gated) * lifted).astype(
-                jnp.bfloat16
-            )
-    if joins:
-        copies[1 + count].wait()
+        pltpu.make_async_copy(other, dst, sem).start()
+
+    return pltpu.make_async_copy(held, dst, sem)
+
+
+def gate_lines(x_ref, piece, hidden, first):
+    ff = piece.shape[1] // 2
+    for r in range(0, x_ref.shape[0], 256):
+        lines = slice(r, r + 256)
+        pre = jnp.dot(x_ref[lines, :], piece[...], preferred_element_type=jnp.float32)
+        gated, lifted = pre[:, :ff], pre[:, ff:]
+        hidden[lines, first : first + ff] = (gated * jax.nn.sigmoid(gated) * lifted).astype(jnp.bfloat16)
+
+
+def early_kernel(
+    holds, xa_hbm, xb_hbm, held0, held1, other0, other1, ha_ref, hb_ref, xa, xb, both, sems
+):
+    ff = both.shape[2] // 2
+    rows = [
+        pltpu.make_async_copy(src, dst, sems.at[k])
+        for k, (src, dst) in enumerate(((xa_hbm, xa), (xb_hbm, xb)))
+    ]
+    for c in rows:
+        c.start()
+    copies = [
+        fetch(holds, a.at[:, : 2 * ff], b.at[:, : 2 * ff], both.at[i], sems.at[2 + i])
+        for i, (a, b) in enumerate(((held0, other0), (held1, other1)))
+    ]
+    for c in rows:
+        c.wait()
+    for i, c in enumerate(copies):
+        c.wait()
+        gate_lines(xa, both.at[i], ha_ref, i * ff)
+        gate_lines(xb, both.at[i], hb_ref, i * ff)
+
+
+def early(holds, xa, xb, pieces):
+    rows, width = xa.shape
+    ff = pieces[0][0].shape[1] // 3
+    shape = jax.ShapeDtypeStruct((rows, 2 * ff), jnp.bfloat16)
+    return pl.pallas_call(
+        early_kernel,
+        out_shape=[shape] * 2,
+        in_specs=[pl.BlockSpec(memory_space=pltpu.SMEM)] + [pl.BlockSpec(memory_space=pltpu.HBM)] * 6,
+        out_specs=[pl.BlockSpec(memory_space=pltpu.VMEM)] * 2,
+        scratch_shapes=[
+            pltpu.VMEM((rows, width), jnp.bfloat16),
+            pltpu.VMEM((rows, width), jnp.bfloat16),
+            pltpu.VMEM((2, width, 2 * ff), jnp.bfloat16),
+            pltpu.SemaphoreType.DMA((4,)),
+        ],
+        cost_estimate=pl.CostEstimate(
+            flops=16 * rows * width * ff, bytes_accessed=16 * width * ff, transcendentals=4 * rows * ff
+        ),
+    )(holds, xa, xb, pieces[0][0], pieces[1][0], pieces[0][1], pieces[1][1])
+
+
+def late_kernel(
+    holds, x_hbm, hid_hbm, h0, h1, h2, h3, o0, o1, o2, o3, out_hbm, x_ref, both, down, hidden, out, sems
+):
+    ff = both.shape[2] // 2
+    rows = [
+        pltpu.make_async_copy(x_hbm, x_ref, sems.at[0]),
+        pltpu.make_async_copy(hid_hbm, hidden.at[:, : 2 * ff], sems.at[1]),
+    ]
+    for c in rows:
+        c.start()
+    gates = [
+        fetch(holds, a.at[:, : 2 * ff], b.at[:, : 2 * ff], both.at[i], sems.at[2 + i])
+        for i, (a, b) in enumerate(((h2, o2), (h3, o3)))
+    ]
+    downs = [
+        fetch(holds, a.at[:, 2 * ff :], b.at[:, 2 * ff :], down.at[i], sems.at[4 + i])
+        for i, (a, b) in enumerate(((h0, o0), (h1, o1), (h2, o2), (h3, o3)))
+    ]
+    rows[0].wait()
+    rows[1].wait()
+    for i, c in enumerate(gates):
+        c.wait()
+        gate_lines(x_ref, both.at[i], hidden, (2 + i) * ff)
+    for c in downs:
+        c.wait()
     stores = []
     for n, cols in enumerate(column_tiles(out.shape[1])):
         weights = jnp.concatenate(
             [
-                jnp.concatenate(
-                    [held[i, b * ff : (b + 1) * ff, 2 * ff :] for b in range(4 * n, 4 * n + 4)], axis=1
-                )
-                for i in range(count)
+                jnp.concatenate([down[i, b * ff : (b + 1) * ff, :] for b in range(4 * n, 4 * n + 4)], axis=1)
+                for i in range(4)
             ],
             axis=0,
         )
-        total = jnp.dot(hidden[...], weights, preferred_element_type=jnp.float32)
-        if joins:
-            total = total + part[:, cols]
-        out[:, cols] = total.astype(out.dtype)
-        stores.append(
-            pltpu.make_async_copy(out.at[:, cols], out_hbm.at[:, cols], sems.at[2 + count + n])
-        )
+        out[:, cols] = jnp.dot(hidden[...], weights, preferred_element_type=jnp.float32).astype(out.dtype)
+        stores.append(pltpu.make_async_copy(out.at[:, cols], out_hbm.at[:, cols], sems.at[8 + n]))
         stores[-1].start()
     for c in stores:
         c.wait()
 
 
-def expert_parts(holds, x, pieces, part, out_type):
+def late(holds, x, hid, pieces):
     rows, width = x.shape
-    count, ff = len(pieces), pieces[0][0].shape[1] // 3
-    joined = [] if part is None else [part]
+    ff = pieces[0][0].shape[1] // 3
     return pl.pallas_call(
-        functools.partial(expert_kernel, count, part is not None),
-        out_shape=jax.ShapeDtypeStruct((rows, width), out_type),
-        in_specs=[pl.BlockSpec(memory_space=pltpu.SMEM)]
-        + [pl.BlockSpec(memory_space=pltpu.HBM)] * (1 + 2 * count + len(joined)),
+        late_kernel,
+        out_shape=jax.ShapeDtypeStruct((rows, width), jnp.bfloat16),
+        in_specs=[pl.BlockSpec(memory_space=pltpu.SMEM)] + [pl.BlockSpec(memory_space=pltpu.HBM)] * 10,
         out_specs=pl.BlockSpec(memory_space=pltpu.HBM),
         scratch_shapes=[
             pltpu.VMEM((rows, width), jnp.bfloat16),
-            pltpu.VMEM((count, width, 3 * ff), jnp.bfloat16),
-            pltpu.VMEM((rows, count * ff), jnp.bfloat16),
-            pltpu.VMEM((rows, width), out_type),
-            pltpu.SemaphoreType.DMA((2 + count + len(column_tiles(width)),)),
-        ]
-        + [pltpu.VMEM((rows, width), jnp.float32)] * len(joined),
+            pltpu.VMEM((2, width, 2 * ff), jnp.bfloat16),
+            pltpu.VMEM((4, width, ff), jnp.bfloat16),
+            pltpu.VMEM((rows, 4 * ff), jnp.bfloat16),
+            pltpu.VMEM((rows, width), jnp.bfloat16),
+            pltpu.SemaphoreType.DMA((8 + len(column_tiles(width)),)),
+        ],
         cost_estimate=pl.CostEstimate(
-            flops=count * 6 * rows * width * ff,
-            bytes_accessed=count * 6 * width * ff,
-            transcendentals=rows * count * ff,
+            flops=16 * rows * width * ff, bytes_accessed=20 * width * ff, transcendentals=2 * rows * ff
         ),
-    )(holds, x, *[p[0] for p in pieces], *[p[1] for p in pieces], *joined)
-
-
-def shift(x, by, relays=False):
+    )(holds, x, hid, *[p[0] for p in pieces], *[p[1] for p in pieces])
+
+
+def shift(x, by, sources=(0, 1)):
     eps, tps = lax.axis_size("ep"), lax.axis_size("tp")
     pairs = [
-        (e * tps + t, e * tps + (t + by) % tps)
+        (e * tps + t, (e ^ 1) * tps + (t + by) % tps)
         for e in range(eps)
         for t in range(tps)
-        if not relays or t % 2 != e % 2
+        if (e + t) % 2 in sources
     ]
     return lax.ppermute(x, ("ep", "tp"), pairs)
 
 
-def to_sibling(x):
-    eps, tps = lax.axis_size("ep"), lax.axis_size("tp")
-    pairs = [
-        (e * tps + t, (e ^ 1) * tps + t) for e in range(eps) for t in range(tps) if t % 2 == e % 2
-    ]
-    return lax.ppermute(x, ("ep", "tp"), pairs)
+def swap_cores(x):
+    return lax.ppermute(x, "ep", [(e, e ^ 1) for e in range(lax.axis_size("ep"))])
 
 
 def rms_scale(row_block, scale_gain):
@@ -452,14 +488,10 @@
 
     one, two = fold(expert_gate[0], expert_up[0], expert_down[0])
     east, west = shift(one, 1), shift(two, -1)
-    east_more, west_more = shift(two, 1, True), shift(one, -1, True)
-    far_east, far_west = shift(east, 1, True), shift(west, -1, True)
-    mine = {
-        "one": one, "two": two, "east": east, "west": west,
-        "east_more": east_more, "west_more": west_more, "far_east": far_east, "far_west": far_west,
-    }
+    east_more, west_more = shift(two, 1, (1,)), shift(one, -1, (1,))
+    far_east, far_west = shift(east, 1, (0,)), shift(west, -1, (0,))
     holds = (ep_index % 2 == tp_index % 2).astype(jnp.int32).reshape(1)
-    pieces = [(a, to_sibling(a)) for a in mine.values()]
+    pieces = [(one, east), (two, west), (far_east, east_more), (far_west, west_more)]
 
     running = jnp.cumsum(jax.nn.log_sigmoid(forget_logit), axis=1)
     packed = pack(key_rows, value_rows, running)
@@ -504,14 +536,19 @@
     arrived = lax.all_to_all(outgoing, "ep", split_axis=0, concat_axis=0, tiled=True)
     arrived = arrived.reshape(slots, width_model)
 
-    part = expert_parts(holds, arrived, pieces[:6], None, jnp.float32)
-    results = expert_parts(holds, arrived, pieces[6:], part, jnp.bfloat16)
-    results, told[0] = lax.optimization_barrier((results, told[0]))
+    twin_rows = swap_cores(arrived)
+    own_hidden, twin_hidden = early(holds, arrived, twin_rows, pieces[:2])
+    for_twin = late(holds, twin_rows, twin_hidden, pieces)
+    from_twin = swap_cores(for_twin)
+    results = late(holds, arrived, own_hidden, pieces)
+    returned = []
+    for k in range(2):
+        cols = slice(k * width_model // 2, (k + 1) * width_model // 2)
+        summed = results[:, cols].astype(jnp.float32) + from_twin[:, cols].astype(jnp.float32)
+        summed = summed.astype(jnp.bfloat16).reshape(experts, capacity, width_model // 2)
+        back = lax.all_to_all(summed, "ep", split_axis=0, concat_axis=0, tiled=True)
+        returned.append(back.reshape(slots, width_model // 2))
     mixer_term = merge(place, told, out_weight)
-    results = results.reshape(experts, capacity, width_model)
-    returned = lax.all_to_all(results, "ep", split_axis=0, concat_axis=0, tiled=True)
-    returned = returned.reshape(slots, width_model)
-
     mixer_summed = lax.psum_scatter(mixer_term, "tp", scatter_dimension=0, tiled=True)
     mixer_out = rms_scale(mixer_summed, out_gain).astype(jnp.bfloat16)
 
@@ -528,17 +565,19 @@
         column == target[:, 1:], shares[:, 1:], 0.0
     )
 
-    def combine(block):
+    def combine(block, back):
         lines = lax.dynamic_slice_in_dim(weight, block * own_rows, own_rows, 0)
         high = lax.reduce_precision(lines, 8, 7)
         both = jnp.concatenate([high, lines - high], axis=1).astype(jnp.bfloat16)
-        twice = jnp.concatenate([returned, returned], axis=0)
+        twice = jnp.concatenate([back, back], axis=0)
         return jnp.dot(both, twice, preferred_element_type=jnp.float32)
 
-    other = lax.ppermute(
-        combine(1 - parity).astype(jnp.bfloat16), "tp", [(t, t ^ 1) for t in range(tp_count)]
-    )
-    moe_out = combine(parity) + other.astype(jnp.float32)
+    halves = []
+    for back in returned:
+        pairs = [(t, t ^ 1) for t in range(tp_count)]
+        other = lax.ppermute(combine(1 - parity, back).astype(jnp.bfloat16), "tp", pairs)
+        halves.append(combine(parity, back) + other.astype(jnp.float32))
+    moe_out = jnp.concatenate(halves, axis=1)
     return (mixer_out, moe_out.astype(jnp.bfloat16))
 
 

time: 211 us -> 239 us (1.13)
  waiting for transfers between devices: 72.9 us -> 100 us
  other arithmetic: 7.23 us -> 17.4 us
  starting transfers between devices: 60.9 us -> 52 us
    ppermute x3, waiting for transfers between devices: 28.2 us -> 0.01 us  [inner(): asked.append(lax.ppermute(queries, 'ep', pairs))]
    all_to_all x1, waiting for transfers between devices: 0.01 us -> 26.8 us  [inner(): lax.all_to_all(outgoing, 'ep', split_axis=0, concat_axis=0, tiled=True)]
    ppermute x6, waiting for transfers between devices: 5.18 us -> 24.4 us  [shift(): return lax.ppermute(x, ('ep', 'tp'), pairs)]
    ppermute x9 -> x4, starting transfers between devices: 23.4 us -> 5.8 us  [the longest x2 5.63 us: swap_cores(): lax.ppermute(x, 'ep', [(e, e ^ 1) for e in range(lax.axis_size('ep'))])]
    ppermute x3, waiting for transfers between devices: 0.01 us -> 8.63 us  [inner(): told.append(lax.ppermute(answers[d], 'ep', pairs))]
    all_to_all x1 -> x2, starting transfers between devices: 8.75 us -> 14.9 us  [inner(): back = lax.all_to_all(summed, 'ep', split_axis=0, concat_axis=0, tiled=True)]
    ppermute x6, starting transfers between devices: 8.46 us -> 13.4 us  [shift(): return lax.ppermute(x, ('ep', 'tp'), pairs)]
    convert_element_type x0 -> x1, other arithmetic: none -> 3.83 us  [inner(): summed.astype(jnp.bfloat16).reshape(experts, capacity, width_model // 2)]
  transfers between devices with their start and end apart: 25 -> 21, of which waited for: 6 -> 8; matrix products, arithmetic and copies ran while one was open for 5% -> 5% of each run, Pallas kernels for 18% -> 20%
where the time goes in v6:
time: 239 us; the launch traced here: 238 us
  waiting for transfers between devices  100 us (42%)
  starting transfers between devices  52 us (22%)
  Pallas kernels  47.9 us (20%)
  other arithmetic  17.4 us (7%)
  between operations  14.6 us (6%)
  matrix products  4.85 us (2%)
    all_to_all x2, waiting for transfers between devices, inner(): back = lax.all_to_all(summed, 'ep', split_axis=0, concat_axis=0, tiled=True)  32.4 us
    all_to_all x1, waiting for transfers between devices, inner(): lax.all_to_all(outgoing, 'ep', split_axis=0, concat_axis=0, tiled=True)  26.8 us
    ppermute x6, waiting for transfers between devices, shift(): return lax.ppermute(x, ('ep', 'tp'), pairs)  24.4 us
    pallas_call x1, Pallas kernels, attend(): pl.pallas_call(attend_kernel, out_shape=[jax.ShapeDtypeStruct((2 * DH + 1...  23.8 us
    all_to_all x2, starting transfers between devices, inner(): back = lax.all_to_all(summed, 'ep', split_axis=0, concat_axis=0, tiled=True)  14.9 us
    ppermute x6, starting transfers between devices, shift(): return lax.ppermute(x, ('ep', 'tp'), pairs)  13.4 us
    pallas_call x2, Pallas kernels, late(): pl.pallas_call(late_kernel, out_shape=jax.ShapeDtypeStruct((rows, width),...  11.2 us
    ppermute x3, waiting for transfers between devices, inner(): told.append(lax.ppermute(answers[d], 'ep', pairs))  8.63 us
  transfers between devices with their start and end apart: 21, of which 8 were waited for; matrix products, arithmetic and copies ran while one was open for 5% of the time, Pallas kernels for 20%

profile of v6, /device:TPU:0, one launch (start us, length us, event | category | flops | bytes accessed | tf_op | source)
XLA Modules:
  0.0 237.5 jit_solution(15025164850282207967)
XLA Ops:
  7.2 1.5 fusion
  11.9 1.6 fusion.2
  13.4 2.0 convolution_convert_fusion
  15.5 8.6 %all-to-all-start = ((bf16[32,16,2048]{2,1,0:T(8,128)(2,1)}), bf16[32,16,2048]{2,1,0:T(8,128)(2,1)S(1)}, u32[]{:S(2)}, u32[]{:S(2)}) async-start(bf16[32,16,2048]{2,1,0:T(8,128)(2,1)} %bitcast.34), calls=%async_computation.1 | async-start | bytes 4194304 | tf_op jit(solution)/shard_map/all_to_all | solution.py:536
  25.5 1.6 pad_maximum_fusion.11
  27.2 3.3 %shard_map.160 = (bf16[2048,384]{1,0:T(8,128)(2,1)}, bf16[2048,384]{1,0:T(8,128)(2,1)}) custom-call(bf16[2048,256]{1,0:T(8,128)(2,1)} %bitcast.35, bf16[2048,256]{1,0:T(8,128)(2,1)} %bitcast.36, bf16[256,2048]{1,0:T(8,128)(2,1)} %bitcast.37), custom_call_target="tpu_custom_call" | custom-call | flops 1000000 | bytes 6291456 | tf_op jit(solution)/shard_map/pallas_call | solution.py:297
  30.5 1.4 collective-permute-start.7
  31.9 1.6 collective-permute-start.8
  33.5 26.8 %all-to-all-done = bf16[32,16,2048]{2,1,0:T(8,128)(2,1)S(1)} async-done(((bf16[32,16,2048]{2,1,0:T(8,128)(2,1)}), bf16[32,16,2048]{2,1,0:T(8,128)(2,1)S(1)}, u32[]{:S(2)}, u32[]{:S(2)}) %all-to-all-start) | async-done | bytes 2097184 | tf_op jit(solution)/shard_map/all_to_all | solution.py:536
  60.3 1.9 collective-permute-start.12
  62.2 1.8 collective-permute-start.11
  64.0 4.4 %collective-permute-done.7.other0.o0 = bf16[2048,384]{1,0:T(8,128)(2,1)} collective-permute-done((bf16[2048,384]{1,0:T(8,128)(2,1)}, bf16[2048,384]{1,0:T(8,128)(2,1)}, u32[]{:S(2)}, u32[]{:S(2)}) %collective-permute-start.7) | collective-permute-done | bytes 1572896 | tf_op jit(solution)/shard_map/ppermute | solution.py:447
  68.3 2.4 collective-permute-start.9
  70.7 4.4 %collective-permute-start.10 = (bf16[2048,384]{1,0:T(8,128)(2,1)}, bf16[2048,384]{1,0:T(8,128)(2,1)}, u32[]{:S(2)}, u32[]{:S(2)}) collective-permute-start(bf16[2048,384]{1,0:T(8,128)(2,1)} %collective-permute-done.8.other1.o1), channel_id=1, source_target_pairs={{0,7},{2,5},{5,0},{7,2},{8,15},{10,13},{13,8},{15,10},{16,23},{18,... | collective-permute-start | bytes 4718600 | tf_op jit(solution)/shard_map/ppermute | solution.py:447
  79.7 5.7 %shard_map.161 = (bf16[512,256]{1,0:T(8,128)(2,1)}, bf16[512,256]{1,0:T(8,128)(2,1)}) custom-call(s32[1]{0:T(128)} %bitcast.12.holds, bf16[512,2048]{1,0:T(8,128)(2,1)} %bitcast.32, bf16[512,2048]{1,0:T(8,128)(2,1)} %collective-permute-done.6.xb_hbm.x_hbm, bf16[2048,384]{1,0:T(8,128)(2,1)} %get-tuple-element.14.held0.h0, ...), custom_call_target="tpu_custom_call" | custom-call | flops 2147483648 | bytes 4194304 | tf_op jit(solution)/shard_map/pallas_call | solution.py:359
  85.5 20.0 %collective-permute-done.9.h2 = bf16[2048,384]{1,0:T(8,128)(2,1)} collective-permute-done((bf16[2048,384]{1,0:T(8,128)(2,1)}, bf16[2048,384]{1,0:T(8,128)(2,1)}, u32[]{:S(2)}, u32[]{:S(2)}) %collective-permute-start.9) | collective-permute-done | bytes 1572896 | tf_op jit(solution)/shard_map/ppermute | solution.py:447
  105.5 5.6 %shard_map.163 = bf16[512,2048]{1,0:T(8,128)(2,1)} custom-call(s32[1]{0:T(128)} %bitcast.12.holds, bf16[512,2048]{1,0:T(8,128)(2,1)} %collective-permute-done.6.xb_hbm.x_hbm, bf16[512,256]{1,0:T(8,128)(2,1)} %get-tuple-element.17.hid_hbm, bf16[2048,384]{1,0:T(8,128)(2,1)} %get-tuple-element.14.held0.h0, bf16[2048,384]{1,0:T(8,128)(2,1)} %get-tuple-element.15.held1.h1, ...), custom_call_target="tpu_custom_call" | custom-call | flops 2147483648 | bytes 5242880 | tf_op jit(solution)/shard_map/pallas_call | solution.py:420
  111.1 5.6 %collective-permute-start.13 = (bf16[512,2048]{1,0:T(8,128)(2,1)}, bf16[512,2048]{1,0:T(8,128)(2,1)S(1)}, u32[]{:S(2)}, u32[]{:S(2)}) collective-permute-start(bf16[512,2048]{1,0:T(8,128)(2,1)} %shard_map.163), channel_id=1, source_target_pairs={{0,4},{4,0},{8,12},{12,8},{16,20},{20,16},{24,28},{28,24},{32,36},... | collective-permute-start | bytes 6291464 | tf_op jit(solution)/shard_map/ppermute | solution.py:451
  116.8 23.8 %shard_map.158 = (bf16[272,512]{1,0:T(8,128)(2,1)}, bf16[272,512]{1,0:T(8,128)(2,1)}, bf16[272,512]{1,0:T(8,128)(2,1)}, bf16[272,512]{1,0:T(8,128)(2,1)}) custom-call(s32[2]{0:T(128)} %pad_add_fusion.pos_ref, bf16[512,256]{1,0:T(8,128)(2,1)} %q0.1, bf16[512,256]{1,0:T(8,128)(2,1)} %collective-permute-done.q1, bf16[512,256]{1,0:T(8,128)(2,1)} %collective-permute-done.1.q2, ...), custom_call_target="tpu_custom_call" | custom-call | flops 8999999488 | bytes 4000000 | tf_op jit(solution)/shard_map/pallas_call | solution.py:170
  141.8 2.0 collective-permute-start.4
  143.9 2.0 collective-permute-start.5
  145.8 3.3 %collective-permute-done.3.p1 = bf16[272,512]{1,0:T(8,128)(2,1)S(1)} collective-permute-done((bf16[272,512]{1,0:T(8,128)(2,1)}, bf16[272,512]{1,0:T(8,128)(2,1)S(1)}, u32[]{:S(2)}, u32[]{:S(2)}) %collective-permute-start.3) | collective-permute-done | bytes 278560 | tf_op jit(solution)/shard_map/ppermute | solution.py:510
  149.2 5.3 %collective-permute-done.4.p2 = bf16[272,512]{1,0:T(8,128)(2,1)} collective-permute-done((bf16[272,512]{1,0:T(8,128)(2,1)}, bf16[272,512]{1,0:T(8,128)(2,1)}, u32[]{:S(2)}, u32[]{:S(2)}) %collective-permute-start.4) | collective-permute-done | bytes 278560 | tf_op jit(solution)/shard_map/ppermute | solution.py:510
  154.5 3.9 %shard_map.159 = bf16[512,2048]{1,0:T(8,128)(2,1)} custom-call(s32[2]{0:T(128)} %pad_add_fusion.pos_ref, bf16[272,512]{1,0:T(8,128)(2,1)} %get-tuple-element.10.p0, bf16[272,512]{1,0:T(8,128)(2,1)} %copy-done.2, bf16[272,512]{1,0:T(8,128)(2,1)} %collective-permute-done.4.p2, bf16[272,512]{1,0:T(8,128)(2,1)} %collective-permute-done.5.p3, bf16[256,2048]{1,0:T(8,128)(2,1)} %w_ref.1), custom_call_target="tpu_custom_call" | custom-call | flops 536870912 | bytes 4000000 | tf_op jit(solution)/shard_map/pallas_call | solution.py:237
  158.4 5.6 %shard_map.162 = bf16[512,2048]{1,0:T(8,128)(2,1)} custom-call(s32[1]{0:T(128)} %bitcast.12.holds, bf16[512,2048]{1,0:T(8,128)(2,1)} %bitcast.33, bf16[512,256]{1,0:T(8,128)(2,1)} %get-tuple-element.16.hid_hbm, bf16[2048,384]{1,0:T(8,128)(2,1)} %get-tuple-element.14.held0.h0, bf16[2048,384]{1,0:T(8,128)(2,1)} %get-tuple-element.15.held1.h1, ...), custom_call_target="tpu_custom_call" | custom-call | flops 2147483648 | bytes 5242880 | tf_op jit(solution)/shard_map/pallas_call | solution.py:420
  164.1 3.8 %add_convert_fusion.1 = (bf16[512,1024]{1,0:T(8,128)(2,1)}, bf16[512,1024]{1,0:T(8,128)(2,1)}) fusion(bf16[512,2048]{1,0:T(8,128)(2,1)S(1)} %collective-permute-done.13, bf16[512,2048]{1,0:T(8,128)(2,1)} %shard_map.162), kind=kLoop, calls=%fused_computation.9 | loop fusion | flops 4194304 | bytes 6291456 | tf_op jit(solution)/shard_map/convert_element_type | solution.py:548
  167.9 11.0 %all-to-all-start.2 = ((bf16[32,16,1024]{2,1,0:T(8,128)(2,1)}), bf16[32,16,1024]{2,1,0:T(8,128)(2,1)S(1)}, u32[]{:S(2)}, u32[]{:S(2)}) async-start(bf16[32,16,1024]{2,1,0:T(8,128)(2,1)} %bitcast.20), calls=%async_computation.3 | async-start | bytes 2097152 | tf_op jit(solution)/shard_map/all_to_all | solution.py:549
  180.0 16.1 %all-to-all-done.2 = bf16[32,16,1024]{2,1,0:T(8,128)(2,1)S(1)} async-done(((bf16[32,16,1024]{2,1,0:T(8,128)(2,1)}), bf16[32,16,1024]{2,1,0:T(8,128)(2,1)S(1)}, u32[]{:S(2)}, u32[]{:S(2)}) %all-to-all-start.2) | async-done | bytes 1048608 | tf_op jit(solution)/shard_map/all_to_all | solution.py:549
  196.1 3.9 %all-to-all-start.1 = ((bf16[32,16,1024]{2,1,0:T(8,128)(2,1)}), bf16[32,16,1024]{2,1,0:T(8,128)(2,1)S(1)}, u32[]{:S(2)}, u32[]{:S(2)}) async-start(bf16[32,16,1024]{2,1,0:T(8,128)(2,1)} %bitcast.18), calls=%async_computation.2 | async-start | bytes 2097152 | tf_op jit(solution)/shard_map/all_to_all | solution.py:549
  201.0 16.3 %all-to-all-done.1 = bf16[32,16,1024]{2,1,0:T(8,128)(2,1)S(1)} async-done(((bf16[32,16,1024]{2,1,0:T(8,128)(2,1)}), bf16[32,16,1024]{2,1,0:T(8,128)(2,1)S(1)}, u32[]{:S(2)}, u32[]{:S(2)}) %all-to-all-start.1) | async-done | bytes 1048608 | tf_op jit(solution)/shard_map/all_to_all | solution.py:549
  218.3 7.8 %collective-permute-done.14 = bf16[128,1024]{1,0:T(8,128)(2,1)S(1)} collective-permute-done((bf16[128,1024]{1,0:T(8,128)(2,1)S(1)}, bf16[128,1024]{1,0:T(8,128)(2,1)S(1)}, u32[]{:S(2)}, u32[]{:S(2)}) %collective-permute-start.14) | collective-permute-done | bytes 262176 | tf_op jit(solution)/shard_map/ppermute | solution.py:578
  228.7 2.0 fusion.11
  (95 shorter events, 15.7 us)
Async XLA Ops:
  7.2 171.8 %copy-start = (bf16[2048,32]{0,1:T(8,128)(2,1)S(1)}, bf16[2048,32]{0,1:T(8,128)(2,1)}, u32[]{:S(2)}) copy-start(bf16[2048,32]{0,1:T(8,128)(2,1)} %param.24) | copy-start | bytes 393220
  15.4 8.7 %copy-start.12 = (f32[2,512]{1,0:T(2,128)S(1)}, f32[2,512]{1,0:T(2,128)}, u32[]{:S(2)}) copy-start(f32[2,512]{1,0:T(2,128)} %param.18) | copy-start | bytes 12292
  15.4 9.9 %copy-start.3 = (bf16[512,128]{1,0:T(8,128)(2,1)S(1)}, bf16[512,128]{1,0:T(8,128)(2,1)}, u32[]{:S(2)}) copy-start(bf16[512,128]{1,0:T(8,128)(2,1)} %param.17) | copy-start | bytes 393220
  15.5 44.9 %all-to-all-start = ((bf16[32,16,2048]{2,1,0:T(8,128)(2,1)}), bf16[32,16,2048]{2,1,0:T(8,128)(2,1)S(1)}, u32[]{:S(2)}, u32[]{:S(2)}) async-start(bf16[32,16,2048]{2,1,0:T(8,128)(2,1)} %bitcast.34), calls=%async_computation.1 | async-start | bytes 4194304 | tf_op jit(solution)/shard_map/all_to_all | solution.py:536
  24.1 92.7 %all-gather.2.cloned.1.call-start = ((), (), s32[]{:S(2)}) async-start(), calls=%async_computation.4 | async-start | bytes 2433024 | tf_op jit(solution)/shard_map/all_gather | solution.py:499
  27.1 48.7 %copy-start.14 = (bf16[512,256]{1,0:T(8,128)(2,1)S(1)}, bf16[512,256]{1,0:T(8,128)(2,1)}, u32[]{:S(2)}) copy-start(bf16[512,256]{1,0:T(8,128)(2,1)} %q0.1) | copy-start | bytes 786436
  27.1 200.3 %reduce-scatter.2.cloned.1.call-start = ((), (), s32[]{:S(2)}) async-start(), calls=%async_computation.5 | async-start | bytes 2621440 | tf_op jit(solution)/shard_map/reduce_scatter | solution.py:552
  30.5 37.8 %collective-permute-start.7 = (bf16[2048,384]{1,0:T(8,128)(2,1)}, bf16[2048,384]{1,0:T(8,128)(2,1)}, u32[]{:S(2)}, u32[]{:S(2)}) collective-permute-start(bf16[2048,384]{1,0:T(8,128)(2,1)} %get-tuple-element.14.held0.h0), channel_id=1, source_target_pairs={{0,5},{1,6},{2,7},{3,4},{4,1},{5,2},{6,3},{7,0},{8,13},{9,14},{10,... | collective-permute-start | bytes 4718600 | tf_op jit(solution)/shard_map/ppermute | solution.py:447
  31.9 38.8 %collective-permute-start.8 = (bf16[2048,384]{1,0:T(8,128)(2,1)}, bf16[2048,384]{1,0:T(8,128)(2,1)}, u32[]{:S(2)}, u32[]{:S(2)}) collective-permute-start(bf16[2048,384]{1,0:T(8,128)(2,1)} %get-tuple-element.15.held1.h1), channel_id=1, source_target_pairs={{0,7},{1,4},{2,5},{3,6},{4,3},{5,0},{6,1},{7,2},{8,15},{9,12},{10,... | collective-permute-start | bytes 4718600 | tf_op jit(solution)/shard_map/ppermute | solution.py:447
  60.3 19.4 %copy-start.1 = (bf16[32,16,2048]{2,1,0:T(8,128)(2,1)}, bf16[32,16,2048]{2,1,0:T(8,128)(2,1)S(1)}, u32[]{:S(2)}) copy-start(bf16[32,16,2048]{2,1,0:T(8,128)(2,1)S(1)} %all-to-all-done) | copy-start | bytes 6291460
  60.3 18.1 %collective-permute-start.6 = (bf16[512,2048]{1,0:T(8,128)(2,1)S(1)}, bf16[512,2048]{1,0:T(8,128)(2,1)}, u32[]{:S(2)}, u32[]{:S(2)}) collective-permute-start(bf16[512,2048]{1,0:T(8,128)(2,1)S(1)} %bitcast.31), channel_id=1, source_target_pairs={{0,4},{4,0},{8,12},{12,8},{16,20},{20,16},{24,28},{28,24},{32,36},... | collective-permute-start | bytes 6291464 | tf_op jit(solution)/shard_map/ppermute | solution.py:451
  60.3 15.5 %collective-permute-start.12 = (bf16[2048,384]{1,0:T(8,128)(2,1)}, bf16[2048,384]{1,0:T(8,128)(2,1)}, u32[]{:S(2)}, u32[]{:S(2)}) collective-permute-start(bf16[2048,384]{1,0:T(8,128)(2,1)} %get-tuple-element.14.held0.h0), channel_id=1, source_target_pairs={{1,4},{3,6},{4,3},{6,1},{9,12},{11,14},{12,11},{14,9},{17,20},{19,... | collective-permute-start | bytes 4718600 | tf_op jit(solution)/shard_map/ppermute | solution.py:447
  62.2 14.9 %collective-permute-start.11 = (bf16[2048,384]{1,0:T(8,128)(2,1)}, bf16[2048,384]{1,0:T(8,128)(2,1)}, u32[]{:S(2)}, u32[]{:S(2)}) collective-permute-start(bf16[2048,384]{1,0:T(8,128)(2,1)} %get-tuple-element.15.held1.h1), channel_id=1, source_target_pairs={{1,6},{3,4},{4,1},{6,3},{9,14},{11,12},{12,9},{14,11},{17,22},{19,... | collective-permute-start | bytes 4718600 | tf_op jit(solution)/shard_map/ppermute | solution.py:447
  68.3 37.2 %collective-permute-start.9 = (bf16[2048,384]{1,0:T(8,128)(2,1)}, bf16[2048,384]{1,0:T(8,128)(2,1)}, u32[]{:S(2)}, u32[]{:S(2)}) collective-permute-start(bf16[2048,384]{1,0:T(8,128)(2,1)} %collective-permute-done.7.other0.o0), channel_id=1, source_target_pairs={{0,5},{2,7},{5,2},{7,0},{8,13},{10,15},{13,10},{15,8},{16,21},{18,... | collective-permute-start | bytes 4718600 | tf_op jit(solution)/shard_map/ppermute | solution.py:447
  70.7 34.8 %collective-permute-start.10 = (bf16[2048,384]{1,0:T(8,128)(2,1)}, bf16[2048,384]{1,0:T(8,128)(2,1)}, u32[]{:S(2)}, u32[]{:S(2)}) collective-permute-start(bf16[2048,384]{1,0:T(8,128)(2,1)} %collective-permute-done.8.other1.o1), channel_id=1, source_target_pairs={{0,7},{2,5},{5,0},{7,2},{8,15},{10,13},{13,8},{15,10},{16,23},{18,... | collective-permute-start | bytes 4718600 | tf_op jit(solution)/shard_map/ppermute | solution.py:447
  75.8 40.9 %collective-permute-start.1 = (bf16[512,256]{1,0:T(8,128)(2,1)S(1)}, bf16[512,256]{1,0:T(8,128)(2,1)}, u32[]{:S(2)}, u32[]{:S(2)}) collective-permute-start(bf16[512,256]{1,0:T(8,128)(2,1)S(1)} %copy-done.14), channel_id=1, source_target_pairs={{64,0},{68,4},{72,8},{76,12},{80,16},{84,20},{88,24},{92,28},{96,3... | collective-permute-start | bytes 786440 | tf_op jit(solution)/shard_map/ppermute | solution.py:505
  77.1 39.6 %collective-permute-start = (bf16[512,256]{1,0:T(8,128)(2,1)S(1)}, bf16[512,256]{1,0:T(8,128)(2,1)}, u32[]{:S(2)}, u32[]{:S(2)}) collective-permute-start(bf16[512,256]{1,0:T(8,128)(2,1)S(1)} %copy-done.14), channel_id=1, source_target_pairs={{32,0},{36,4},{40,8},{44,12},{48,16},{52,20},{56,24},{60,28},{64,3... | collective-permute-start | bytes 786440 | tf_op jit(solution)/shard_map/ppermute | solution.py:505
  78.4 38.3 %collective-permute-start.2 = (bf16[512,256]{1,0:T(8,128)(2,1)S(1)}, bf16[512,256]{1,0:T(8,128)(2,1)}, u32[]{:S(2)}, u32[]{:S(2)}) collective-permute-start(bf16[512,256]{1,0:T(8,128)(2,1)S(1)} %copy-done.14), channel_id=1, source_target_pairs={{96,0},{100,4},{104,8},{108,12},{112,16},{116,20},{120,24},{124,28... | collective-permute-start | bytes 786440 | tf_op jit(solution)/shard_map/ppermute | solution.py:505
  111.1 53.0 %collective-permute-start.13 = (bf16[512,2048]{1,0:T(8,128)(2,1)}, bf16[512,2048]{1,0:T(8,128)(2,1)S(1)}, u32[]{:S(2)}, u32[]{:S(2)}) collective-permute-start(bf16[512,2048]{1,0:T(8,128)(2,1)} %shard_map.163), channel_id=1, source_target_pairs={{0,4},{4,0},{8,12},{12,8},{16,20},{20,16},{24,28},{28,24},{32,36},... | collective-permute-start | bytes 6291464 | tf_op jit(solution)/shard_map/ppermute | solution.py:451
  140.5 8.6 %collective-permute-start.3 = (bf16[272,512]{1,0:T(8,128)(2,1)}, bf16[272,512]{1,0:T(8,128)(2,1)S(1)}, u32[]{:S(2)}, u32[]{:S(2)}) collective-permute-start(bf16[272,512]{1,0:T(8,128)(2,1)} %get-tuple-element.11), channel_id=1, source_target_pairs={{0,32},{4,36},{8,40},{12,44},{16,48},{20,52},{24,56},{28,60},{32,6... | collective-permute-start | bytes 835592 | tf_op jit(solution)/shard_map/ppermute | solution.py:510
  141.8 12.6 %collective-permute-start.4 = (bf16[272,512]{1,0:T(8,128)(2,1)}, bf16[272,512]{1,0:T(8,128)(2,1)}, u32[]{:S(2)}, u32[]{:S(2)}) collective-permute-start(bf16[272,512]{1,0:T(8,128)(2,1)} %get-tuple-element.12), channel_id=1, source_target_pairs={{0,64},{4,68},{8,72},{12,76},{16,80},{20,84},{24,88},{28,92},{32,9... | collective-permute-start | bytes 835592 | tf_op jit(solution)/shard_map/ppermute | solution.py:510
  143.9 10.6 %collective-permute-start.5 = (bf16[272,512]{1,0:T(8,128)(2,1)}, bf16[272,512]{1,0:T(8,128)(2,1)}, u32[]{:S(2)}, u32[]{:S(2)}) collective-permute-start(bf16[272,512]{1,0:T(8,128)(2,1)} %get-tuple-element.13), channel_id=1, source_target_pairs={{0,96},{4,100},{8,104},{12,108},{16,112},{20,116},{24,120},{28,124... | collective-permute-start | bytes 835592 | tf_op jit(solution)/shard_map/ppermute | solution.py:510
  167.9 11.5 %copy-start.5 = (s32[256,2]{0,1:T(2,128)S(1)}, s32[256,2]{0,1:T(2,128)}, u32[]{:S(2)}) copy-start(s32[256,2]{0,1:T(2,128)} %copy-done.4) | copy-start | bytes 6148
  167.9 11.6 %copy-start.6 = (bf16[2048,4]{0,1:T(4,128)(2,1)S(1)}, bf16[2048,4]{0,1:T(4,128)(2,1)}, u32[]{:S(2)}) copy-start(bf16[2048,4]{0,1:T(4,128)(2,1)} %param.23) | copy-start | bytes 49156
  167.9 12.0 %copy-start.13 = (s32[256]{0:T(256)S(1)}, s32[256]{0:T(256)}, u32[]{:S(2)}) copy-start(s32[256]{0:T(256)} %get-tuple-element.21) | copy-start | bytes 3076
  167.9 28.2 %all-to-all-start.2 = ((bf16[32,16,1024]{2,1,0:T(8,128)(2,1)}), bf16[32,16,1024]{2,1,0:T(8,128)(2,1)S(1)}, u32[]{:S(2)}, u32[]{:S(2)}) async-start(bf16[32,16,1024]{2,1,0:T(8,128)(2,1)} %bitcast.20), calls=%async_computation.3 | async-start | bytes 2097152 | tf_op jit(solution)/shard_map/all_to_all | solution.py:549
  178.9 21.2 %copy-start.8 = (s32[256,1]{0,1:T(1,128)S(1)}, s32[256,1]{0,1:T(1,128)}, u32[]{:S(2)}) copy-start(s32[256,1]{0,1:T(1,128)} %copy-done.7) | copy-start | bytes 3076
  178.9 21.2 %copy-start.10 = (s32[256,1]{0,1:T(1,128)S(1)}, s32[256,1]{0,1:T(1,128)}, u32[]{:S(2)}) copy-start(s32[256,1]{0,1:T(1,128)} %copy-done.9) | copy-start | bytes 3076
  196.1 21.1 %all-to-all-start.1 = ((bf16[32,16,1024]{2,1,0:T(8,128)(2,1)}), bf16[32,16,1024]{2,1,0:T(8,128)(2,1)S(1)}, u32[]{:S(2)}, u32[]{:S(2)}) async-start(bf16[32,16,1024]{2,1,0:T(8,128)(2,1)} %bitcast.18), calls=%async_computation.2 | async-start | bytes 2097152 | tf_op jit(solution)/shard_map/all_to_all | solution.py:549
  200.9 16.9 %collective-permute-start.15 = (bf16[128,1024]{1,0:T(8,128)(2,1)S(1)}, bf16[128,1024]{1,0:T(8,128)(2,1)S(1)}, u32[]{:S(2)}, u32[]{:S(2)}) collective-permute-start(bf16[128,1024]{1,0:T(8,128)(2,1)S(1)} %fusion.8), channel_id=1, source_target_pairs={{0,1},{1,0},{2,3},{3,2},{4,5},{5,4},{6,7},{7,6},{8,9},{9,8},{10,11... | collective-permute-start | bytes 786440 | tf_op jit(solution)/shard_map/ppermute | solution.py:578
  217.7 8.4 %collective-permute-start.14 = (bf16[128,1024]{1,0:T(8,128)(2,1)S(1)}, bf16[128,1024]{1,0:T(8,128)(2,1)S(1)}, u32[]{:S(2)}, u32[]{:S(2)}) collective-permute-start(bf16[128,1024]{1,0:T(8,128)(2,1)S(1)} %fusion.7), channel_id=1, source_target_pairs={{0,1},{1,0},{2,3},{3,2},{4,5},{5,4},{6,7},{7,6},{8,9},{9,8},{10,11... | collective-permute-start | bytes 786440 | tf_op jit(solution)/shard_map/ppermute | solution.py:578
  218.3 10.4 %copy-start.11 = (f32[2048]{0:T(1024)S(1)}, f32[2048]{0:T(1024)}, u32[]{:S(2)}) copy-start(f32[2048]{0:T(1024)} %param.20) | copy-start | bytes 24580
  (4 other events, 13.5 us)
Sparse Core Ops, SparseCore 0:
  27.2 33.5 all-gather.1
  158.5 32.1 reduce-scatter.1
